TPU v7x, 128 devices: a whole 4x4x4 slice. The times are simulated.
128 devices in a mesh: ep: 32 (over z, y, core), tp: 4 (over x).
Axes of the slice: x: 4, y: 4, z: 4, core: 2. Of those that a mesh axis runs over, the one named last changes fastest.
Arguments:
- mix_input: bfloat16 [16384, 4096], P(('ep', 'tp')), may hold values from -30 to 30
- moe_input: bfloat16 [16384, 4096], P(('ep', 'tp')), may hold values from -6 to 6
- norm_mix: float32 [4096], replicated, may hold values from 0.1 to 1.9
- query_weight: bfloat16 [4096, 2048], P(None, 'tp'), may hold values from -0.09375 to 0.09375
- forget_weight: bfloat16 [4096, 2048], P(None, 'tp'), may hold values from -0.09375 to 0.09375
- value_weight: bfloat16 [4096, 2048], P(None, 'tp'), may hold values from -0.09375 to 0.09375
- forget_gap: float32 [2048], P('tp'), may hold values from 1e-05 to 0.06
- norm_out: float32 [2048], P('tp'), may hold values from 0.1 to 1.9
- norm_moe: float32 [4096], replicated, may hold values from 0.1 to 1.9
- router_weight: bfloat16 [4096, 32], replicated, may hold values from -0.09375 to 0.09375
- expert_gate: bfloat16 [32, 4096, 1024], P('ep', None, 'tp'), may hold values from -2 to 2, as said below
- expert_up: bfloat16 [32, 4096, 1024], P('ep', None, 'tp'), may hold values from -2 to 2, as said below
- expert_down: bfloat16 [32, 1024, 4096], P('ep', None, 'tp'), may hold values from -0.1875 to 0.1875
- routes: int32 [16384, 2], P('ep'), may hold values from 0 to 31, all different within a row; in each aligned block of 128 rows (0 to 127, 128 to 255, ...) at most 16 rows name the same one
Outputs:
- mixer_out: bfloat16 [16384, 2048], P('ep', 'tp')
- expert_out: bfloat16 [16384, 4096], P('ep', 'tp')
Inputs may be any that keep to these rules, and one draw needn't show every extreme that they name: `routes`: each row names 2 different experts; in each aligned block of 128 rows no expert is named by more than 16 rows. `expert_gate`: independent entries, scaled by the fan-in 4096. `expert_up`: independent entries, scaled by the fan-in 4096.
All inputs are finite; a program needn't handle non-finite values.
Results may differ from a plain program's by a relative error of at most 0.012.
The roundings to bfloat16 on the way count: a program that leaves them out, or rounds other values in their place, can miss the bound.
Values may be sent and summed in bfloat16 or wider, within the bound.
No kernel may reach another device: no remote copies, remote signals or barrier semaphores. Data moves between devices by JAX's collectives and lax.ppermute only.
A program may use at most 192 MiB of HBM per device.

v0:
```python
import functools

import jax
import jax.numpy as jnp
from jax import lax
from jax.experimental import pallas as pl
from jax.experimental.pallas import tpu as pltpu
from jax.sharding import Mesh
from jax.sharding import PartitionSpec as P

HEAD_DIM = 128

CAP = 16
HALF = 8
EP = ("ep_0", "ep_1", "ep_2")
EP_TP = ("ep_0", "ep_1", "ep_2", "tp")

EPSILON = 1e-06
CLAMP_LIMIT = 7.0
SWISH_SLOPE = 1.702
F32 = jnp.float32
BF16 = jnp.bfloat16


def mm(a, b, contract=((1,), (0,))):
    return lax.dot_general(a, b, (contract, ((), ())), preferred_element_type=F32)


def halves(a):
    high = a.astype(BF16)
    return high, (a - high.astype(F32)).astype(BF16)


def params(mib=56, axes=("arbitrary",)):
    return pltpu.CompilerParams(vmem_limit_bytes=mib << 20, dimension_semantics=axes)


def normed(row_data, gain_vec):
    as_float = row_data.astype(F32)
    scale = lax.rsqrt(jnp.mean(as_float * as_float, axis=-1, keepdims=True) + EPSILON)
    return as_float * scale * gain_vec


def chosen(routes, experts):
    toks = routes.shape[1]
    ids = lax.broadcasted_iota(jnp.int32, (experts, toks), 0)
    first = routes[0:1, :] == ids
    second = routes[1:2, :] == ids
    count = jnp.where(first | second, 1.0, 0.0)
    earlier = (
        lax.broadcasted_iota(jnp.int32, (toks, toks), 0)
        < lax.broadcasted_iota(jnp.int32, (toks, toks), 1)
    )
    before = mm(count.astype(BF16), jnp.where(earlier, 1.0, 0.0).astype(BF16))
    return first, second, count, before


def slot_matrix(weight, before, count, half):
    experts, toks = weight.shape
    place = lax.broadcasted_iota(jnp.int32, (experts, HALF, toks), 1) + half * HALF
    here = (before[:, None, :] == place.astype(F32)) & (count[:, None, :] > 0.5)
    return jnp.where(here, weight[:, None, :], 0.0).reshape(experts * HALF, toks)


def fill(routes, rows, experts):
    _, _, count, before = chosen(routes, experts)
    pick = [slot_matrix(count, before, count, half) for half in range(2)]
    both = mm(jnp.concatenate(pick, axis=0).astype(BF16), rows).astype(BF16)
    return both[: experts * HALF], both[experts * HALF :]


def front_kernel(src, x_ref, gain_ref, routes_ref, rows_ref, buf_ref, *, group):
    step = pl.program_id(0)
    width = x_ref.shape[1]

    @pl.when(step == 0)
    def _():
        rows_ref[...] = normed(x_ref[...], gain_ref[...]).astype(BF16)

    low, high = fill(routes_ref[0] - step * group, rows_ref[...], group)
    buf_ref[:, :width] = low
    buf_ref[:, width:] = high


def refill_kernel(src, own_ref, rows_ref, router_ref, routes_ref, logits_ref, low_ref, high_ref, *, group):
    step = pl.program_id(0)

    @pl.when(step == 0)
    def _():
        for k, ref in enumerate((own_ref, rows_ref)):
            logits_ref[k] = mm(router_ref[...], ref[...], ((1,), (1,))).astype(BF16)

    low_ref[...], high_ref[...] = fill(routes_ref[0] - step * group, rows_ref[...], group)


def front(src, x, gain, routes, experts):
    toks, width = x.shape
    group = 16
    whole = lambda i, s: (0, 0)
    return pl.pallas_call(
        functools.partial(front_kernel, group=group),
        grid_spec=pltpu.PrefetchScalarGridSpec(
            num_scalar_prefetch=1,
            grid=(experts // group,),
            in_specs=[
                pl.BlockSpec((toks, width), whole),
                pl.BlockSpec((1, width), whole),
                pl.BlockSpec((1, 2, toks), lambda i, s: (s[0], 0, 0)),
            ],
            out_specs=[
                pl.BlockSpec((toks, width), whole),
                pl.BlockSpec((group * HALF, 2 * width), lambda i, s: (i, 0)),
            ],
        ),
        out_shape=[
            jax.ShapeDtypeStruct((toks, width), BF16),
            jax.ShapeDtypeStruct((experts * HALF, 2 * width), BF16),
        ],
        compiler_params=params(),
        name="front",
    )(src, x, gain, routes)


def refill(src, own, rows, router, routes):
    toks, width = rows.shape
    experts = router.shape[0]
    group = 16
    whole = lambda i, s: (0, 0)
    return pl.pallas_call(
        functools.partial(refill_kernel, group=group),
        grid_spec=pltpu.PrefetchScalarGridSpec(
            num_scalar_prefetch=1,
            grid=(experts // group,),
            in_specs=[
                pl.BlockSpec((toks, width), whole),
                pl.BlockSpec((toks, width), whole),
                pl.BlockSpec(router.shape, whole),
                pl.BlockSpec((1, 2, toks), lambda i, s: (s[1], 0, 0)),
            ],
            out_specs=[
                pl.BlockSpec((2, experts, toks), lambda i, s: (0, 0, 0)),
                pl.BlockSpec((group * HALF, width), lambda i, s: (i, 0)),
                pl.BlockSpec((group * HALF, width), lambda i, s: (i, 0)),
            ],
        ),
        out_shape=[
            jax.ShapeDtypeStruct((2, experts, toks), BF16),
            jax.ShapeDtypeStruct((experts * HALF, width), BF16),
            jax.ShapeDtypeStruct((experts * HALF, width), BF16),
        ],
        compiler_params=params(),
        name="refill",
    )(src, own, rows, router, routes)


def mixer_kernel(
    src, a0, a1, a2, a3, q_ref, f_ref, v_ref, gap_ref, inside_ref, query_ref, packed_ref, qa, fa, va, group
):
    step = pl.program_id(0)

    @pl.when(step == 0)
    def _():
        qa[...] = jnp.zeros_like(qa)
        fa[...] = jnp.zeros_like(fa)
        va[...] = jnp.zeros_like(va)

    toks = a0.shape[0]
    for k, part in enumerate((a0, a1, a2, a3)):
        group[pl.ds(pl.multiple_of(src[k] * toks, toks), toks), :] = part[...]
    a = group[...]
    qa[...] += mm(a, q_ref[...])
    fa[...] += mm(a, f_ref[...])
    va[...] += mm(a, v_ref[...])

    @pl.when(step == pl.num_programs(0) - 1)
    def _():
        rows = a.shape[0]
        causal = (
            lax.broadcasted_iota(jnp.int32, (rows, rows), 0)
            >= lax.broadcasted_iota(jnp.int32, (rows, rows), 1)
        )
        ones = jnp.where(causal[:toks, :toks], 1.0, 0.0).astype(BF16)
        shut = gap_ref[...] * jax.nn.sigmoid(-fa[...])
        fa[...] = jnp.log1p(-shut)
        cols = shut.shape[1]
        base = None
        for k in range(rows // toks):
            part = fa[k * toks : (k + 1) * toks, :]
            high = part.astype(BF16)
            rest = part - high.astype(F32)
            mid = rest.astype(BF16)
            low = (rest - mid.astype(F32)).astype(BF16)
            sums = mm(ones, jnp.concatenate([high, mid, low], axis=1))
            sums = sums[:, :cols] + sums[:, cols : 2 * cols] + sums[:, 2 * cols :]
            sums = sums if base is None else sums + base
            base = sums[toks - 1 :, :]
            fa[k * toks : (k + 1) * toks, :] = sums
        sums = fa[...]
        last = sums[rows - 1 :, :]
        query_ref[...] = qa[...] * jnp.exp(sums)
        keys = shut * jnp.exp(-sums)
        late = shut * jnp.exp(last - sums)
        half = rows // 2
        for h in range(packed_ref.shape[0]):
            at = slice(h * HEAD_DIM, (h + 1) * HEAD_DIM)
            q_high, q_low = halves(query_ref[:, at])
            k_high, k_low = halves(keys[:, at])
            v_high, v_low = halves(va[:, at])
            l_high, l_low = halves(late[:, at])
            left = jnp.concatenate([q_high, q_low, q_high], axis=1)
            right = jnp.concatenate([k_high, k_high, k_low], axis=1)
            values = jnp.concatenate([v_high, v_low], axis=1)
            for k in range(2):
                end = (k + 1) * half
                scores = mm(left[end - half : end], right[:end], ((1,), (1,)))
                s_high, s_low = halves(jnp.where(causal[end - half : end, :end], scores, 0.0))
                part = mm(s_high, values[:end])
                part = part[:, :HEAD_DIM] + part[:, HEAD_DIM:] + mm(s_low, v_high[:end])
                inside_ref[end - half : end, at] = part
            outer = mm(values, jnp.concatenate([l_high, l_low], axis=1), ((0,), (0,)))
            packed_ref[h, :HEAD_DIM, :] = (
                outer[:HEAD_DIM, :HEAD_DIM]
                + outer[:HEAD_DIM, HEAD_DIM:]
                + outer[HEAD_DIM:, :HEAD_DIM]
            )
            packed_ref[h, HEAD_DIM:, :] = jnp.broadcast_to(last[:, at], (8, HEAD_DIM))


def mixer(src, parts, wq, wf, wv, gap):
    toks, width = parts[0].shape
    rows = 4 * toks
    cols = wq.shape[1]
    heads = cols // HEAD_DIM
    kb = 512
    fixed = lambda i, s: (0, 0)
    weight = pl.BlockSpec((kb, cols), lambda i, s: (i, 0))
    return pl.pallas_call(
        mixer_kernel,
        grid_spec=pltpu.PrefetchScalarGridSpec(
            num_scalar_prefetch=1,
            grid=(width // kb,),
            in_specs=[pl.BlockSpec((toks, kb), lambda i, s: (0, i))] * 4
            + [weight, weight, weight, pl.BlockSpec((1, cols), fixed)],
            out_specs=[
                pl.BlockSpec((rows, cols), fixed),
                pl.BlockSpec((rows, cols), fixed),
                pl.BlockSpec((heads, HEAD_DIM + 8, HEAD_DIM), lambda i, s: (0, 0, 0)),
            ],
            scratch_shapes=[pltpu.VMEM((rows, cols), F32)] * 3 + [pltpu.VMEM((rows, kb), BF16)],
        ),
        out_shape=[
            jax.ShapeDtypeStruct((rows, cols), F32),
            jax.ShapeDtypeStruct((rows, cols), F32),
            jax.ShapeDtypeStruct((heads, HEAD_DIM + 8, HEAD_DIM), F32),
        ],
        compiler_params=params(),
        name="mixer",
    )(src, *parts, wq, wf, wv, gap)


def readout_kernel(inside_ref, query_ref, state_ref, gain_ref, out_ref):
    q_high, q_low = halves(query_ref[...])
    s_high, s_low = halves(state_ref[0])
    total = inside_ref[...] + mm(
        jnp.concatenate([q_high, q_low, q_high], axis=1),
        jnp.concatenate([s_high, s_high, s_low], axis=1),
        ((1,), (1,)),
    )
    out_ref[...] = normed(total, gain_ref[...]).astype(BF16)


def readout(inside, query, state, gain):
    rows, cols = inside.shape
    block = pl.BlockSpec((rows, HEAD_DIM), lambda h: (0, h))
    return pl.pallas_call(
        readout_kernel,
        grid=(cols // HEAD_DIM,),
        in_specs=[
            block,
            block,
            pl.BlockSpec((1, HEAD_DIM, HEAD_DIM), lambda h: (h, 0, 0)),
            pl.BlockSpec((1, HEAD_DIM), lambda h: (0, h)),
        ],
        out_specs=block,
        out_shape=jax.ShapeDtypeStruct((rows, cols), BF16),
        compiler_params=params(),
        name="readout",
    )(inside, query, state, gain)


def pieces(packed):
    return packed[:, HEAD_DIM : HEAD_DIM + 1, :], packed[:, :HEAD_DIM, :]


def link(earlier, later):
    return earlier[0] + later[0], jnp.exp(later[0]) * earlier[1] + later[1]


def pack(part):
    heads = part[1].shape[0]
    return jnp.concatenate(
        [part[1], jnp.broadcast_to(part[0], (heads, 8, HEAD_DIM))], axis=1
    )


def masked(flag, part):
    return jax.tree.map(lambda a: jnp.where(flag, a, 0.0), part)


def both_cores(a):
    return lax.ppermute(a, "ep_2", [(0, 1), (1, 0)])


def along_rows(packed):
    core = lax.axis_index("ep_2")
    other = both_cores(packed)
    is_second = core == 1
    low = jnp.where(is_second, other, packed)
    high = jnp.where(is_second, packed, other)
    half = packed.shape[0] // 2
    mine = lambda a: lax.dynamic_slice_in_dim(a, core * half, half, 0)
    chip = link(pieces(mine(low)), pieces(mine(high)))
    count = lax.axis_size("ep_1")
    sent = pack(chip)
    came = [
        lax.ppermute(sent, "ep_1", [(i, (i + d) % count) for i in range(count)])
        for d in range(count - 1, 0, -1)
    ]
    return low, chip, came


def along_planes(chip, came):
    row = lax.axis_index("ep_1")
    before = after = None
    for k, part in enumerate(came):
        d = len(came) - k
        early = masked(row >= d, pieces(part))
        late = masked(row < d, pieces(part))
        before = early if before is None else link(before, early)
        after = late if after is None else link(after, late)
    plane = pack(link(link(before, chip), after))
    count = lax.axis_size("ep_0")
    planes = [
        lax.ppermute(plane, "ep_0", [(i, i + d) for i in range(count - d)])
        for d in range(count - 1, 0, -1)
    ]
    return before, planes


def arriving_state(low, before, planes):
    is_second = lax.axis_index("ep_2") == 1
    total = None
    for part in planes:
        total = pieces(part) if total is None else link(total, pieces(part))
    state = link(total, before)[1]
    swapped = both_cores(state)
    entering = jnp.concatenate(
        [jnp.where(is_second, swapped, state), jnp.where(is_second, state, swapped)], axis=0
    )
    first_core = pieces(low)
    return jnp.where(is_second, jnp.exp(first_core[0]) * entering + first_core[1], entering)


def hidden_kernel(own_ref, near_ref, go_ref, uo_ref, gf_ref, uf_ref, out_ref, gate, up):
    step = pl.program_id(0)

    @pl.when(step == 0)
    def _():
        gate[...] = jnp.zeros_like(gate)
        up[...] = jnp.zeros_like(up)

    rows = jnp.concatenate([own_ref[...], near_ref[...]], axis=0)
    n = go_ref.shape[1]
    gate[:, :n] += mm(rows, go_ref[...])
    gate[:, n:] += mm(rows, gf_ref[...])
    up[:, :n] += mm(rows, uo_ref[...])
    up[:, n:] += mm(rows, uf_ref[...])

    @pl.when(step == pl.num_programs(0) - 1)
    def _():
        gated = jnp.minimum(gate[...], CLAMP_LIMIT)
        opened = jnp.clip(up[...], -CLAMP_LIMIT, CLAMP_LIMIT)
        out_ref[...] = (
            (opened + 1.0) * gated * jax.nn.sigmoid(SWISH_SLOPE * gated)
        ).astype(BF16)


def hidden_units(own, near, half, weights):
    count = own.shape[0]
    width, n = weights[0].shape
    kb = 1024
    weight = pl.BlockSpec((kb, n), lambda i: (i, 0))
    return pl.pallas_call(
        hidden_kernel,
        grid=(width // kb,),
        in_specs=[
            pl.BlockSpec((count, kb), lambda i: (0, i + half * (width // kb))),
            pl.BlockSpec((count, kb), lambda i: (0, i)),
            weight,
            weight,
            weight,
            weight,
        ],
        out_specs=pl.BlockSpec((2 * count, 2 * n), lambda i: (0, 0)),
        out_shape=jax.ShapeDtypeStruct((2 * count, 2 * n), BF16),
        scratch_shapes=[pltpu.VMEM((2 * count, 2 * n), F32)] * 2,
        compiler_params=params(),
        name="hidden",
    )(own, near, *weights)


def down_kernel(src, h_own, h_near, h_far, h_opp, down_ref, out_ref):
    k = pl.program_id(0)
    n = down_ref.shape[0] // 4
    rows = out_ref.shape[0]
    unit = lambda s: down_ref[pl.ds(pl.multiple_of(s * n, n), n), :]
    for this, (mine, other, twin) in enumerate(
        ((h_own, h_near, 1), (h_near, h_own, 0), (h_far, h_opp, 3), (h_opp, h_far, 2))
    ):

        @pl.when(k == this)
        def _():
            s, t = src[this], src[twin]
            total = mm(mine[:rows, :n], unit(s)) + mm(mine[:rows, n:], unit(3 - s))
            total += mm(other[rows:, :n], unit(t)) + mm(other[rows:, n:], unit(3 - t))
            out_ref[...] = total.astype(BF16)


def down_rows(src, parts, down):
    both, width = parts[0].shape
    cols = down.shape[1]
    whole = lambda k, s: (0, 0)
    return pl.pallas_call(
        down_kernel,
        grid_spec=pltpu.PrefetchScalarGridSpec(
            num_scalar_prefetch=1,
            grid=(4,),
            in_specs=[pl.BlockSpec((both, width), whole)] * 4 + [pl.BlockSpec(down.shape, whole)],
            out_specs=pl.BlockSpec((both // 2, cols), lambda k, s: (0, s[k])),
        ),
        out_shape=jax.ShapeDtypeStruct((both // 2, 4 * cols), BF16),
        compiler_params=params(),
        name="down",
    )(src, *parts, down)


def places_kernel(src, routes_ref, logits_ref, out_ref):
    experts = logits_ref.shape[1]
    first, second, count, before = chosen(routes_ref[0], experts)
    logits = logits_ref[0].astype(F32)
    l0 = jnp.sum(jnp.where(first, logits, 0.0), axis=0, keepdims=True)
    l1 = jnp.sum(jnp.where(second, logits, 0.0), axis=0, keepdims=True)
    w0 = 1.0 / (1.0 + jnp.exp(l1 - l0))
    w1 = 1.0 / (1.0 + jnp.exp(l0 - l1))
    weight = jnp.where(first, w0, 0.0) + jnp.where(second, w1, 0.0)
    both = [slot_matrix(weight, before, count, half) for half in range(2)]
    place = jnp.concatenate(both, axis=0).T
    out_ref[0] = jnp.concatenate(halves(place), axis=0)


def places(src, routes, logits):
    experts, toks = logits.shape[1:]
    return pl.pallas_call(
        places_kernel,
        grid_spec=pltpu.PrefetchScalarGridSpec(
            num_scalar_prefetch=1,
            grid=(4,),
            in_specs=[
                pl.BlockSpec((1, 2, toks), lambda k, s: (s[k], 0, 0)),
                pl.BlockSpec((1, experts, toks), lambda k, s: (k, 0, 0)),
            ],
            out_specs=pl.BlockSpec((1, 2 * toks, experts * CAP), lambda k, s: (k, 0, 0)),
        ),
        out_shape=jax.ShapeDtypeStruct((4, 2 * toks, experts * CAP), BF16),
        compiler_params=params(),
        name="places",
    )(src, routes, logits)


def combine_kernel(src, low_ref, high_ref, place_ref, out_ref):
    slots = low_ref.shape[0]
    total = mm(place_ref[0, :, :slots], low_ref[...]) + mm(place_ref[0, :, slots:], high_ref[...])
    toks = out_ref.shape[0]
    out_ref[...] = (total[:toks] + total[toks:]).astype(BF16)


def combined(src, low, high, place):
    slots = low.shape[0]
    cols = low.shape[1] // 4
    toks = place.shape[1] // 2
    res = pl.BlockSpec((slots, cols), lambda k, s: (0, s[k]))
    return pl.pallas_call(
        combine_kernel,
        grid_spec=pltpu.PrefetchScalarGridSpec(
            num_scalar_prefetch=1,
            grid=(4,),
            in_specs=[
                res,
                res,
                pl.BlockSpec((1,) + place.shape[1:], lambda k, s: (k, 0, 0)),
            ],
            out_specs=pl.BlockSpec((toks, cols), lambda k, s: (s[k], 0)),
        ),
        out_shape=jax.ShapeDtypeStruct((4 * toks, cols), BF16),
        compiler_params=params(),
        name="combine",
    )(src, low, high, place)


NEAR = [(i, i ^ 1) for i in range(4)]
FAR = [(i, 3 - i) for i in range(4)]


def to_near(a):
    return lax.ppermute(a, "tp", NEAR)


def to_far(a):
    return lax.ppermute(a, "tp", FAR)


def shared(a):
    far = to_far(a)
    near = to_near(a)
    return a, near, far, to_near(far)


def swap(a):
    experts = 32
    rows, cols = a.shape
    out = lax.all_to_all(
        a.reshape(experts, rows // experts, cols), EP, split_axis=0, concat_axis=0, tiled=True
    )
    return out.reshape(rows, cols)


def per_device(
    mix_input,
    moe_input,
    norm_mix,
    query_weight,
    forget_weight,
    value_weight,
    forget_gap,
    norm_out,
    norm_moe,
    router_weight,
    expert_gate,
    expert_up,
    expert_down,
    routes,
):
    toks = moe_input.shape[0]
    x = lax.axis_index("tp").astype(jnp.int32)
    src = jnp.stack([x, x ^ 1, 3 - x, x ^ 2])
    by_block = routes.reshape(4, toks, 2).transpose(0, 2, 1)
    router = router_weight.T

    rows_a = normed(mix_input, norm_mix).astype(BF16)
    group_a = shared(rows_a)
    rows_b, own = front(src, moe_input, norm_moe.reshape(1, -1), by_block, router_weight.shape[1])
    own_rows = swap(own)
    rows_near = to_near(rows_b)
    gate_far = to_far(expert_gate[0])
    up_far = to_far(expert_up[0])
    logits, low, high = refill(src, rows_b, rows_near, router, by_block)
    low, own_rows = lax.optimization_barrier((low, own_rows))
    low_rows = swap(low)
    high, low_rows = lax.optimization_barrier((high, low_rows))
    high_rows = swap(high)
    logits = jnp.concatenate([logits, to_far(logits)])
    place = places(src, by_block, logits)

    inside, query, packed = mixer(
        src, group_a, query_weight, forget_weight, value_weight, forget_gap.reshape(1, -1)
    )
    first_core, chip, came = along_rows(packed)

    low_rows, packed = lax.optimization_barrier((low_rows, packed))
    weights = (expert_gate[0], expert_up[0], gate_far, up_far)
    h_low = hidden_units(own_rows, low_rows, 0, weights)
    h_low = shared(h_low)
    high_rows, far = lax.optimization_barrier((high_rows, h_low[2]))
    h_high = hidden_units(own_rows, high_rows, 1, weights)
    h_high = shared(h_high)
    opp, high_own = lax.optimization_barrier((h_low[3], h_high[0]))
    down_low = down_rows(src, h_low[:2] + (far, opp), expert_down[0])
    back_low = swap(down_low)
    came, _ = lax.optimization_barrier((came, down_low))
    before, planes = along_planes(chip, came)
    down_high = down_rows(src, (high_own,) + h_high[1:], expert_down[0])
    back_high = swap(down_high)
    planes, _ = lax.optimization_barrier((planes, down_high))

    state = arriving_state(first_core, before, planes)
    mixer_out = readout(inside, query, state, norm_out.reshape(1, -1))
    expert_out = combined(src, back_low, back_high, place)
    return (mixer_out, expert_out)


def solution(mesh):
    finer = Mesh(mesh.devices.reshape(4, 4, 2, mesh.shape["tp"]), ("ep_0", "ep_1", "ep_2", "tp"))
    placed = (
        P(EP_TP, None),
        P(EP_TP, None),
        P(),
        P(None, "tp"),
        P(None, "tp"),
        P(None, "tp"),
        P("tp"),
        P("tp"),
        P(),
        P(),
        P(EP, None, "tp"),
        P(EP, None, "tp"),
        P(EP, None, "tp"),
        P(EP, None),
    )

    return jax.shard_map(
        per_device,
        mesh=finer,
        in_specs=placed,
        out_specs=(P(EP, "tp"), P(EP, "tp")),
        check_vma=False,
    )
```

profile of v0, /device:TPU:8, one launch (start us, length us, event | category | flops | bytes accessed | tf_op | source)
XLA Modules:
  0.0 344.2 jit_solution(1780788532820483332)
XLA Ops:
  1.3 5.8 %front.1 = (bf16[128,4096]{1,0:T(8,128)(2,1)}, bf16[256,8192]{1,0:T(8,128)(2,1)}) custom-call(s32[4]{0:T(128)} %pad_add_fusion.src, bf16[128,4096]{1,0:T(8,128)(2,1)} %x_ref.1, f32[1,4096]{1,0:T(1,128)} %bitcast.50, s32[4,2,128]{2,1,0:T(2,128)} %bitcast.47), custom_call_target="tpu_custom_call" | custom-call | tf_op jit(solution)/shard_map/front/pallas_call | solution.py:100
  7.0 8.7 %all-to-all-start = ((bf16[32,8,8192]{2,1,0:T(8,128)(2,1)}), bf16[32,8,8192]{2,1,0:T(8,128)(2,1)}, u32[]{:S(2)}, u32[]{:S(2)}) async-start(bf16[32,8,8192]{2,1,0:T(8,128)(2,1)} %bitcast.43), calls=%async_computation | async-start | bytes 8388608 | tf_op jit(solution)/shard_map/all_to_all | solution.py:531
  15.8 1.6 collective-permute-start.7
  17.7 23.4 %collective-permute-done.7.rows_ref = bf16[128,4096]{1,0:T(8,128)(2,1)S(1)} collective-permute-done((bf16[128,4096]{1,0:T(8,128)(2,1)S(1)}, bf16[128,4096]{1,0:T(8,128)(2,1)S(1)}, u32[]{:S(2)}, u32[]{:S(2)}) %collective-permute-start.7) | collective-permute-done | bytes 1048608 | tf_op jit(solution)/shard_map/ppermute | solution.py:515
  41.1 1.0 copy-done.5
  42.0 6.0 %refill.1 = (bf16[2,32,128]{2,1,0:T(8,128)(2,1)}, bf16[256,4096]{1,0:T(8,128)(2,1)}, bf16[256,4096]{1,0:T(8,128)(2,1)}) custom-call(s32[4]{0:T(128)} %pad_add_fusion.src, bf16[128,4096]{1,0:T(8,128)(2,1)} %get-tuple-element.28.own_ref, bf16[128,4096]{1,0:T(8,128)(2,1)} %copy-done.5, bf16[32,4096]{1,0:T(8,128)(2,1)} %bitcast.46, s32[4,2,128]{2,1,0:T(2,128)} %bitcast.48), custom_call_target="tpu_custom_call" | custom-call | tf_op jit(solution)/shard_map/refill/pallas_call | solution.py:129
  48.1 19.2 %all-to-all-done = bf16[32,8,8192]{2,1,0:T(8,128)(2,1)} async-done(((bf16[32,8,8192]{2,1,0:T(8,128)(2,1)}), bf16[32,8,8192]{2,1,0:T(8,128)(2,1)}, u32[]{:S(2)}, u32[]{:S(2)}) %all-to-all-start) | async-done | bytes 4194336 | tf_op jit(solution)/shard_map/all_to_all | solution.py:531
  67.2 6.6 %all-to-all-start.1 = ((bf16[32,8,4096]{2,1,0:T(8,128)(2,1)}), bf16[32,8,4096]{2,1,0:T(8,128)(2,1)S(1)}, u32[]{:S(2)}, u32[]{:S(2)}) async-start(bf16[32,8,4096]{2,1,0:T(8,128)(2,1)} %bitcast.45), calls=%async_computation.1 | async-start | bytes 4194304 | tf_op jit(solution)/shard_map/all_to_all | solution.py:531
  73.9 1.3 fusion.2.a0
  75.2 2.8 collective-permute-start.1
  78.4 2.8 collective-permute-start.9
  81.2 21.5 %collective-permute-done.1.a2 = bf16[128,4096]{1,0:T(8,128)(2,1)S(1)} collective-permute-done((bf16[128,4096]{1,0:T(8,128)(2,1)}, bf16[128,4096]{1,0:T(8,128)(2,1)S(1)}, u32[]{:S(2)}, u32[]{:S(2)}) %collective-permute-start.1) | collective-permute-done | bytes 1048608 | tf_op jit(solution)/shard_map/ppermute | solution.py:519
  104.3 7.5 %all-to-all-start.2 = ((bf16[32,8,4096]{2,1,0:T(8,128)(2,1)}), bf16[32,8,4096]{2,1,0:T(8,128)(2,1)}, u32[]{:S(2)}, u32[]{:S(2)}) async-start(bf16[32,8,4096]{2,1,0:T(8,128)(2,1)} %bitcast.44), calls=%async_computation.2 | async-start | bytes 4194304 | tf_op jit(solution)/shard_map/all_to_all | solution.py:531
  111.8 16.5 %collective-permute-done.2.a3 = bf16[128,4096]{1,0:T(8,128)(2,1)} collective-permute-done((bf16[128,4096]{1,0:T(8,128)(2,1)S(1)}, bf16[128,4096]{1,0:T(8,128)(2,1)}, u32[]{:S(2)}, u32[]{:S(2)}) %collective-permute-start.2) | collective-permute-done | bytes 1048608 | tf_op jit(solution)/shard_map/ppermute | solution.py:515
  128.3 17.5 %mixer.1 = (f32[512,512]{1,0:T(8,128)}, f32[512,512]{1,0:T(8,128)}, f32[4,136,128]{2,1,0:T(8,128)}) custom-call(s32[4]{0:T(128)} %pad_add_fusion.src, bf16[128,4096]{1,0:T(8,128)(2,1)} %fusion.2.a0, bf16[128,4096]{1,0:T(8,128)(2,1)} %collective-permute-done.a1, bf16[128,4096]{1,0:T(8,128)(2,1)} %copy-done.6, bf16[128,4096]{1,0:T(8,128)(2,1)} %collective-permute-done.2.a3, ...), custom_call_target="tpu_custom_call" | custom-call | tf_op jit(solution)/shard_map/mixer/pallas_call | solution.py:237
  145.9 1.8 collective-permute-done.8.gf_ref
  147.7 44.1 %collective-permute-done.9.uf_ref = bf16[4096,256]{1,0:T(8,128)(2,1)} collective-permute-done((bf16[4096,256]{1,0:T(8,128)(2,1)}, bf16[4096,256]{1,0:T(8,128)(2,1)}, u32[]{:S(2)}, u32[]{:S(2)}) %collective-permute-start.9) | collective-permute-done | bytes 2097184 | tf_op jit(solution)/shard_map/ppermute | solution.py:519
  191.8 8.8 %hidden.2.h_own = bf16[512,512]{1,0:T(8,128)(2,1)} custom-call(bf16[256,8192]{1,0:T(8,128)(2,1)} %bitcast.13.own_ref, bf16[256,4096]{1,0:T(8,128)(2,1)} %bitcast.42, bf16[4096,256]{1,0:T(8,128)(2,1)} %bitcast.16.go_ref, bf16[4096,256]{1,0:T(8,128)(2,1)} %bitcast.17.uo_ref, bf16[4096,256]{1,0:T(8,128)(2,1)} %collective-permute-done.8.gf_ref, ...), custom_call_target="tpu_custom_call" | custom-call | tf_op jit(solution)/shard_map/hidden/pallas_call | solution.py:393
  200.6 2.8 collective-permute-start.11
  203.4 11.8 %collective-permute-done.11.h_far = bf16[512,512]{1,0:T(8,128)(2,1)S(1)} collective-permute-done((bf16[512,512]{1,0:T(8,128)(2,1)}, bf16[512,512]{1,0:T(8,128)(2,1)S(1)}, u32[]{:S(2)}, u32[]{:S(2)}) %collective-permute-start.11) | collective-permute-done | bytes 524320 | tf_op jit(solution)/shard_map/ppermute | solution.py:519
  215.1 2.0 collective-permute-start.10
  217.2 8.9 %hidden.3.h_own = bf16[512,512]{1,0:T(8,128)(2,1)} custom-call(bf16[256,8192]{1,0:T(8,128)(2,1)} %bitcast.13.own_ref, bf16[256,4096]{1,0:T(8,128)(2,1)} %bitcast.19.near_ref, bf16[4096,256]{1,0:T(8,128)(2,1)} %bitcast.16.go_ref, bf16[4096,256]{1,0:T(8,128)(2,1)} %bitcast.17.uo_ref, bf16[4096,256]{1,0:T(8,128)(2,1)} %collective-permute-done.8.gf_ref, ...), custom_call_target="tpu_custom_call" | custom-call | tf_op jit(solution)/shard_map/hidden/pallas_call | solution.py:393
  226.0 3.9 %collective-permute-done.12.h_opp = bf16[512,512]{1,0:T(8,128)(2,1)S(1)} collective-permute-done((bf16[512,512]{1,0:T(8,128)(2,1)S(1)}, bf16[512,512]{1,0:T(8,128)(2,1)S(1)}, u32[]{:S(2)}, u32[]{:S(2)}) %collective-permute-start.12) | collective-permute-done | bytes 524320 | tf_op jit(solution)/shard_map/ppermute | solution.py:515
  229.9 8.7 %collective-permute-done.10.h_near = bf16[512,512]{1,0:T(8,128)(2,1)S(1)} collective-permute-done((bf16[512,512]{1,0:T(8,128)(2,1)}, bf16[512,512]{1,0:T(8,128)(2,1)S(1)}, u32[]{:S(2)}, u32[]{:S(2)}) %collective-permute-start.10) | collective-permute-done | bytes 524320 | tf_op jit(solution)/shard_map/ppermute | solution.py:515
  238.6 0.8 copy-done.11
  239.4 6.8 %down.2 = bf16[256,4096]{1,0:T(8,128)(2,1)} custom-call(s32[4]{0:T(128)} %pad_add_fusion.src, bf16[512,512]{1,0:T(8,128)(2,1)} %hidden.2.h_own, bf16[512,512]{1,0:T(8,128)(2,1)} %copy-done.11, bf16[512,512]{1,0:T(8,128)(2,1)} %copy-done.9, bf16[512,512]{1,0:T(8,128)(2,1)} %copy-done.10, bf16[1024,1024]{1,0:T(8,128)(2,1)} %bitcast.37), custom_call_target="tpu_custom_call" | custom-call | tf_op jit(solution)/shard_map/down/pallas_call | solution.py:433
  246.2 7.6 %all-to-all-start.3 = ((bf16[32,8,4096]{2,1,0:T(8,128)(2,1)}), bf16[32,8,4096]{2,1,0:T(8,128)(2,1)S(1)}, u32[]{:S(2)}, u32[]{:S(2)}) async-start(bf16[32,8,4096]{2,1,0:T(8,128)(2,1)} %bitcast.41), calls=%async_computation.3 | async-start | bytes 4194304 | tf_op jit(solution)/shard_map/all_to_all | solution.py:531
  254.0 2.7 collective-permute-start.17
  256.9 12.6 %collective-permute-done.17.h_far = bf16[512,512]{1,0:T(8,128)(2,1)} collective-permute-done((bf16[512,512]{1,0:T(8,128)(2,1)S(1)}, bf16[512,512]{1,0:T(8,128)(2,1)}, u32[]{:S(2)}, u32[]{:S(2)}) %collective-permute-start.17) | collective-permute-done | bytes 524320 | tf_op jit(solution)/shard_map/ppermute | solution.py:519
  271.1 2.7 collective-permute-start.5
  273.8 1.8 collective-permute-start.6
  275.6 7.9 %collective-permute-done.4 = f32[2,136,128]{2,1,0:T(8,128)} collective-permute-done((f32[2,136,128]{2,1,0:T(8,128)}, f32[2,136,128]{2,1,0:T(8,128)}, u32[]{:S(2)}, u32[]{:S(2)}) %collective-permute-start.4) | collective-permute-done | bytes 139296 | tf_op jit(solution)/shard_map/ppermute | solution.py:326
  283.5 2.4 collective-permute-done.5
  286.7 6.8 %down.3 = bf16[256,4096]{1,0:T(8,128)(2,1)} custom-call(s32[4]{0:T(128)} %pad_add_fusion.src, bf16[512,512]{1,0:T(8,128)(2,1)} %hidden.3.h_own, bf16[512,512]{1,0:T(8,128)(2,1)} %copy-done.8, bf16[512,512]{1,0:T(8,128)(2,1)} %collective-permute-done.17.h_far, bf16[512,512]{1,0:T(8,128)(2,1)} %collective-permute-done.18.h_opp, bf16[1024,1024]{1,0:T(8,128)(2,1)} %bitcast.38), custom_call_target="tpu_custom_call" | custom-call | tf_op jit(solution)/shard_map/down/pallas_call | solution.py:433
  293.5 1.3 copy-done
  294.9 7.0 %all-to-all-start.4 = ((bf16[32,8,4096]{2,1,0:T(8,128)(2,1)}), bf16[32,8,4096]{2,1,0:T(8,128)(2,1)}, u32[]{:S(2)}, u32[]{:S(2)}) async-start(bf16[32,8,4096]{2,1,0:T(8,128)(2,1)} %bitcast.40), calls=%async_computation.4 | async-start | bytes 4194304 | tf_op jit(solution)/shard_map/all_to_all | solution.py:531
  302.7 1.1 add_add_fusion
  303.8 4.6 %collective-permute-start.13 = (f32[2,136,128]{2,1,0:T(8,128)S(1)}, f32[2,136,128]{2,1,0:T(8,128)S(1)}, u32[]{:S(2)}, u32[]{:S(2)}) collective-permute-start(f32[2,136,128]{2,1,0:T(8,128)S(1)} %pad_maximum_fusion.2), channel_id=1, source_target_pairs={{0,96},{1,97},{2,98},{3,99},{4,100},{5,101},{6,102},{7,103},{8,104... | collective-permute-start | bytes 417800 | tf_op jit(solution)/shard_map/ppermute | solution.py:344
  308.5 1.3 collective-permute-start.14
  309.8 2.8 collective-permute-start.15
  312.6 2.8 collective-permute-start.20
  315.4 2.2 collective-permute-done.20
  318.2 4.1 %places.1.place_ref = bf16[4,256,512]{2,1,0:T(8,128)(2,1)} custom-call(s32[4]{0:T(128)} %pad_add_fusion.src, s32[4,2,128]{2,1,0:T(2,128)} %bitcast.49, bf16[4,32,128]{2,1,0:T(8,128)(2,1)} %pad_maximum_fusion.3.logits_ref), custom_call_target="tpu_custom_call" | custom-call | tf_op jit(solution)/shard_map/places/pallas_call | solution.py:463
  322.3 8.6 %collective-permute-done.13 = f32[2,136,128]{2,1,0:T(8,128)S(1)} collective-permute-done((f32[2,136,128]{2,1,0:T(8,128)S(1)}, f32[2,136,128]{2,1,0:T(8,128)S(1)}, u32[]{:S(2)}, u32[]{:S(2)}) %collective-permute-start.13) | collective-permute-done | bytes 139296 | tf_op jit(solution)/shard_map/ppermute | solution.py:344
  331.1 1.1 multiply_add_fusion
  332.3 1.3 collective-permute-done.19
  334.4 4.2 %readout.1 = bf16[512,512]{1,0:T(8,128)(2,1)} custom-call(f32[512,512]{1,0:T(8,128)} %get-tuple-element.25.inside_ref, f32[512,512]{1,0:T(8,128)} %get-tuple-element.26.query_ref, f32[4,128,128]{2,1,0:T(8,128)} %fusion.3.state_ref, f32[1,512]{1,0:T(1,128)} %bitcast.66), custom_call_target="tpu_custom_call" | custom-call | tf_op jit(solution)/shard_map/readout/pallas_call | solution.py:275
  338.6 5.6 %combine.1 = bf16[512,1024]{1,0:T(8,128)(2,1)} custom-call(s32[4]{0:T(128)} %pad_add_fusion.src, bf16[256,4096]{1,0:T(8,128)(2,1)} %bitcast.39, bf16[256,4096]{1,0:T(8,128)(2,1)} %bitcast.35.high_ref, bf16[4,256,512]{2,1,0:T(8,128)(2,1)} %places.1.place_ref), custom_call_target="tpu_custom_call" | custom-call | tf_op jit(solution)/shard_map/combine/pallas_call | solution.py:492
  (69 shorter events, 8.2 us)
Async XLA Ops:
  7.0 8.8 %copy-start.4 = (bf16[128,4096]{1,0:T(8,128)(2,1)S(1)}, bf16[128,4096]{1,0:T(8,128)(2,1)}, u32[]{:S(2)}) copy-start(bf16[128,4096]{1,0:T(8,128)(2,1)} %get-tuple-element.28.own_ref) | copy-start | bytes 3145732
  7.0 10.3 %copy-start.2 = (bf16[128,4096]{1,0:T(8,128)(2,1)S(1)}, bf16[128,4096]{1,0:T(8,128)(2,1)}, u32[]{:S(2)}) copy-start(bf16[128,4096]{1,0:T(8,128)(2,1)} %param.14) | copy-start | bytes 3145732
  7.0 60.2 %all-to-all-start = ((bf16[32,8,8192]{2,1,0:T(8,128)(2,1)}), bf16[32,8,8192]{2,1,0:T(8,128)(2,1)}, u32[]{:S(2)}, u32[]{:S(2)}) async-start(bf16[32,8,8192]{2,1,0:T(8,128)(2,1)} %bitcast.43), calls=%async_computation | async-start | bytes 8388608 | tf_op jit(solution)/shard_map/all_to_all | solution.py:531
  15.8 25.3 %collective-permute-start.7 = (bf16[128,4096]{1,0:T(8,128)(2,1)S(1)}, bf16[128,4096]{1,0:T(8,128)(2,1)S(1)}, u32[]{:S(2)}, u32[]{:S(2)}) collective-permute-start(bf16[128,4096]{1,0:T(8,128)(2,1)S(1)} %copy-done.4), channel_id=1, source_target_pairs={{0,1},{1,0},{2,3},{3,2},{4,5},{5,4},{6,7},{7,6},{8,9},{9,8},{10,11... | collective-permute-start | bytes 3145736 | tf_op jit(solution)/shard_map/ppermute | solution.py:515
  41.1 1.0 copy-start.5
  67.2 6.7 %copy-start.12 = (f32[4096]{0:T(1024)S(1)}, f32[4096]{0:T(1024)}, u32[]{:S(2)}) copy-start(f32[4096]{0:T(1024)} %param.16) | copy-start | bytes 49156
  67.2 35.7 %all-to-all-start.1 = ((bf16[32,8,4096]{2,1,0:T(8,128)(2,1)}), bf16[32,8,4096]{2,1,0:T(8,128)(2,1)S(1)}, u32[]{:S(2)}, u32[]{:S(2)}) async-start(bf16[32,8,4096]{2,1,0:T(8,128)(2,1)} %bitcast.45), calls=%async_computation.1 | async-start | bytes 4194304 | tf_op jit(solution)/shard_map/all_to_all | solution.py:531
  75.2 27.5 %collective-permute-start.1 = (bf16[128,4096]{1,0:T(8,128)(2,1)}, bf16[128,4096]{1,0:T(8,128)(2,1)S(1)}, u32[]{:S(2)}, u32[]{:S(2)}) collective-permute-start(bf16[128,4096]{1,0:T(8,128)(2,1)} %fusion.2.a0), channel_id=1, source_target_pairs={{0,3},{1,2},{2,1},{3,0},{4,7},{5,6},{6,5},{7,4},{8,11},{9,10},{10,... | collective-permute-start | bytes 3145736 | tf_op jit(solution)/shard_map/ppermute | solution.py:519
  77.9 69.7 %collective-permute-start.8 = (bf16[4096,256]{1,0:T(8,128)(2,1)}, bf16[4096,256]{1,0:T(8,128)(2,1)}, u32[]{:S(2)}, u32[]{:S(2)}) collective-permute-start(bf16[4096,256]{1,0:T(8,128)(2,1)} %bitcast.16.go_ref), channel_id=1, source_target_pairs={{0,3},{1,2},{2,1},{3,0},{4,7},{5,6},{6,5},{7,4},{8,11},{9,10},{10,... | collective-permute-start | bytes 6291464 | tf_op jit(solution)/shard_map/ppermute | solution.py:519
  78.4 113.4 %collective-permute-start.9 = (bf16[4096,256]{1,0:T(8,128)(2,1)}, bf16[4096,256]{1,0:T(8,128)(2,1)}, u32[]{:S(2)}, u32[]{:S(2)}) collective-permute-start(bf16[4096,256]{1,0:T(8,128)(2,1)} %bitcast.17.uo_ref), channel_id=1, source_target_pairs={{0,3},{1,2},{2,1},{3,0},{4,7},{5,6},{6,5},{7,4},{8,11},{9,10},{10,... | collective-permute-start | bytes 6291464 | tf_op jit(solution)/shard_map/ppermute | solution.py:519
  81.2 30.7 %collective-permute-start = (bf16[128,4096]{1,0:T(8,128)(2,1)}, bf16[128,4096]{1,0:T(8,128)(2,1)}, u32[]{:S(2)}, u32[]{:S(2)}) collective-permute-start(bf16[128,4096]{1,0:T(8,128)(2,1)} %fusion.2.a0), channel_id=1, source_target_pairs={{0,1},{1,0},{2,3},{3,2},{4,5},{5,4},{6,7},{7,6},{8,9},{9,8},{10,11... | collective-permute-start | bytes 3145736 | tf_op jit(solution)/shard_map/ppermute | solution.py:515
  102.6 1.0 copy-start.6
  102.6 25.7 %collective-permute-start.2 = (bf16[128,4096]{1,0:T(8,128)(2,1)S(1)}, bf16[128,4096]{1,0:T(8,128)(2,1)}, u32[]{:S(2)}, u32[]{:S(2)}) collective-permute-start(bf16[128,4096]{1,0:T(8,128)(2,1)S(1)} %collective-permute-done.1.a2), channel_id=1, source_target_pairs={{0,1},{1,0},{2,3},{3,2},{4,5},{5,4},{6,7},{7,6},{8,9},{9,8},{10,11... | collective-permute-start | bytes 3145736 | tf_op jit(solution)/shard_map/ppermute | solution.py:515
  102.9 1.4 copy-start.1
  104.3 112.9 %all-to-all-start.2 = ((bf16[32,8,4096]{2,1,0:T(8,128)(2,1)}), bf16[32,8,4096]{2,1,0:T(8,128)(2,1)}, u32[]{:S(2)}, u32[]{:S(2)}) async-start(bf16[32,8,4096]{2,1,0:T(8,128)(2,1)} %bitcast.44), calls=%async_computation.2 | async-start | bytes 4194304 | tf_op jit(solution)/shard_map/all_to_all | solution.py:531
  200.6 14.5 %collective-permute-start.11 = (bf16[512,512]{1,0:T(8,128)(2,1)}, bf16[512,512]{1,0:T(8,128)(2,1)S(1)}, u32[]{:S(2)}, u32[]{:S(2)}) collective-permute-start(bf16[512,512]{1,0:T(8,128)(2,1)} %hidden.2.h_own), channel_id=1, source_target_pairs={{0,3},{1,2},{2,1},{3,0},{4,7},{5,6},{6,5},{7,4},{8,11},{9,10},{10,... | collective-permute-start | bytes 1572872 | tf_op jit(solution)/shard_map/ppermute | solution.py:519
  215.1 10.9 %copy-start.9 = (bf16[512,512]{1,0:T(8,128)(2,1)}, bf16[512,512]{1,0:T(8,128)(2,1)S(1)}, u32[]{:S(2)}) copy-start(bf16[512,512]{1,0:T(8,128)(2,1)S(1)} %collective-permute-done.11.h_far) | copy-start | bytes 1572868
  215.1 14.8 %collective-permute-start.12 = (bf16[512,512]{1,0:T(8,128)(2,1)S(1)}, bf16[512,512]{1,0:T(8,128)(2,1)S(1)}, u32[]{:S(2)}, u32[]{:S(2)}) collective-permute-start(bf16[512,512]{1,0:T(8,128)(2,1)S(1)} %collective-permute-done.11.h_far), channel_id=1, source_target_pairs={{0,1},{1,0},{2,3},{3,2},{4,5},{5,4},{6,7},{7,6},{8,9},{9,8},{10,11... | collective-permute-start | bytes 1572872 | tf_op jit(solution)/shard_map/ppermute | solution.py:515
  215.1 23.5 %collective-permute-start.10 = (bf16[512,512]{1,0:T(8,128)(2,1)}, bf16[512,512]{1,0:T(8,128)(2,1)S(1)}, u32[]{:S(2)}, u32[]{:S(2)}) collective-permute-start(bf16[512,512]{1,0:T(8,128)(2,1)} %hidden.2.h_own), channel_id=1, source_target_pairs={{0,1},{1,0},{2,3},{3,2},{4,5},{5,4},{6,7},{7,6},{8,9},{9,8},{10,11... | collective-permute-start | bytes 1572872 | tf_op jit(solution)/shard_map/ppermute | solution.py:515
  229.9 8.7 %copy-start.10 = (bf16[512,512]{1,0:T(8,128)(2,1)}, bf16[512,512]{1,0:T(8,128)(2,1)S(1)}, u32[]{:S(2)}) copy-start(bf16[512,512]{1,0:T(8,128)(2,1)S(1)} %collective-permute-done.12.h_opp) | copy-start | bytes 1572868
  238.6 0.8 copy-start.11
  246.2 7.6 %copy-start.7 = (f32[4,136,128]{2,1,0:T(8,128)S(1)}, f32[4,136,128]{2,1,0:T(8,128)}, u32[]{:S(2)}) copy-start(f32[4,136,128]{2,1,0:T(8,128)} %get-tuple-element.27) | copy-start | bytes 835588
  246.2 7.8 %copy-start.3 = (bf16[512,512]{1,0:T(8,128)(2,1)S(1)}, bf16[512,512]{1,0:T(8,128)(2,1)}, u32[]{:S(2)}) copy-start(bf16[512,512]{1,0:T(8,128)(2,1)} %hidden.3.h_own) | copy-start | bytes 1572868
  246.2 47.3 %all-to-all-start.3 = ((bf16[32,8,4096]{2,1,0:T(8,128)(2,1)}), bf16[32,8,4096]{2,1,0:T(8,128)(2,1)S(1)}, u32[]{:S(2)}, u32[]{:S(2)}) async-start(bf16[32,8,4096]{2,1,0:T(8,128)(2,1)} %bitcast.41), calls=%async_computation.3 | async-start | bytes 4194304 | tf_op jit(solution)/shard_map/all_to_all | solution.py:531
  253.8 2.9 collective-permute-start.3
  254.0 15.5 %collective-permute-start.17 = (bf16[512,512]{1,0:T(8,128)(2,1)S(1)}, bf16[512,512]{1,0:T(8,128)(2,1)}, u32[]{:S(2)}, u32[]{:S(2)}) collective-permute-start(bf16[512,512]{1,0:T(8,128)(2,1)S(1)} %copy-done.3), channel_id=1, source_target_pairs={{0,3},{1,2},{2,1},{3,0},{4,7},{5,6},{6,5},{7,4},{8,11},{9,10},{10,... | collective-permute-start | bytes 1572872 | tf_op jit(solution)/shard_map/ppermute | solution.py:519
  256.8 29.1 %collective-permute-start.16 = (bf16[512,512]{1,0:T(8,128)(2,1)S(1)}, bf16[512,512]{1,0:T(8,128)(2,1)S(1)}, u32[]{:S(2)}, u32[]{:S(2)}) collective-permute-start(bf16[512,512]{1,0:T(8,128)(2,1)S(1)} %copy-done.3), channel_id=1, source_target_pairs={{0,1},{1,0},{2,3},{3,2},{4,5},{5,4},{6,7},{7,6},{8,9},{9,8},{10,11... | collective-permute-start | bytes 1572872 | tf_op jit(solution)/shard_map/ppermute | solution.py:515
  269.6 16.4 %collective-permute-start.18 = (bf16[512,512]{1,0:T(8,128)(2,1)}, bf16[512,512]{1,0:T(8,128)(2,1)}, u32[]{:S(2)}, u32[]{:S(2)}) collective-permute-start(bf16[512,512]{1,0:T(8,128)(2,1)} %collective-permute-done.17.h_far), channel_id=1, source_target_pairs={{0,1},{1,0},{2,3},{3,2},{4,5},{5,4},{6,7},{7,6},{8,9},{9,8},{10,11... | collective-permute-start | bytes 1572872 | tf_op jit(solution)/shard_map/ppermute | solution.py:515
  270.1 0.7 copy-start.14
  270.9 12.6 %collective-permute-start.4 = (f32[2,136,128]{2,1,0:T(8,128)}, f32[2,136,128]{2,1,0:T(8,128)}, u32[]{:S(2)}, u32[]{:S(2)}) collective-permute-start(f32[2,136,128]{2,1,0:T(8,128)} %pad_maximum_fusion.1), channel_id=1, source_target_pairs={{0,24},{8,0},{16,8},{24,16},{1,25},{9,1},{17,9},{25,17},{2,26},{10... | collective-permute-start | bytes 417800 | tf_op jit(solution)/shard_map/ppermute | solution.py:326
  271.1 14.8 %collective-permute-start.5 = (f32[2,136,128]{2,1,0:T(8,128)}, f32[2,136,128]{2,1,0:T(8,128)}, u32[]{:S(2)}, u32[]{:S(2)}) collective-permute-start(f32[2,136,128]{2,1,0:T(8,128)} %pad_maximum_fusion.1), channel_id=1, source_target_pairs={{0,16},{8,24},{16,0},{24,8},{1,17},{9,25},{17,1},{25,9},{2,18},{10... | collective-permute-start | bytes 417800 | tf_op jit(solution)/shard_map/ppermute | solution.py:326
  273.8 12.1 %collective-permute-start.6 = (f32[2,136,128]{2,1,0:T(8,128)}, f32[2,136,128]{2,1,0:T(8,128)}, u32[]{:S(2)}, u32[]{:S(2)}) collective-permute-start(f32[2,136,128]{2,1,0:T(8,128)} %pad_maximum_fusion.1), channel_id=1, source_target_pairs={{0,8},{8,16},{16,24},{24,0},{1,9},{9,17},{17,25},{25,1},{2,10},{10... | collective-permute-start | bytes 417800 | tf_op jit(solution)/shard_map/ppermute | solution.py:326
  285.9 0.8 copy-start.8
  293.5 1.4 copy-start
  293.5 9.1 %copy-start.15 = (f32[2,1,128]{2,1,0:T(1,128)S(1)}, f32[2,1,128]{2,1,0:T(1,128)}, u32[]{:S(2)}) copy-start(f32[2,1,128]{2,1,0:T(1,128)} %copy-done.14) | copy-start | bytes 3076
  293.5 9.1 %copy-start.16 = (f32[2,1,128]{2,1,0:T(1,128)S(1)}, f32[2,1,128]{2,1,0:T(1,128)}, u32[]{:S(2)}) copy-start(f32[2,1,128]{2,1,0:T(1,128)} %get-tuple-element.52) | copy-start | bytes 3076
  293.5 19.0 %copy-start.13 = (bf16[2,32,128]{2,1,0:T(8,128)(2,1)S(1)}, bf16[2,32,128]{2,1,0:T(8,128)(2,1)}, u32[]{:S(2)}) copy-start(bf16[2,32,128]{2,1,0:T(8,128)(2,1)} %get-tuple-element.47) | copy-start | bytes 49156
  294.9 43.7 %all-to-all-start.4 = ((bf16[32,8,4096]{2,1,0:T(8,128)(2,1)}), bf16[32,8,4096]{2,1,0:T(8,128)(2,1)}, u32[]{:S(2)}, u32[]{:S(2)}) async-start(bf16[32,8,4096]{2,1,0:T(8,128)(2,1)} %bitcast.40), calls=%async_computation.4 | async-start | bytes 4194304 | tf_op jit(solution)/shard_map/all_to_all | solution.py:531
  303.8 27.1 %collective-permute-start.13 = (f32[2,136,128]{2,1,0:T(8,128)S(1)}, f32[2,136,128]{2,1,0:T(8,128)S(1)}, u32[]{:S(2)}, u32[]{:S(2)}) collective-permute-start(f32[2,136,128]{2,1,0:T(8,128)S(1)} %pad_maximum_fusion.2), channel_id=1, source_target_pairs={{0,96},{1,97},{2,98},{3,99},{4,100},{5,101},{6,102},{7,103},{8,104... | collective-permute-start | bytes 417800 | tf_op jit(solution)/shard_map/ppermute | solution.py:344
  308.5 22.4 %collective-permute-start.14 = (f32[2,136,128]{2,1,0:T(8,128)S(1)}, f32[2,136,128]{2,1,0:T(8,128)S(1)}, u32[]{:S(2)}, u32[]{:S(2)}) collective-permute-start(f32[2,136,128]{2,1,0:T(8,128)S(1)} %pad_maximum_fusion.2), channel_id=1, source_target_pairs={{0,64},{32,96},{1,65},{33,97},{2,66},{34,98},{3,67},{35,99},{4,68}... | collective-permute-start | bytes 417800 | tf_op jit(solution)/shard_map/ppermute | solution.py:344
  309.8 21.3 %collective-permute-start.15 = (f32[2,136,128]{2,1,0:T(8,128)S(1)}, f32[2,136,128]{2,1,0:T(8,128)S(1)}, u32[]{:S(2)}, u32[]{:S(2)}) collective-permute-start(f32[2,136,128]{2,1,0:T(8,128)S(1)} %pad_maximum_fusion.2), channel_id=1, source_target_pairs={{0,32},{32,64},{64,96},{1,33},{33,65},{65,97},{2,34},{34,66},{66,9... | collective-permute-start | bytes 417800 | tf_op jit(solution)/shard_map/ppermute | solution.py:344
  312.6 5.0 %collective-permute-start.20 = (bf16[2,32,128]{2,1,0:T(8,128)(2,1)S(1)}, bf16[2,32,128]{2,1,0:T(8,128)(2,1)S(1)}, u32[]{:S(2)}, u32[]{:S(2)}) collective-permute-start(bf16[2,32,128]{2,1,0:T(8,128)(2,1)S(1)} %copy-done.13), channel_id=1, source_target_pairs={{0,3},{1,2},{2,1},{3,0},{4,7},{5,6},{6,5},{7,4},{8,11},{9,10},{10,... | collective-permute-start | bytes 49160 | tf_op jit(solution)/shard_map/ppermute | solution.py:519
  332.2 1.4 collective-permute-start.19
where the time goes:
time: 347 us; the launch traced here: 344 us
  waiting for transfers between devices  186 us (54%)
  Pallas kernels  74.5 us (21%)
  starting transfers between devices  69.5 us (20%)
  other arithmetic  7.92 us (2%)
  local copies, waits for them, and re-layouts  5.32 us (2%)
    ppermute x6, waiting for transfers between devices, to_far(): return lax.ppermute(a, 'tp', FAR)  94 us
    ppermute x7, waiting for transfers between devices, to_near(): return lax.ppermute(a, 'tp', NEAR)  52.4 us
    all_to_all x5, starting transfers between devices, swap(): lax.all_to_all(a.reshape(experts, rows // experts, cols), EP, split_axis=...  37.6 us
    all_to_all x5, waiting for transfers between devices, swap(): lax.all_to_all(a.reshape(experts, rows // experts, cols), EP, split_axis=...  19.2 us
    pallas_call x2, Pallas kernels, hidden_units(): pl.pallas_call(hidden_kernel, grid=(width // kb,), in_specs=[pl.BlockSpec...  17.7 us
    pallas_call x1, Pallas kernels, mixer(): pl.pallas_call(mixer_kernel, grid_spec=pltpu.PrefetchScalarGridSpec(num_s...  17.5 us
    ppermute x6, starting transfers between devices, to_far(): return lax.ppermute(a, 'tp', FAR)  14.3 us
    pallas_call x2, Pallas kernels, down_rows(): pl.pallas_call(down_kernel, grid_spec=pltpu.PrefetchScalarGridSpec(num_sc...  13.6 us
  transfers between devices with their start and end apart: 26, of which 16 were waited for; matrix products, arithmetic and copies ran while one was open for 2% of the time, Pallas kernels for 16%

commit v1 on v0

--- a/solution.py
+++ b/solution.py
@@ -409,7 +409,40 @@
     )(own, near, *weights)
 
 
-def down_kernel(src, h_own, h_near, h_far, h_opp, down_ref, out_ref):
+def down_kernel(src, this, twin, down_ref, out_ref, *, first):
+    k = pl.program_id(0)
+    n = down_ref.shape[0] // 4
+    rows = out_ref.shape[0]
+    unit = lambda s: down_ref[pl.ds(pl.multiple_of(s * n, n), n), :]
+    for step, (mine, other) in enumerate(((this, twin), (twin, this))):
+
+        @pl.when(k == step)
+        def _():
+            s, t = src[first + step], src[first + 1 - step]
+            total = mm(mine[:rows, :n], unit(s)) + mm(mine[:rows, n:], unit(3 - s))
+            total += mm(other[rows:, :n], unit(t)) + mm(other[rows:, n:], unit(3 - t))
+            out_ref[...] = total.astype(BF16)
+
+
+def down_rows(src, this, twin, first, down):
+    both, width = this.shape
+    cols = down.shape[1]
+    whole = lambda k, s: (0, 0)
+    return pl.pallas_call(
+        functools.partial(down_kernel, first=first),
+        grid_spec=pltpu.PrefetchScalarGridSpec(
+            num_scalar_prefetch=1,
+            grid=(2,),
+            in_specs=[pl.BlockSpec((both, width), whole)] * 2 + [pl.BlockSpec(down.shape, whole)],
+            out_specs=pl.BlockSpec((both // 2, cols), lambda k, s: (0, k)),
+        ),
+        out_shape=jax.ShapeDtypeStruct((both // 2, 2 * cols), BF16),
+        compiler_params=params(),
+        name="down",
+    )(src, this, twin, down)
+
+
+def down4_kernel(src, h_own, h_near, h_far, h_opp, down_ref, out_ref):
     k = pl.program_id(0)
     n = down_ref.shape[0] // 4
     rows = out_ref.shape[0]
@@ -426,21 +459,21 @@
             out_ref[...] = total.astype(BF16)
 
 
-def down_rows(src, parts, down):
+def down_rows4(src, parts, down):
     both, width = parts[0].shape
     cols = down.shape[1]
     whole = lambda k, s: (0, 0)
     return pl.pallas_call(
-        down_kernel,
+        down4_kernel,
         grid_spec=pltpu.PrefetchScalarGridSpec(
             num_scalar_prefetch=1,
             grid=(4,),
             in_specs=[pl.BlockSpec((both, width), whole)] * 4 + [pl.BlockSpec(down.shape, whole)],
-            out_specs=pl.BlockSpec((both // 2, cols), lambda k, s: (0, s[k])),
+            out_specs=pl.BlockSpec((both // 2, cols), lambda k, s: (0, k)),
         ),
         out_shape=jax.ShapeDtypeStruct((both // 2, 4 * cols), BF16),
         compiler_params=params(),
-        name="down",
+        name="down4",
     )(src, *parts, down)
 
 
@@ -477,26 +510,32 @@
     )(src, routes, logits)
 
 
-def combine_kernel(src, low_ref, high_ref, place_ref, out_ref):
-    slots = low_ref.shape[0]
-    total = mm(place_ref[0, :, :slots], low_ref[...]) + mm(place_ref[0, :, slots:], high_ref[...])
+def combine_kernel(src, first_ref, second_ref, high_ref, place_ref, out_ref):
+    k = pl.program_id(0)
+    slots = high_ref.shape[0]
     toks = out_ref.shape[0]
-    out_ref[...] = (total[:toks] + total[toks:]).astype(BF16)
-
-
-def combined(src, low, high, place):
-    slots = low.shape[0]
-    cols = low.shape[1] // 4
+    for pair, low_ref in enumerate((first_ref, second_ref)):
+
+        @pl.when(k // 2 == pair)
+        def _():
+            total = mm(place_ref[0, :, :slots], low_ref[...])
+            total += mm(place_ref[0, :, slots:], high_ref[...])
+            out_ref[...] = (total[:toks] + total[toks:]).astype(BF16)
+
+
+def combined(src, first, second, high, place):
+    slots = high.shape[0]
+    cols = high.shape[1] // 4
     toks = place.shape[1] // 2
-    res = pl.BlockSpec((slots, cols), lambda k, s: (0, s[k]))
     return pl.pallas_call(
         combine_kernel,
         grid_spec=pltpu.PrefetchScalarGridSpec(
             num_scalar_prefetch=1,
             grid=(4,),
             in_specs=[
-                res,
-                res,
+                pl.BlockSpec((slots, cols), lambda k, s: (0, jnp.minimum(k, 1))),
+                pl.BlockSpec((slots, cols), lambda k, s: (0, jnp.maximum(k - 2, 0))),
+                pl.BlockSpec((slots, cols), lambda k, s: (0, k)),
                 pl.BlockSpec((1,) + place.shape[1:], lambda k, s: (k, 0, 0)),
             ],
             out_specs=pl.BlockSpec((toks, cols), lambda k, s: (s[k], 0)),
@@ -504,7 +543,7 @@
         out_shape=jax.ShapeDtypeStruct((4 * toks, cols), BF16),
         compiler_params=params(),
         name="combine",
-    )(src, low, high, place)
+    )(src, first, second, high, place)
 
 
 NEAR = [(i, i ^ 1) for i in range(4)]
@@ -580,21 +619,24 @@
     weights = (expert_gate[0], expert_up[0], gate_far, up_far)
     h_low = hidden_units(own_rows, low_rows, 0, weights)
     h_low = shared(h_low)
+    came, _ = lax.optimization_barrier((came, h_low[0]))
+    before, planes = along_planes(chip, came)
+    down_first = down_rows(src, h_low[0], h_low[1], 0, expert_down[0])
+    back_first = swap(down_first)
     high_rows, far = lax.optimization_barrier((high_rows, h_low[2]))
     h_high = hidden_units(own_rows, high_rows, 1, weights)
     h_high = shared(h_high)
-    opp, high_own = lax.optimization_barrier((h_low[3], h_high[0]))
-    down_low = down_rows(src, h_low[:2] + (far, opp), expert_down[0])
-    back_low = swap(down_low)
-    came, _ = lax.optimization_barrier((came, down_low))
-    before, planes = along_planes(chip, came)
-    down_high = down_rows(src, (high_own,) + h_high[1:], expert_down[0])
+    down_second = down_rows(src, far, h_low[3], 2, expert_down[0])
+    down_second, back_first = lax.optimization_barrier((down_second, back_first))
+    back_second = swap(down_second)
+    down_high = down_rows4(src, h_high, expert_down[0])
+    down_high, back_second = lax.optimization_barrier((down_high, back_second))
     back_high = swap(down_high)
     planes, _ = lax.optimization_barrier((planes, down_high))
 
     state = arriving_state(first_core, before, planes)
     mixer_out = readout(inside, query, state, norm_out.reshape(1, -1))
-    expert_out = combined(src, back_low, back_high, place)
+    expert_out = combined(src, back_first, back_second, back_high, place)
     return (mixer_out, expert_out)
 
 

time: 347 us -> 343 us (0.988)
  waiting for transfers between devices: 186 us -> 169 us
  starting transfers between devices: 69.5 us -> 78.1 us
    ppermute x6, waiting for transfers between devices: 94 us -> 18.4 us  [to_far(): return lax.ppermute(a, 'tp', FAR)]
    ppermute x7, waiting for transfers between devices: 52.4 us -> 89 us  [to_near(): return lax.ppermute(a, 'tp', NEAR)]
    all_to_all x5 -> x6, waiting for transfers between devices: 19.2 us -> 39.6 us  [swap(): lax.all_to_all(a.reshape(experts, rows // experts, cols), EP, split_axis=...]
    all_to_all x5 -> x6, starting transfers between devices: 37.6 us -> 44 us  [swap(): lax.all_to_all(a.reshape(experts, rows // experts, cols), EP, split_axis=...]
    pallas_call x2 -> x3, Pallas kernels: 13.6 us -> 16.5 us  [the longest x2 9.75 us: down_rows(): pl.pallas_call(functools.partial(down_kernel, first=first), grid_spec=plt...]
  transfers between devices with their start and end apart: 26 -> 27, of which waited for: 16 -> 15; matrix products, arithmetic and copies ran while one was open for 2% -> 2% of each run, Pallas kernels for 16% -> 19%
where the time goes in v1:
time: 343 us; the launch traced here: 340 us
  waiting for transfers between devices  169 us (49%)
  starting transfers between devices  78.1 us (23%)
  Pallas kernels  77.5 us (23%)
  other arithmetic  8.85 us (3%)
  local copies, waits for them, and re-layouts  6.55 us (2%)
    ppermute x7, waiting for transfers between devices, to_near(): return lax.ppermute(a, 'tp', NEAR)  89 us
    all_to_all x6, starting transfers between devices, swap(): lax.all_to_all(a.reshape(experts, rows // experts, cols), EP, split_axis=...  44 us
    all_to_all x6, waiting for transfers between devices, swap(): lax.all_to_all(a.reshape(experts, rows // experts, cols), EP, split_axis=...  39.6 us
    ppermute x6, waiting for transfers between devices, to_far(): return lax.ppermute(a, 'tp', FAR)  18.4 us
    pallas_call x2, Pallas kernels, hidden_units(): pl.pallas_call(hidden_kernel, grid=(width // kb,), in_specs=[pl.BlockSpec...  17.7 us
    pallas_call x1, Pallas kernels, mixer(): pl.pallas_call(mixer_kernel, grid_spec=pltpu.PrefetchScalarGridSpec(num_s...  17.5 us
    ppermute x6, starting transfers between devices, to_far(): return lax.ppermute(a, 'tp', FAR)  14.2 us
    ppermute x3, waiting for transfers between devices, along_rows(): lax.ppermute(sent, 'ep_1', [(i, (i + d) % count) for i in range(count)])  11.3 us
  transfers between devices with their start and end apart: 27, of which 15 were waited for; matrix products, arithmetic and copies ran while one was open for 2% of the time, Pallas kernels for 19%

profile of v1, /device:TPU:8, one launch (start us, length us, event | category | flops | bytes accessed | tf_op | source)
XLA Modules:
  0.0 340.4 jit_solution(15879769935117779643)
XLA Ops:
  1.3 5.8 %front.1 = (bf16[128,4096]{1,0:T(8,128)(2,1)}, bf16[256,8192]{1,0:T(8,128)(2,1)}) custom-call(s32[4]{0:T(128)} %pad_add_fusion.src, bf16[128,4096]{1,0:T(8,128)(2,1)} %x_ref.1, f32[1,4096]{1,0:T(1,128)} %bitcast.57, s32[4,2,128]{2,1,0:T(2,128)} %bitcast.54), custom_call_target="tpu_custom_call" | custom-call | tf_op jit(solution)/shard_map/front/pallas_call | solution.py:100
  7.0 8.7 %all-to-all-start = ((bf16[32,8,8192]{2,1,0:T(8,128)(2,1)}), bf16[32,8,8192]{2,1,0:T(8,128)(2,1)}, u32[]{:S(2)}, u32[]{:S(2)}) async-start(bf16[32,8,8192]{2,1,0:T(8,128)(2,1)} %bitcast.50), calls=%async_computation | async-start | bytes 8388608 | tf_op jit(solution)/shard_map/all_to_all | solution.py:570
  15.8 1.6 collective-permute-start.7
  17.3 23.7 %collective-permute-done.7.rows_ref = bf16[128,4096]{1,0:T(8,128)(2,1)S(1)} collective-permute-done((bf16[128,4096]{1,0:T(8,128)(2,1)S(1)}, bf16[128,4096]{1,0:T(8,128)(2,1)S(1)}, u32[]{:S(2)}, u32[]{:S(2)}) %collective-permute-start.7) | collective-permute-done | bytes 1048608 | tf_op jit(solution)/shard_map/ppermute | solution.py:554
  42.0 6.0 %refill.1 = (bf16[2,32,128]{2,1,0:T(8,128)(2,1)}, bf16[256,4096]{1,0:T(8,128)(2,1)}, bf16[256,4096]{1,0:T(8,128)(2,1)}) custom-call(s32[4]{0:T(128)} %pad_add_fusion.src, bf16[128,4096]{1,0:T(8,128)(2,1)} %get-tuple-element.30.own_ref, bf16[128,4096]{1,0:T(8,128)(2,1)} %copy-done.8, bf16[32,4096]{1,0:T(8,128)(2,1)} %bitcast.53, s32[4,2,128]{2,1,0:T(2,128)} %bitcast.55), custom_call_target="tpu_custom_call" | custom-call | tf_op jit(solution)/shard_map/refill/pallas_call | solution.py:129
  48.0 19.1 %all-to-all-done = bf16[32,8,8192]{2,1,0:T(8,128)(2,1)} async-done(((bf16[32,8,8192]{2,1,0:T(8,128)(2,1)}), bf16[32,8,8192]{2,1,0:T(8,128)(2,1)}, u32[]{:S(2)}, u32[]{:S(2)}) %all-to-all-start) | async-done | bytes 4194336 | tf_op jit(solution)/shard_map/all_to_all | solution.py:570
  67.2 6.6 %all-to-all-start.1 = ((bf16[32,8,4096]{2,1,0:T(8,128)(2,1)}), bf16[32,8,4096]{2,1,0:T(8,128)(2,1)S(1)}, u32[]{:S(2)}, u32[]{:S(2)}) async-start(bf16[32,8,4096]{2,1,0:T(8,128)(2,1)} %bitcast.52), calls=%async_computation.1 | async-start | bytes 4194304 | tf_op jit(solution)/shard_map/all_to_all | solution.py:570
  74.2 1.3 fusion.2.a0
  75.5 2.8 collective-permute-start.1
  78.7 2.8 collective-permute-start.9
  81.5 20.4 %all-to-all-done.1 = bf16[32,8,4096]{2,1,0:T(8,128)(2,1)S(1)} async-done(((bf16[32,8,4096]{2,1,0:T(8,128)(2,1)}), bf16[32,8,4096]{2,1,0:T(8,128)(2,1)S(1)}, u32[]{:S(2)}, u32[]{:S(2)}) %all-to-all-start.1) | async-done | bytes 2097184 | tf_op jit(solution)/shard_map/all_to_all | solution.py:570
  101.9 1.4 copy-done.2
  103.3 6.1 %all-to-all-start.2 = ((bf16[32,8,4096]{2,1,0:T(8,128)(2,1)}), bf16[32,8,4096]{2,1,0:T(8,128)(2,1)S(1)}, u32[]{:S(2)}, u32[]{:S(2)}) async-start(bf16[32,8,4096]{2,1,0:T(8,128)(2,1)} %bitcast.51), calls=%async_computation.2 | async-start | bytes 4194304 | tf_op jit(solution)/shard_map/all_to_all | solution.py:570
  109.4 1.6 collective-permute-start
  111.5 24.2 %collective-permute-done.a1 = bf16[128,4096]{1,0:T(8,128)(2,1)S(1)} collective-permute-done((bf16[128,4096]{1,0:T(8,128)(2,1)}, bf16[128,4096]{1,0:T(8,128)(2,1)S(1)}, u32[]{:S(2)}, u32[]{:S(2)}) %collective-permute-start) | collective-permute-done | bytes 1048608 | tf_op jit(solution)/shard_map/ppermute | solution.py:554
  135.7 21.6 %collective-permute-done.2.a3 = bf16[128,4096]{1,0:T(8,128)(2,1)S(1)} collective-permute-done((bf16[128,4096]{1,0:T(8,128)(2,1)}, bf16[128,4096]{1,0:T(8,128)(2,1)S(1)}, u32[]{:S(2)}, u32[]{:S(2)}) %collective-permute-start.2) | collective-permute-done | bytes 1048608 | tf_op jit(solution)/shard_map/ppermute | solution.py:554
  158.3 17.5 %mixer.1 = (f32[512,512]{1,0:T(8,128)}, f32[512,512]{1,0:T(8,128)}, f32[4,136,128]{2,1,0:T(8,128)}) custom-call(s32[4]{0:T(128)} %pad_add_fusion.src, bf16[128,4096]{1,0:T(8,128)(2,1)} %fusion.2.a0, bf16[128,4096]{1,0:T(8,128)(2,1)} %copy-done.9, bf16[128,4096]{1,0:T(8,128)(2,1)} %collective-permute-done.1.a2, bf16[128,4096]{1,0:T(8,128)(2,1)} %copy-done.10, ...), custom_call_target="tpu_custom_call" | custom-call | tf_op jit(solution)/shard_map/mixer/pallas_call | solution.py:237
  175.9 16.2 %collective-permute-done.9.uf_ref = bf16[4096,256]{1,0:T(8,128)(2,1)} collective-permute-done((bf16[4096,256]{1,0:T(8,128)(2,1)}, bf16[4096,256]{1,0:T(8,128)(2,1)}, u32[]{:S(2)}, u32[]{:S(2)}) %collective-permute-start.9) | collective-permute-done | bytes 2097184 | tf_op jit(solution)/shard_map/ppermute | solution.py:558
  192.1 8.8 %hidden.2.this = bf16[512,512]{1,0:T(8,128)(2,1)} custom-call(bf16[256,8192]{1,0:T(8,128)(2,1)} %bitcast.13.own_ref, bf16[256,4096]{1,0:T(8,128)(2,1)} %bitcast.45, bf16[4096,256]{1,0:T(8,128)(2,1)} %bitcast.16.go_ref, bf16[4096,256]{1,0:T(8,128)(2,1)} %bitcast.17.uo_ref, bf16[4096,256]{1,0:T(8,128)(2,1)} %collective-permute-done.8.gf_ref, ...), custom_call_target="tpu_custom_call" | custom-call | tf_op jit(solution)/shard_map/hidden/pallas_call | solution.py:393
  201.2 2.6 collective-permute-start.13
  203.7 10.5 %collective-permute-done.18.twin = bf16[512,512]{1,0:T(8,128)(2,1)S(1)} collective-permute-done((bf16[512,512]{1,0:T(8,128)(2,1)}, bf16[512,512]{1,0:T(8,128)(2,1)S(1)}, u32[]{:S(2)}, u32[]{:S(2)}) %collective-permute-start.18) | collective-permute-done | bytes 524320 | tf_op jit(solution)/shard_map/ppermute | solution.py:554
  215.0 4.9 %down.3 = bf16[256,2048]{1,0:T(8,128)(2,1)} custom-call(s32[4]{0:T(128)} %pad_add_fusion.src, bf16[512,512]{1,0:T(8,128)(2,1)} %hidden.2.this, bf16[512,512]{1,0:T(8,128)(2,1)} %copy-done.13, bf16[1024,1024]{1,0:T(8,128)(2,1)} %bitcast.39), custom_call_target="tpu_custom_call" | custom-call | tf_op jit(solution)/shard_map/down/pallas_call | solution.py:431
  219.9 7.6 %all-to-all-start.3 = ((bf16[32,8,2048]{2,1,0:T(8,128)(2,1)}), bf16[32,8,2048]{2,1,0:T(8,128)(2,1)S(1)}, u32[]{:S(2)}, u32[]{:S(2)}) async-start(bf16[32,8,2048]{2,1,0:T(8,128)(2,1)} %bitcast.49), calls=%async_computation.3 | async-start | bytes 2097152 | tf_op jit(solution)/shard_map/all_to_all | solution.py:570
  227.9 8.9 %hidden.3.h_own = bf16[512,512]{1,0:T(8,128)(2,1)} custom-call(bf16[256,8192]{1,0:T(8,128)(2,1)} %bitcast.13.own_ref, bf16[256,4096]{1,0:T(8,128)(2,1)} %bitcast.44, bf16[4096,256]{1,0:T(8,128)(2,1)} %bitcast.16.go_ref, bf16[4096,256]{1,0:T(8,128)(2,1)} %bitcast.17.uo_ref, bf16[4096,256]{1,0:T(8,128)(2,1)} %collective-permute-done.8.gf_ref, ...), custom_call_target="tpu_custom_call" | custom-call | tf_op jit(solution)/shard_map/hidden/pallas_call | solution.py:393
  236.7 2.8 collective-permute-start.15
  239.5 2.4 collective-permute-done.17.twin
  241.8 4.9 %down.2 = bf16[256,2048]{1,0:T(8,128)(2,1)} custom-call(s32[4]{0:T(128)} %pad_add_fusion.src, bf16[512,512]{1,0:T(8,128)(2,1)} %collective-permute-done.13.this, bf16[512,512]{1,0:T(8,128)(2,1)} %collective-permute-done.17.twin, bf16[1024,1024]{1,0:T(8,128)(2,1)} %bitcast.40), custom_call_target="tpu_custom_call" | custom-call | tf_op jit(solution)/shard_map/down/pallas_call | solution.py:431
  246.7 7.5 %all-to-all-start.4 = ((bf16[32,8,2048]{2,1,0:T(8,128)(2,1)}), bf16[32,8,2048]{2,1,0:T(8,128)(2,1)S(1)}, u32[]{:S(2)}, u32[]{:S(2)}) async-start(bf16[32,8,2048]{2,1,0:T(8,128)(2,1)} %bitcast.48), calls=%async_computation.4 | async-start | bytes 2097152 | tf_op jit(solution)/shard_map/all_to_all | solution.py:570
  255.7 1.7 collective-permute-start.16
  258.9 2.7 collective-permute-start.5
  261.6 1.8 collective-permute-start.6
  263.4 7.7 %collective-permute-done.4 = f32[2,136,128]{2,1,0:T(8,128)} collective-permute-done((f32[2,136,128]{2,1,0:T(8,128)}, f32[2,136,128]{2,1,0:T(8,128)}, u32[]{:S(2)}, u32[]{:S(2)}) %collective-permute-start.4) | collective-permute-done | bytes 139296 | tf_op jit(solution)/shard_map/ppermute | solution.py:326
  271.1 3.6 %collective-permute-done.5 = f32[2,136,128]{2,1,0:T(8,128)} collective-permute-done((f32[2,136,128]{2,1,0:T(8,128)}, f32[2,136,128]{2,1,0:T(8,128)}, u32[]{:S(2)}, u32[]{:S(2)}) %collective-permute-start.5) | collective-permute-done | bytes 139296 | tf_op jit(solution)/shard_map/ppermute | solution.py:326
  274.7 6.7 %collective-permute-done.16.h_opp = bf16[512,512]{1,0:T(8,128)(2,1)} collective-permute-done((bf16[512,512]{1,0:T(8,128)(2,1)}, bf16[512,512]{1,0:T(8,128)(2,1)}, u32[]{:S(2)}, u32[]{:S(2)}) %collective-permute-start.16) | collective-permute-done | bytes 524320 | tf_op jit(solution)/shard_map/ppermute | solution.py:554
  281.4 6.8 %down4.1 = bf16[256,4096]{1,0:T(8,128)(2,1)} custom-call(s32[4]{0:T(128)} %pad_add_fusion.src, bf16[512,512]{1,0:T(8,128)(2,1)} %hidden.3.h_own, bf16[512,512]{1,0:T(8,128)(2,1)} %copy-done.12, bf16[512,512]{1,0:T(8,128)(2,1)} %collective-permute-done.15.h_far, bf16[512,512]{1,0:T(8,128)(2,1)} %collective-permute-done.16.h_opp, bf16[1024,1024]{1,0:T(8,128)(2,1)} %bitcast.41), custom_call_target="tpu_custom_call" | custom-call | tf_op jit(solution)/shard_map/down4/pallas_call | solution.py:466
  289.2 7.4 %all-to-all-start.5 = ((bf16[32,8,4096]{2,1,0:T(8,128)(2,1)}), bf16[32,8,4096]{2,1,0:T(8,128)(2,1)S(1)}, u32[]{:S(2)}, u32[]{:S(2)}) async-start(bf16[32,8,4096]{2,1,0:T(8,128)(2,1)} %bitcast.42), calls=%async_computation.5 | async-start | bytes 4194304 | tf_op jit(solution)/shard_map/all_to_all | solution.py:570
  297.4 1.1 add_add_fusion
  298.5 4.6 %collective-permute-start.10 = (f32[2,136,128]{2,1,0:T(8,128)S(1)}, f32[2,136,128]{2,1,0:T(8,128)S(1)}, u32[]{:S(2)}, u32[]{:S(2)}) collective-permute-start(f32[2,136,128]{2,1,0:T(8,128)S(1)} %pad_maximum_fusion.2), channel_id=1, source_target_pairs={{0,96},{1,97},{2,98},{3,99},{4,100},{5,101},{6,102},{7,103},{8,104... | collective-permute-start | bytes 417800 | tf_op jit(solution)/shard_map/ppermute | solution.py:344
  303.2 1.3 collective-permute-start.11
  304.5 2.8 collective-permute-start.12
  307.3 2.8 collective-permute-start.20
  310.1 2.2 collective-permute-done.20
  312.9 4.0 %places.1.place_ref = bf16[4,256,512]{2,1,0:T(8,128)(2,1)} custom-call(s32[4]{0:T(128)} %pad_add_fusion.src, s32[4,2,128]{2,1,0:T(2,128)} %bitcast.56, bf16[4,32,128]{2,1,0:T(8,128)(2,1)} %pad_maximum_fusion.3.logits_ref), custom_call_target="tpu_custom_call" | custom-call | tf_op jit(solution)/shard_map/places/pallas_call | solution.py:496
  316.9 8.7 %collective-permute-done.10 = f32[2,136,128]{2,1,0:T(8,128)S(1)} collective-permute-done((f32[2,136,128]{2,1,0:T(8,128)S(1)}, f32[2,136,128]{2,1,0:T(8,128)S(1)}, u32[]{:S(2)}, u32[]{:S(2)}) %collective-permute-start.10) | collective-permute-done | bytes 139296 | tf_op jit(solution)/shard_map/ppermute | solution.py:344
  327.1 1.3 collective-permute-done.19
  329.1 4.2 %readout.1 = bf16[512,512]{1,0:T(8,128)(2,1)} custom-call(f32[512,512]{1,0:T(8,128)} %get-tuple-element.27.inside_ref, f32[512,512]{1,0:T(8,128)} %get-tuple-element.28.query_ref, f32[4,128,128]{2,1,0:T(8,128)} %fusion.3.state_ref, f32[1,512]{1,0:T(1,128)} %bitcast.73), custom_call_target="tpu_custom_call" | custom-call | tf_op jit(solution)/shard_map/readout/pallas_call | solution.py:275
  333.3 1.3 copy-done
  334.7 5.7 %combine.1 = bf16[512,1024]{1,0:T(8,128)(2,1)} custom-call(s32[4]{0:T(128)} %pad_add_fusion.src, bf16[256,2048]{1,0:T(8,128)(2,1)} %bitcast.46, bf16[256,2048]{1,0:T(8,128)(2,1)} %bitcast.47, bf16[256,4096]{1,0:T(8,128)(2,1)} %bitcast.43, bf16[4,256,512]{2,1,0:T(8,128)(2,1)} %places.1.place_ref), custom_call_target="tpu_custom_call" | custom-call | tf_op jit(solution)/shard_map/combine/pallas_call | solution.py:530
  (76 shorter events, 12.8 us)
Async XLA Ops:
  7.0 8.7 %copy-start.7 = (bf16[128,4096]{1,0:T(8,128)(2,1)S(1)}, bf16[128,4096]{1,0:T(8,128)(2,1)}, u32[]{:S(2)}) copy-start(bf16[128,4096]{1,0:T(8,128)(2,1)} %get-tuple-element.30.own_ref) | copy-start | bytes 3145732
  7.0 60.2 %all-to-all-start = ((bf16[32,8,8192]{2,1,0:T(8,128)(2,1)}), bf16[32,8,8192]{2,1,0:T(8,128)(2,1)}, u32[]{:S(2)}, u32[]{:S(2)}) async-start(bf16[32,8,8192]{2,1,0:T(8,128)(2,1)} %bitcast.50), calls=%async_computation | async-start | bytes 8388608 | tf_op jit(solution)/shard_map/all_to_all | solution.py:570
  15.8 25.3 %collective-permute-start.7 = (bf16[128,4096]{1,0:T(8,128)(2,1)S(1)}, bf16[128,4096]{1,0:T(8,128)(2,1)S(1)}, u32[]{:S(2)}, u32[]{:S(2)}) collective-permute-start(bf16[128,4096]{1,0:T(8,128)(2,1)S(1)} %copy-done.7), channel_id=1, source_target_pairs={{0,1},{1,0},{2,3},{3,2},{4,5},{5,4},{6,7},{7,6},{8,9},{9,8},{10,11... | collective-permute-start | bytes 3145736 | tf_op jit(solution)/shard_map/ppermute | solution.py:554
  41.0 1.0 copy-start.8
  67.2 6.7 %copy-start.5 = (bf16[128,4096]{1,0:T(8,128)(2,1)S(1)}, bf16[128,4096]{1,0:T(8,128)(2,1)}, u32[]{:S(2)}) copy-start(bf16[128,4096]{1,0:T(8,128)(2,1)} %param.14) | copy-start | bytes 3145732
  67.2 7.0 %copy-start.14 = (f32[4096]{0:T(1024)S(1)}, f32[4096]{0:T(1024)}, u32[]{:S(2)}) copy-start(f32[4096]{0:T(1024)} %param.16) | copy-start | bytes 49156
  67.2 34.7 %all-to-all-start.1 = ((bf16[32,8,4096]{2,1,0:T(8,128)(2,1)}), bf16[32,8,4096]{2,1,0:T(8,128)(2,1)S(1)}, u32[]{:S(2)}, u32[]{:S(2)}) async-start(bf16[32,8,4096]{2,1,0:T(8,128)(2,1)} %bitcast.52), calls=%async_computation.1 | async-start | bytes 4194304 | tf_op jit(solution)/shard_map/all_to_all | solution.py:570
  75.5 35.5 %collective-permute-start.1 = (bf16[128,4096]{1,0:T(8,128)(2,1)}, bf16[128,4096]{1,0:T(8,128)(2,1)}, u32[]{:S(2)}, u32[]{:S(2)}) collective-permute-start(bf16[128,4096]{1,0:T(8,128)(2,1)} %fusion.2.a0), channel_id=1, source_target_pairs={{0,3},{1,2},{2,1},{3,0},{4,7},{5,6},{6,5},{7,4},{8,11},{9,10},{10,... | collective-permute-start | bytes 3145736 | tf_op jit(solution)/shard_map/ppermute | solution.py:558
  78.2 97.6 %collective-permute-start.8 = (bf16[4096,256]{1,0:T(8,128)(2,1)}, bf16[4096,256]{1,0:T(8,128)(2,1)}, u32[]{:S(2)}, u32[]{:S(2)}) collective-permute-start(bf16[4096,256]{1,0:T(8,128)(2,1)} %bitcast.16.go_ref), channel_id=1, source_target_pairs={{0,3},{1,2},{2,1},{3,0},{4,7},{5,6},{6,5},{7,4},{8,11},{9,10},{10,... | collective-permute-start | bytes 6291464 | tf_op jit(solution)/shard_map/ppermute | solution.py:558
  78.7 113.4 %collective-permute-start.9 = (bf16[4096,256]{1,0:T(8,128)(2,1)}, bf16[4096,256]{1,0:T(8,128)(2,1)}, u32[]{:S(2)}, u32[]{:S(2)}) collective-permute-start(bf16[4096,256]{1,0:T(8,128)(2,1)} %bitcast.17.uo_ref), channel_id=1, source_target_pairs={{0,3},{1,2},{2,1},{3,0},{4,7},{5,6},{6,5},{7,4},{8,11},{9,10},{10,... | collective-permute-start | bytes 6291464 | tf_op jit(solution)/shard_map/ppermute | solution.py:558
  101.9 1.4 copy-start.2
  103.3 116.6 %all-to-all-start.2 = ((bf16[32,8,4096]{2,1,0:T(8,128)(2,1)}), bf16[32,8,4096]{2,1,0:T(8,128)(2,1)S(1)}, u32[]{:S(2)}, u32[]{:S(2)}) async-start(bf16[32,8,4096]{2,1,0:T(8,128)(2,1)} %bitcast.51), calls=%async_computation.2 | async-start | bytes 4194304 | tf_op jit(solution)/shard_map/all_to_all | solution.py:570
  109.4 26.3 %collective-permute-start = (bf16[128,4096]{1,0:T(8,128)(2,1)}, bf16[128,4096]{1,0:T(8,128)(2,1)S(1)}, u32[]{:S(2)}, u32[]{:S(2)}) collective-permute-start(bf16[128,4096]{1,0:T(8,128)(2,1)} %fusion.2.a0), channel_id=1, source_target_pairs={{0,1},{1,0},{2,3},{3,2},{4,5},{5,4},{6,7},{7,6},{8,9},{9,8},{10,11... | collective-permute-start | bytes 3145736 | tf_op jit(solution)/shard_map/ppermute | solution.py:554
  111.0 46.4 %collective-permute-start.2 = (bf16[128,4096]{1,0:T(8,128)(2,1)}, bf16[128,4096]{1,0:T(8,128)(2,1)S(1)}, u32[]{:S(2)}, u32[]{:S(2)}) collective-permute-start(bf16[128,4096]{1,0:T(8,128)(2,1)} %collective-permute-done.1.a2), channel_id=1, source_target_pairs={{0,1},{1,0},{2,3},{3,2},{4,5},{5,4},{6,7},{7,6},{8,9},{9,8},{10,11... | collective-permute-start | bytes 3145736 | tf_op jit(solution)/shard_map/ppermute | solution.py:554
  135.7 21.6 %copy-start.9 = (bf16[128,4096]{1,0:T(8,128)(2,1)}, bf16[128,4096]{1,0:T(8,128)(2,1)S(1)}, u32[]{:S(2)}) copy-start(bf16[128,4096]{1,0:T(8,128)(2,1)S(1)} %collective-permute-done.a1) | copy-start | bytes 3145732
  157.3 1.0 copy-start.10
  200.9 13.3 %collective-permute-start.18 = (bf16[512,512]{1,0:T(8,128)(2,1)}, bf16[512,512]{1,0:T(8,128)(2,1)S(1)}, u32[]{:S(2)}, u32[]{:S(2)}) collective-permute-start(bf16[512,512]{1,0:T(8,128)(2,1)} %hidden.2.this), channel_id=1, source_target_pairs={{0,1},{1,0},{2,3},{3,2},{4,5},{5,4},{6,7},{7,6},{8,9},{9,8},{10,11... | collective-permute-start | bytes 1572872 | tf_op jit(solution)/shard_map/ppermute | solution.py:554
  201.2 26.3 %collective-permute-start.13 = (bf16[512,512]{1,0:T(8,128)(2,1)}, bf16[512,512]{1,0:T(8,128)(2,1)}, u32[]{:S(2)}, u32[]{:S(2)}) collective-permute-start(bf16[512,512]{1,0:T(8,128)(2,1)} %hidden.2.this), channel_id=1, source_target_pairs={{0,3},{1,2},{2,1},{3,0},{4,7},{5,6},{6,5},{7,4},{8,11},{9,10},{10,... | collective-permute-start | bytes 1572872 | tf_op jit(solution)/shard_map/ppermute | solution.py:558
  214.2 0.8 copy-start.13
  219.9 8.0 %copy-start.11 = (f32[4,136,128]{2,1,0:T(8,128)S(1)}, f32[4,136,128]{2,1,0:T(8,128)}, u32[]{:S(2)}) copy-start(f32[4,136,128]{2,1,0:T(8,128)} %get-tuple-element.29) | copy-start | bytes 835588
  219.9 8.0 %copy-start.1 = (bf16[32,8,4096]{2,1,0:T(8,128)(2,1)}, bf16[32,8,4096]{2,1,0:T(8,128)(2,1)S(1)}, u32[]{:S(2)}) copy-start(bf16[32,8,4096]{2,1,0:T(8,128)(2,1)S(1)} %all-to-all-done.2) | copy-start | bytes 6291460
  219.9 26.9 %all-to-all-start.3 = ((bf16[32,8,2048]{2,1,0:T(8,128)(2,1)}), bf16[32,8,2048]{2,1,0:T(8,128)(2,1)S(1)}, u32[]{:S(2)}, u32[]{:S(2)}) async-start(bf16[32,8,2048]{2,1,0:T(8,128)(2,1)} %bitcast.49), calls=%async_computation.3 | async-start | bytes 2097152 | tf_op jit(solution)/shard_map/all_to_all | solution.py:570
  227.5 14.3 %collective-permute-start.17 = (bf16[512,512]{1,0:T(8,128)(2,1)}, bf16[512,512]{1,0:T(8,128)(2,1)}, u32[]{:S(2)}, u32[]{:S(2)}) collective-permute-start(bf16[512,512]{1,0:T(8,128)(2,1)} %collective-permute-done.13.this), channel_id=1, source_target_pairs={{0,1},{1,0},{2,3},{3,2},{4,5},{5,4},{6,7},{7,6},{8,9},{9,8},{10,11... | collective-permute-start | bytes 1572872 | tf_op jit(solution)/shard_map/ppermute | solution.py:554
  227.9 26.4 %collective-permute-start.3 = (f32[4,136,128]{2,1,0:T(8,128)S(1)}, f32[4,136,128]{2,1,0:T(8,128)}, u32[]{:S(2)}, u32[]{:S(2)}) collective-permute-start(f32[4,136,128]{2,1,0:T(8,128)S(1)} %copy-done.11), channel_id=1, source_target_pairs={{0,4},{4,0},{1,5},{5,1},{2,6},{6,2},{3,7},{7,3},{8,12},{12,8},{9,1... | collective-permute-start | bytes 835592 | tf_op jit(solution)/shard_map/ppermute | solution.py:311
  236.7 18.9 %collective-permute-start.15 = (bf16[512,512]{1,0:T(8,128)(2,1)}, bf16[512,512]{1,0:T(8,128)(2,1)}, u32[]{:S(2)}, u32[]{:S(2)}) collective-permute-start(bf16[512,512]{1,0:T(8,128)(2,1)} %hidden.3.h_own), channel_id=1, source_target_pairs={{0,3},{1,2},{2,1},{3,0},{4,7},{5,6},{6,5},{7,4},{8,11},{9,10},{10,... | collective-permute-start | bytes 1572872 | tf_op jit(solution)/shard_map/ppermute | solution.py:558
  246.7 8.5 %copy-start.6 = (bf16[512,512]{1,0:T(8,128)(2,1)S(1)}, bf16[512,512]{1,0:T(8,128)(2,1)}, u32[]{:S(2)}) copy-start(bf16[512,512]{1,0:T(8,128)(2,1)} %hidden.3.h_own) | copy-start | bytes 1572868
  246.7 41.5 %copy-start.3 = (bf16[32,8,2048]{2,1,0:T(8,128)(2,1)}, bf16[32,8,2048]{2,1,0:T(8,128)(2,1)S(1)}, u32[]{:S(2)}) copy-start(bf16[32,8,2048]{2,1,0:T(8,128)(2,1)S(1)} %all-to-all-done.3) | copy-start | bytes 3145732
  246.7 41.5 %all-to-all-start.4 = ((bf16[32,8,2048]{2,1,0:T(8,128)(2,1)}), bf16[32,8,2048]{2,1,0:T(8,128)(2,1)S(1)}, u32[]{:S(2)}, u32[]{:S(2)}) async-start(bf16[32,8,2048]{2,1,0:T(8,128)(2,1)} %bitcast.48), calls=%async_computation.4 | async-start | bytes 2097152 | tf_op jit(solution)/shard_map/all_to_all | solution.py:570
  255.3 19.4 %collective-permute-start.14 = (bf16[512,512]{1,0:T(8,128)(2,1)S(1)}, bf16[512,512]{1,0:T(8,128)(2,1)S(1)}, u32[]{:S(2)}, u32[]{:S(2)}) collective-permute-start(bf16[512,512]{1,0:T(8,128)(2,1)S(1)} %copy-done.6), channel_id=1, source_target_pairs={{0,1},{1,0},{2,3},{3,2},{4,5},{5,4},{6,7},{7,6},{8,9},{9,8},{10,11... | collective-permute-start | bytes 1572872 | tf_op jit(solution)/shard_map/ppermute | solution.py:554
  255.7 25.8 %collective-permute-start.16 = (bf16[512,512]{1,0:T(8,128)(2,1)}, bf16[512,512]{1,0:T(8,128)(2,1)}, u32[]{:S(2)}, u32[]{:S(2)}) collective-permute-start(bf16[512,512]{1,0:T(8,128)(2,1)} %collective-permute-done.15.h_far), channel_id=1, source_target_pairs={{0,1},{1,0},{2,3},{3,2},{4,5},{5,4},{6,7},{7,6},{8,9},{9,8},{10,11... | collective-permute-start | bytes 1572872 | tf_op jit(solution)/shard_map/ppermute | solution.py:554
  258.0 0.7 copy-start.16
  258.7 12.4 %collective-permute-start.4 = (f32[2,136,128]{2,1,0:T(8,128)}, f32[2,136,128]{2,1,0:T(8,128)}, u32[]{:S(2)}, u32[]{:S(2)}) collective-permute-start(f32[2,136,128]{2,1,0:T(8,128)} %pad_maximum_fusion.1), channel_id=1, source_target_pairs={{0,24},{8,0},{16,8},{24,16},{1,25},{9,1},{17,9},{25,17},{2,26},{10... | collective-permute-start | bytes 417800 | tf_op jit(solution)/shard_map/ppermute | solution.py:326
  258.9 15.8 %collective-permute-start.5 = (f32[2,136,128]{2,1,0:T(8,128)}, f32[2,136,128]{2,1,0:T(8,128)}, u32[]{:S(2)}, u32[]{:S(2)}) collective-permute-start(f32[2,136,128]{2,1,0:T(8,128)} %pad_maximum_fusion.1), channel_id=1, source_target_pairs={{0,16},{8,24},{16,0},{24,8},{1,17},{9,25},{17,1},{25,9},{2,18},{10... | collective-permute-start | bytes 417800 | tf_op jit(solution)/shard_map/ppermute | solution.py:326
  261.6 13.1 %collective-permute-start.6 = (f32[2,136,128]{2,1,0:T(8,128)}, f32[2,136,128]{2,1,0:T(8,128)}, u32[]{:S(2)}, u32[]{:S(2)}) collective-permute-start(f32[2,136,128]{2,1,0:T(8,128)} %pad_maximum_fusion.1), channel_id=1, source_target_pairs={{0,8},{8,16},{16,24},{24,0},{1,9},{9,17},{17,25},{25,1},{2,10},{10... | collective-permute-start | bytes 417800 | tf_op jit(solution)/shard_map/ppermute | solution.py:326
  274.7 6.7 %copy-start.12 = (bf16[512,512]{1,0:T(8,128)(2,1)}, bf16[512,512]{1,0:T(8,128)(2,1)S(1)}, u32[]{:S(2)}) copy-start(bf16[512,512]{1,0:T(8,128)(2,1)S(1)} %collective-permute-done.14.h_near) | copy-start | bytes 1572868
  288.2 1.0 copy-start.4
  288.2 9.1 %copy-start.17 = (f32[2,1,128]{2,1,0:T(1,128)S(1)}, f32[2,1,128]{2,1,0:T(1,128)}, u32[]{:S(2)}) copy-start(f32[2,1,128]{2,1,0:T(1,128)} %copy-done.16) | copy-start | bytes 3076
  288.2 9.1 %copy-start.18 = (f32[2,1,128]{2,1,0:T(1,128)S(1)}, f32[2,1,128]{2,1,0:T(1,128)}, u32[]{:S(2)}) copy-start(f32[2,1,128]{2,1,0:T(1,128)} %get-tuple-element.56) | copy-start | bytes 3076
  288.2 19.0 %copy-start.15 = (bf16[2,32,128]{2,1,0:T(8,128)(2,1)S(1)}, bf16[2,32,128]{2,1,0:T(8,128)(2,1)}, u32[]{:S(2)}) copy-start(bf16[2,32,128]{2,1,0:T(8,128)(2,1)} %get-tuple-element.51) | copy-start | bytes 49156
  289.2 44.1 %all-to-all-start.5 = ((bf16[32,8,4096]{2,1,0:T(8,128)(2,1)}), bf16[32,8,4096]{2,1,0:T(8,128)(2,1)S(1)}, u32[]{:S(2)}, u32[]{:S(2)}) async-start(bf16[32,8,4096]{2,1,0:T(8,128)(2,1)} %bitcast.42), calls=%async_computation.5 | async-start | bytes 4194304 | tf_op jit(solution)/shard_map/all_to_all | solution.py:570
  298.5 27.1 %collective-permute-start.10 = (f32[2,136,128]{2,1,0:T(8,128)S(1)}, f32[2,136,128]{2,1,0:T(8,128)S(1)}, u32[]{:S(2)}, u32[]{:S(2)}) collective-permute-start(f32[2,136,128]{2,1,0:T(8,128)S(1)} %pad_maximum_fusion.2), channel_id=1, source_target_pairs={{0,96},{1,97},{2,98},{3,99},{4,100},{5,101},{6,102},{7,103},{8,104... | collective-permute-start | bytes 417800 | tf_op jit(solution)/shard_map/ppermute | solution.py:344
  303.2 22.5 %collective-permute-start.11 = (f32[2,136,128]{2,1,0:T(8,128)S(1)}, f32[2,136,128]{2,1,0:T(8,128)S(1)}, u32[]{:S(2)}, u32[]{:S(2)}) collective-permute-start(f32[2,136,128]{2,1,0:T(8,128)S(1)} %pad_maximum_fusion.2), channel_id=1, source_target_pairs={{0,64},{32,96},{1,65},{33,97},{2,66},{34,98},{3,67},{35,99},{4,68}... | collective-permute-start | bytes 417800 | tf_op jit(solution)/shard_map/ppermute | solution.py:344
  304.5 21.4 %collective-permute-start.12 = (f32[2,136,128]{2,1,0:T(8,128)S(1)}, f32[2,136,128]{2,1,0:T(8,128)S(1)}, u32[]{:S(2)}, u32[]{:S(2)}) collective-permute-start(f32[2,136,128]{2,1,0:T(8,128)S(1)} %pad_maximum_fusion.2), channel_id=1, source_target_pairs={{0,32},{32,64},{64,96},{1,33},{33,65},{65,97},{2,34},{34,66},{66,9... | collective-permute-start | bytes 417800 | tf_op jit(solution)/shard_map/ppermute | solution.py:344
  307.3 5.0 %collective-permute-start.20 = (bf16[2,32,128]{2,1,0:T(8,128)(2,1)S(1)}, bf16[2,32,128]{2,1,0:T(8,128)(2,1)S(1)}, u32[]{:S(2)}, u32[]{:S(2)}) collective-permute-start(bf16[2,32,128]{2,1,0:T(8,128)(2,1)S(1)} %copy-done.15), channel_id=1, source_target_pairs={{0,3},{1,2},{2,1},{3,0},{4,7},{5,6},{6,5},{7,4},{8,11},{9,10},{10,... | collective-permute-start | bytes 49160 | tf_op jit(solution)/shard_map/ppermute | solution.py:558
  327.0 1.4 collective-permute-start.19
  333.3 1.4 copy-start

commit v2 on v1

--- a/solution.py
+++ b/solution.py
@@ -341,7 +341,7 @@
     plane = pack(link(link(before, chip), after))
     count = lax.axis_size("ep_0")
     planes = [
-        lax.ppermute(plane, "ep_0", [(i, i + d) for i in range(count - d)])
+        lax.ppermute(plane, "ep_0", [(i, (i + d) % count) for i in range(count)])
         for d in range(count - 1, 0, -1)
     ]
     return before, planes
@@ -349,9 +349,11 @@
 
 def arriving_state(low, before, planes):
     is_second = lax.axis_index("ep_2") == 1
+    at = lax.axis_index("ep_0")
     total = None
-    for part in planes:
-        total = pieces(part) if total is None else link(total, pieces(part))
+    for k, part in enumerate(planes):
+        part = masked(at >= len(planes) - k, pieces(part))
+        total = part if total is None else link(total, part)
     state = link(total, before)[1]
     swapped = both_cores(state)
     entering = jnp.concatenate(
@@ -548,6 +550,7 @@
 
 NEAR = [(i, i ^ 1) for i in range(4)]
 FAR = [(i, 3 - i) for i in range(4)]
+OPPOSITE = [(i, i ^ 2) for i in range(4)]
 
 
 def to_near(a):
@@ -558,10 +561,10 @@
     return lax.ppermute(a, "tp", FAR)
 
 
-def shared(a):
+def shared(a, direct=True):
     far = to_far(a)
     near = to_near(a)
-    return a, near, far, to_near(far)
+    return a, near, far, (lax.ppermute(a, "tp", OPPOSITE) if direct else to_near(far))
 
 
 def swap(a):
@@ -596,7 +599,7 @@
     router = router_weight.T
 
     rows_a = normed(mix_input, norm_mix).astype(BF16)
-    group_a = shared(rows_a)
+    group_a = shared(rows_a, direct=False)
     rows_b, own = front(src, moe_input, norm_moe.reshape(1, -1), by_block, router_weight.shape[1])
     own_rows = swap(own)
     rows_near = to_near(rows_b)
@@ -619,16 +622,17 @@
     weights = (expert_gate[0], expert_up[0], gate_far, up_far)
     h_low = hidden_units(own_rows, low_rows, 0, weights)
     h_low = shared(h_low)
-    came, _ = lax.optimization_barrier((came, h_low[0]))
-    before, planes = along_planes(chip, came)
     down_first = down_rows(src, h_low[0], h_low[1], 0, expert_down[0])
     back_first = swap(down_first)
-    high_rows, far = lax.optimization_barrier((high_rows, h_low[2]))
     h_high = hidden_units(own_rows, high_rows, 1, weights)
     h_high = shared(h_high)
+    far, high_own = lax.optimization_barrier((h_low[2], h_high[0]))
+    h_high = (high_own,) + h_high[1:]
     down_second = down_rows(src, far, h_low[3], 2, expert_down[0])
     down_second, back_first = lax.optimization_barrier((down_second, back_first))
     back_second = swap(down_second)
+    came, _ = lax.optimization_barrier((came, down_second))
+    before, planes = along_planes(chip, came)
     down_high = down_rows4(src, h_high, expert_down[0])
     down_high, back_second = lax.optimization_barrier((down_high, back_second))
     back_high = swap(down_high)

time: 343 us -> 361 us (1.052)
  waiting for transfers between devices: 169 us -> 193 us
  starting transfers between devices: 78.1 us -> 72.1 us
    ppermute x6, waiting for transfers between devices: 18.4 us -> 39.8 us  [to_far(): return lax.ppermute(a, 'tp', FAR)]
    ppermute x3 -> x5, waiting for transfers between devices: 8.89 us -> 18.3 us  [the longest x3 16.2 us: along_planes(): lax.ppermute(plane, 'ep_0', [(i, (i + d) % count) for i in range(count)])]
    ppermute x7 -> x5, waiting for transfers between devices: 89 us -> 82.6 us  [to_near(): return lax.ppermute(a, 'tp', NEAR)]
    ppermute x3 -> x5, starting transfers between devices: 8.71 us -> 5.86 us  [the longest x3 4.47 us: along_planes(): lax.ppermute(plane, 'ep_0', [(i, (i + d) % count) for i in range(count)])]
  transfers between devices with their start and end apart: 27 -> 27, of which waited for: 15 -> 18; matrix products, arithmetic and copies ran while one was open for 2% -> 2% of each run, Pallas kernels for 19% -> 18%
where the time goes in v2:
time: 361 us; the launch traced here: 359 us
  waiting for transfers between devices  193 us (53%)
  Pallas kernels  77.5 us (21%)
  starting transfers between devices  72.1 us (20%)
  other arithmetic  8.87 us (2%)
  local copies, waits for them, and re-layouts  6.54 us (2%)
    ppermute x5, waiting for transfers between devices, to_near(): return lax.ppermute(a, 'tp', NEAR)  82.6 us
    all_to_all x6, starting transfers between devices, swap(): lax.all_to_all(a.reshape(experts, rows // experts, cols), EP, split_axis=...  44 us
    ppermute x6, waiting for transfers between devices, to_far(): return lax.ppermute(a, 'tp', FAR)  39.8 us
    all_to_all x6, waiting for transfers between devices, swap(): lax.all_to_all(a.reshape(experts, rows // experts, cols), EP, split_axis=...  39.6 us
    pallas_call x2, Pallas kernels, hidden_units(): pl.pallas_call(hidden_kernel, grid=(width // kb,), in_specs=[pl.BlockSpec...  17.7 us
    pallas_call x1, Pallas kernels, mixer(): pl.pallas_call(mixer_kernel, grid_spec=pltpu.PrefetchScalarGridSpec(num_s...  17.5 us
    ppermute x3, waiting for transfers between devices, along_planes(): lax.ppermute(plane, 'ep_0', [(i, (i + d) % count) for i in range(count)])  16.2 us
    ppermute x6, starting transfers between devices, to_far(): return lax.ppermute(a, 'tp', FAR)  13.5 us
  transfers between devices with their start and end apart: 27, of which 18 were waited for; matrix products, arithmetic and copies ran while one was open for 2% of the time, Pallas kernels for 18%

profile of v2, /device:TPU:8, one launch (start us, length us, event | category | flops | bytes accessed | tf_op | source)
XLA Modules:
  0.0 358.5 jit_solution(16087865346490410416)
XLA Ops:
  1.3 5.8 %front.1 = (bf16[128,4096]{1,0:T(8,128)(2,1)}, bf16[256,8192]{1,0:T(8,128)(2,1)}) custom-call(s32[4]{0:T(128)} %pad_add_fusion.src, bf16[128,4096]{1,0:T(8,128)(2,1)} %x_ref.1, f32[1,4096]{1,0:T(1,128)} %bitcast.57, s32[4,2,128]{2,1,0:T(2,128)} %bitcast.54), custom_call_target="tpu_custom_call" | custom-call | tf_op jit(solution)/shard_map/front/pallas_call | solution.py:100
  7.0 8.7 %all-to-all-start = ((bf16[32,8,8192]{2,1,0:T(8,128)(2,1)}), bf16[32,8,8192]{2,1,0:T(8,128)(2,1)}, u32[]{:S(2)}, u32[]{:S(2)}) async-start(bf16[32,8,8192]{2,1,0:T(8,128)(2,1)} %bitcast.50), calls=%async_computation | async-start | bytes 8388608 | tf_op jit(solution)/shard_map/all_to_all | solution.py:573
  15.8 1.6 collective-permute-start.7
  17.3 23.7 %collective-permute-done.7.rows_ref = bf16[128,4096]{1,0:T(8,128)(2,1)S(1)} collective-permute-done((bf16[128,4096]{1,0:T(8,128)(2,1)S(1)}, bf16[128,4096]{1,0:T(8,128)(2,1)S(1)}, u32[]{:S(2)}, u32[]{:S(2)}) %collective-permute-start.7) | collective-permute-done | bytes 1048608 | tf_op jit(solution)/shard_map/ppermute | solution.py:557
  42.0 6.0 %refill.1 = (bf16[2,32,128]{2,1,0:T(8,128)(2,1)}, bf16[256,4096]{1,0:T(8,128)(2,1)}, bf16[256,4096]{1,0:T(8,128)(2,1)}) custom-call(s32[4]{0:T(128)} %pad_add_fusion.src, bf16[128,4096]{1,0:T(8,128)(2,1)} %get-tuple-element.30.own_ref, bf16[128,4096]{1,0:T(8,128)(2,1)} %copy-done.8, bf16[32,4096]{1,0:T(8,128)(2,1)} %bitcast.53, s32[4,2,128]{2,1,0:T(2,128)} %bitcast.55), custom_call_target="tpu_custom_call" | custom-call | tf_op jit(solution)/shard_map/refill/pallas_call | solution.py:129
  48.0 19.1 %all-to-all-done = bf16[32,8,8192]{2,1,0:T(8,128)(2,1)} async-done(((bf16[32,8,8192]{2,1,0:T(8,128)(2,1)}), bf16[32,8,8192]{2,1,0:T(8,128)(2,1)}, u32[]{:S(2)}, u32[]{:S(2)}) %all-to-all-start) | async-done | bytes 4194336 | tf_op jit(solution)/shard_map/all_to_all | solution.py:573
  67.2 6.6 %all-to-all-start.1 = ((bf16[32,8,4096]{2,1,0:T(8,128)(2,1)}), bf16[32,8,4096]{2,1,0:T(8,128)(2,1)S(1)}, u32[]{:S(2)}, u32[]{:S(2)}) async-start(bf16[32,8,4096]{2,1,0:T(8,128)(2,1)} %bitcast.52), calls=%async_computation.1 | async-start | bytes 4194304 | tf_op jit(solution)/shard_map/all_to_all | solution.py:573
  75.5 2.8 collective-permute-start.1
  78.7 2.8 collective-permute-start.9
  81.5 20.4 %all-to-all-done.1 = bf16[32,8,4096]{2,1,0:T(8,128)(2,1)S(1)} async-done(((bf16[32,8,4096]{2,1,0:T(8,128)(2,1)}), bf16[32,8,4096]{2,1,0:T(8,128)(2,1)S(1)}, u32[]{:S(2)}, u32[]{:S(2)}) %all-to-all-start.1) | async-done | bytes 2097184 | tf_op jit(solution)/shard_map/all_to_all | solution.py:573
  101.9 1.4 copy-done.2
  103.3 6.1 %all-to-all-start.2 = ((bf16[32,8,4096]{2,1,0:T(8,128)(2,1)}), bf16[32,8,4096]{2,1,0:T(8,128)(2,1)S(1)}, u32[]{:S(2)}, u32[]{:S(2)}) async-start(bf16[32,8,4096]{2,1,0:T(8,128)(2,1)} %bitcast.51), calls=%async_computation.2 | async-start | bytes 4194304 | tf_op jit(solution)/shard_map/all_to_all | solution.py:573
  109.4 1.6 collective-permute-start
  111.5 24.2 %collective-permute-done.a1 = bf16[128,4096]{1,0:T(8,128)(2,1)S(1)} collective-permute-done((bf16[128,4096]{1,0:T(8,128)(2,1)}, bf16[128,4096]{1,0:T(8,128)(2,1)S(1)}, u32[]{:S(2)}, u32[]{:S(2)}) %collective-permute-start) | collective-permute-done | bytes 1048608 | tf_op jit(solution)/shard_map/ppermute | solution.py:557
  135.7 21.6 %collective-permute-done.2.a3 = bf16[128,4096]{1,0:T(8,128)(2,1)S(1)} collective-permute-done((bf16[128,4096]{1,0:T(8,128)(2,1)}, bf16[128,4096]{1,0:T(8,128)(2,1)S(1)}, u32[]{:S(2)}, u32[]{:S(2)}) %collective-permute-start.2) | collective-permute-done | bytes 1048608 | tf_op jit(solution)/shard_map/ppermute | solution.py:557
  158.3 17.5 %mixer.1 = (f32[512,512]{1,0:T(8,128)}, f32[512,512]{1,0:T(8,128)}, f32[4,136,128]{2,1,0:T(8,128)}) custom-call(s32[4]{0:T(128)} %pad_add_fusion.src, bf16[128,4096]{1,0:T(8,128)(2,1)} %fusion.2.a0, bf16[128,4096]{1,0:T(8,128)(2,1)} %copy-done.9, bf16[128,4096]{1,0:T(8,128)(2,1)} %collective-permute-done.1.a2, bf16[128,4096]{1,0:T(8,128)(2,1)} %copy-done.10, ...), custom_call_target="tpu_custom_call" | custom-call | tf_op jit(solution)/shard_map/mixer/pallas_call | solution.py:237
  175.9 16.2 %collective-permute-done.9.uf_ref = bf16[4096,256]{1,0:T(8,128)(2,1)} collective-permute-done((bf16[4096,256]{1,0:T(8,128)(2,1)}, bf16[4096,256]{1,0:T(8,128)(2,1)}, u32[]{:S(2)}, u32[]{:S(2)}) %collective-permute-start.9) | collective-permute-done | bytes 2097184 | tf_op jit(solution)/shard_map/ppermute | solution.py:561
  192.1 8.8 %hidden.2.this = bf16[512,512]{1,0:T(8,128)(2,1)} custom-call(bf16[256,8192]{1,0:T(8,128)(2,1)} %bitcast.13.own_ref, bf16[256,4096]{1,0:T(8,128)(2,1)} %bitcast.45, bf16[4096,256]{1,0:T(8,128)(2,1)} %bitcast.16.go_ref, bf16[4096,256]{1,0:T(8,128)(2,1)} %bitcast.17.uo_ref, bf16[4096,256]{1,0:T(8,128)(2,1)} %collective-permute-done.8.gf_ref, ...), custom_call_target="tpu_custom_call" | custom-call | tf_op jit(solution)/shard_map/hidden/pallas_call | solution.py:395
  201.2 13.0 %collective-permute-done.12.twin = bf16[512,512]{1,0:T(8,128)(2,1)S(1)} collective-permute-done((bf16[512,512]{1,0:T(8,128)(2,1)}, bf16[512,512]{1,0:T(8,128)(2,1)S(1)}, u32[]{:S(2)}, u32[]{:S(2)}) %collective-permute-start.12) | collective-permute-done | bytes 524320 | tf_op jit(solution)/shard_map/ppermute | solution.py:557
  215.0 4.9 %down.3 = bf16[256,2048]{1,0:T(8,128)(2,1)} custom-call(s32[4]{0:T(128)} %pad_add_fusion.src, bf16[512,512]{1,0:T(8,128)(2,1)} %hidden.2.this, bf16[512,512]{1,0:T(8,128)(2,1)} %copy-done.13, bf16[1024,1024]{1,0:T(8,128)(2,1)} %bitcast.39), custom_call_target="tpu_custom_call" | custom-call | tf_op jit(solution)/shard_map/down/pallas_call | solution.py:433
  219.9 7.6 %all-to-all-start.3 = ((bf16[32,8,2048]{2,1,0:T(8,128)(2,1)}), bf16[32,8,2048]{2,1,0:T(8,128)(2,1)S(1)}, u32[]{:S(2)}, u32[]{:S(2)}) async-start(bf16[32,8,2048]{2,1,0:T(8,128)(2,1)} %bitcast.49), calls=%async_computation.3 | async-start | bytes 2097152 | tf_op jit(solution)/shard_map/all_to_all | solution.py:573
  227.5 2.8 collective-permute-start.10
  230.4 8.8 %hidden.3.h_own = bf16[512,512]{1,0:T(8,128)(2,1)} custom-call(bf16[256,8192]{1,0:T(8,128)(2,1)} %bitcast.13.own_ref, bf16[256,4096]{1,0:T(8,128)(2,1)} %bitcast.44, bf16[4096,256]{1,0:T(8,128)(2,1)} %bitcast.16.go_ref, bf16[4096,256]{1,0:T(8,128)(2,1)} %bitcast.17.uo_ref, bf16[4096,256]{1,0:T(8,128)(2,1)} %collective-permute-done.8.gf_ref, ...), custom_call_target="tpu_custom_call" | custom-call | tf_op jit(solution)/shard_map/hidden/pallas_call | solution.py:395
  239.2 15.1 %collective-permute-done.10.this = bf16[512,512]{1,0:T(8,128)(2,1)} collective-permute-done((bf16[512,512]{1,0:T(8,128)(2,1)}, bf16[512,512]{1,0:T(8,128)(2,1)}, u32[]{:S(2)}, u32[]{:S(2)}) %collective-permute-start.10) | collective-permute-done | bytes 524320 | tf_op jit(solution)/shard_map/ppermute | solution.py:561
  254.3 4.9 %down.2 = bf16[256,2048]{1,0:T(8,128)(2,1)} custom-call(s32[4]{0:T(128)} %pad_add_fusion.src, bf16[512,512]{1,0:T(8,128)(2,1)} %collective-permute-done.10.this, bf16[512,512]{1,0:T(8,128)(2,1)} %collective-permute-done.11.twin, bf16[1024,1024]{1,0:T(8,128)(2,1)} %bitcast.40), custom_call_target="tpu_custom_call" | custom-call | tf_op jit(solution)/shard_map/down/pallas_call | solution.py:433
  259.2 7.5 %all-to-all-start.4 = ((bf16[32,8,2048]{2,1,0:T(8,128)(2,1)}), bf16[32,8,2048]{2,1,0:T(8,128)(2,1)S(1)}, u32[]{:S(2)}, u32[]{:S(2)}) async-start(bf16[32,8,2048]{2,1,0:T(8,128)(2,1)} %bitcast.48), calls=%async_computation.4 | async-start | bytes 2097152 | tf_op jit(solution)/shard_map/all_to_all | solution.py:573
  268.3 2.8 collective-permute-start.17
  271.1 1.4 collective-permute-start.18
  273.5 2.7 collective-permute-start.5
  276.2 7.4 %collective-permute-done.4 = f32[2,136,128]{2,1,0:T(8,128)} collective-permute-done((f32[2,136,128]{2,1,0:T(8,128)}, f32[2,136,128]{2,1,0:T(8,128)}, u32[]{:S(2)}, u32[]{:S(2)}) %collective-permute-start.4) | collective-permute-done | bytes 139296 | tf_op jit(solution)/shard_map/ppermute | solution.py:326
  283.6 1.7 collective-permute-start.6
  285.3 1.8 collective-permute-done.5
  287.2 1.8 collective-permute-done.6
  289.0 5.4 %collective-permute-done.17.h_far = bf16[512,512]{1,0:T(8,128)(2,1)} collective-permute-done((bf16[512,512]{1,0:T(8,128)(2,1)S(1)}, bf16[512,512]{1,0:T(8,128)(2,1)}, u32[]{:S(2)}, u32[]{:S(2)}) %collective-permute-start.17) | collective-permute-done | bytes 524320 | tf_op jit(solution)/shard_map/ppermute | solution.py:561
  294.5 2.1 collective-permute-done.18.h_opp
  296.5 6.8 %down4.1 = bf16[256,4096]{1,0:T(8,128)(2,1)} custom-call(s32[4]{0:T(128)} %pad_add_fusion.src, bf16[512,512]{1,0:T(8,128)(2,1)} %hidden.3.h_own, bf16[512,512]{1,0:T(8,128)(2,1)} %copy-done.12, bf16[512,512]{1,0:T(8,128)(2,1)} %collective-permute-done.17.h_far, bf16[512,512]{1,0:T(8,128)(2,1)} %collective-permute-done.18.h_opp, bf16[1024,1024]{1,0:T(8,128)(2,1)} %bitcast.41), custom_call_target="tpu_custom_call" | custom-call | tf_op jit(solution)/shard_map/down4/pallas_call | solution.py:468
  304.3 7.4 %all-to-all-start.5 = ((bf16[32,8,4096]{2,1,0:T(8,128)(2,1)}), bf16[32,8,4096]{2,1,0:T(8,128)(2,1)S(1)}, u32[]{:S(2)}, u32[]{:S(2)}) async-start(bf16[32,8,4096]{2,1,0:T(8,128)(2,1)} %bitcast.42), calls=%async_computation.5 | async-start | bytes 4194304 | tf_op jit(solution)/shard_map/all_to_all | solution.py:573
  313.7 2.8 collective-permute-start.13
  318.1 1.9 collective-permute-start.20
  320.0 3.1 collective-permute-done.20
  323.7 4.0 %places.1.place_ref = bf16[4,256,512]{2,1,0:T(8,128)(2,1)} custom-call(s32[4]{0:T(128)} %pad_add_fusion.src, s32[4,2,128]{2,1,0:T(2,128)} %bitcast.56, bf16[4,32,128]{2,1,0:T(8,128)(2,1)} %pad_maximum_fusion.3.logits_ref), custom_call_target="tpu_custom_call" | custom-call | tf_op jit(solution)/shard_map/places/pallas_call | solution.py:498
  327.7 12.6 %collective-permute-done.13 = f32[2,136,128]{2,1,0:T(8,128)S(1)} collective-permute-done((f32[2,136,128]{2,1,0:T(8,128)S(1)}, f32[2,136,128]{2,1,0:T(8,128)S(1)}, u32[]{:S(2)}, u32[]{:S(2)}) %collective-permute-start.13) | collective-permute-done | bytes 139296 | tf_op jit(solution)/shard_map/ppermute | solution.py:344
  340.3 1.5 collective-permute-done.14
  341.8 2.2 collective-permute-done.15
  345.2 1.3 collective-permute-done.19
  347.3 4.2 %readout.1 = bf16[512,512]{1,0:T(8,128)(2,1)} custom-call(f32[512,512]{1,0:T(8,128)} %get-tuple-element.27.inside_ref, f32[512,512]{1,0:T(8,128)} %get-tuple-element.28.query_ref, f32[4,128,128]{2,1,0:T(8,128)} %fusion.3.state_ref, f32[1,512]{1,0:T(1,128)} %bitcast.73), custom_call_target="tpu_custom_call" | custom-call | tf_op jit(solution)/shard_map/readout/pallas_call | solution.py:275
  351.4 1.3 copy-done
  352.8 5.7 %combine.1 = bf16[512,1024]{1,0:T(8,128)(2,1)} custom-call(s32[4]{0:T(128)} %pad_add_fusion.src, bf16[256,2048]{1,0:T(8,128)(2,1)} %bitcast.46, bf16[256,2048]{1,0:T(8,128)(2,1)} %bitcast.47, bf16[256,4096]{1,0:T(8,128)(2,1)} %bitcast.43, bf16[4,256,512]{2,1,0:T(8,128)(2,1)} %places.1.place_ref), custom_call_target="tpu_custom_call" | custom-call | tf_op jit(solution)/shard_map/combine/pallas_call | solution.py:532
  (76 shorter events, 16.0 us)
Async XLA Ops:
  7.0 8.7 %copy-start.7 = (bf16[128,4096]{1,0:T(8,128)(2,1)S(1)}, bf16[128,4096]{1,0:T(8,128)(2,1)}, u32[]{:S(2)}) copy-start(bf16[128,4096]{1,0:T(8,128)(2,1)} %get-tuple-element.30.own_ref) | copy-start | bytes 3145732
  7.0 60.2 %all-to-all-start = ((bf16[32,8,8192]{2,1,0:T(8,128)(2,1)}), bf16[32,8,8192]{2,1,0:T(8,128)(2,1)}, u32[]{:S(2)}, u32[]{:S(2)}) async-start(bf16[32,8,8192]{2,1,0:T(8,128)(2,1)} %bitcast.50), calls=%async_computation | async-start | bytes 8388608 | tf_op jit(solution)/shard_map/all_to_all | solution.py:573
  15.8 25.3 %collective-permute-start.7 = (bf16[128,4096]{1,0:T(8,128)(2,1)S(1)}, bf16[128,4096]{1,0:T(8,128)(2,1)S(1)}, u32[]{:S(2)}, u32[]{:S(2)}) collective-permute-start(bf16[128,4096]{1,0:T(8,128)(2,1)S(1)} %copy-done.7), channel_id=1, source_target_pairs={{0,1},{1,0},{2,3},{3,2},{4,5},{5,4},{6,7},{7,6},{8,9},{9,8},{10,11... | collective-permute-start | bytes 3145736 | tf_op jit(solution)/shard_map/ppermute | solution.py:557
  41.0 1.0 copy-start.8
  67.2 6.7 %copy-start.5 = (bf16[128,4096]{1,0:T(8,128)(2,1)S(1)}, bf16[128,4096]{1,0:T(8,128)(2,1)}, u32[]{:S(2)}) copy-start(bf16[128,4096]{1,0:T(8,128)(2,1)} %param.14) | copy-start | bytes 3145732
  67.2 7.0 %copy-start.14 = (f32[4096]{0:T(1024)S(1)}, f32[4096]{0:T(1024)}, u32[]{:S(2)}) copy-start(f32[4096]{0:T(1024)} %param.16) | copy-start | bytes 49156
  67.2 34.7 %all-to-all-start.1 = ((bf16[32,8,4096]{2,1,0:T(8,128)(2,1)}), bf16[32,8,4096]{2,1,0:T(8,128)(2,1)S(1)}, u32[]{:S(2)}, u32[]{:S(2)}) async-start(bf16[32,8,4096]{2,1,0:T(8,128)(2,1)} %bitcast.52), calls=%async_computation.1 | async-start | bytes 4194304 | tf_op jit(solution)/shard_map/all_to_all | solution.py:573
  75.5 35.5 %collective-permute-start.1 = (bf16[128,4096]{1,0:T(8,128)(2,1)}, bf16[128,4096]{1,0:T(8,128)(2,1)}, u32[]{:S(2)}, u32[]{:S(2)}) collective-permute-start(bf16[128,4096]{1,0:T(8,128)(2,1)} %fusion.2.a0), channel_id=1, source_target_pairs={{0,3},{1,2},{2,1},{3,0},{4,7},{5,6},{6,5},{7,4},{8,11},{9,10},{10,... | collective-permute-start | bytes 3145736 | tf_op jit(solution)/shard_map/ppermute | solution.py:561
  78.2 97.6 %collective-permute-start.8 = (bf16[4096,256]{1,0:T(8,128)(2,1)}, bf16[4096,256]{1,0:T(8,128)(2,1)}, u32[]{:S(2)}, u32[]{:S(2)}) collective-permute-start(bf16[4096,256]{1,0:T(8,128)(2,1)} %bitcast.16.go_ref), channel_id=1, source_target_pairs={{0,3},{1,2},{2,1},{3,0},{4,7},{5,6},{6,5},{7,4},{8,11},{9,10},{10,... | collective-permute-start | bytes 6291464 | tf_op jit(solution)/shard_map/ppermute | solution.py:561
  78.7 113.4 %collective-permute-start.9 = (bf16[4096,256]{1,0:T(8,128)(2,1)}, bf16[4096,256]{1,0:T(8,128)(2,1)}, u32[]{:S(2)}, u32[]{:S(2)}) collective-permute-start(bf16[4096,256]{1,0:T(8,128)(2,1)} %bitcast.17.uo_ref), channel_id=1, source_target_pairs={{0,3},{1,2},{2,1},{3,0},{4,7},{5,6},{6,5},{7,4},{8,11},{9,10},{10,... | collective-permute-start | bytes 6291464 | tf_op jit(solution)/shard_map/ppermute | solution.py:561
  101.9 1.4 copy-start.2
  103.3 116.6 %all-to-all-start.2 = ((bf16[32,8,4096]{2,1,0:T(8,128)(2,1)}), bf16[32,8,4096]{2,1,0:T(8,128)(2,1)S(1)}, u32[]{:S(2)}, u32[]{:S(2)}) async-start(bf16[32,8,4096]{2,1,0:T(8,128)(2,1)} %bitcast.51), calls=%async_computation.2 | async-start | bytes 4194304 | tf_op jit(solution)/shard_map/all_to_all | solution.py:573
  109.4 26.3 %collective-permute-start = (bf16[128,4096]{1,0:T(8,128)(2,1)}, bf16[128,4096]{1,0:T(8,128)(2,1)S(1)}, u32[]{:S(2)}, u32[]{:S(2)}) collective-permute-start(bf16[128,4096]{1,0:T(8,128)(2,1)} %fusion.2.a0), channel_id=1, source_target_pairs={{0,1},{1,0},{2,3},{3,2},{4,5},{5,4},{6,7},{7,6},{8,9},{9,8},{10,11... | collective-permute-start | bytes 3145736 | tf_op jit(solution)/shard_map/ppermute | solution.py:557
  111.0 46.4 %collective-permute-start.2 = (bf16[128,4096]{1,0:T(8,128)(2,1)}, bf16[128,4096]{1,0:T(8,128)(2,1)S(1)}, u32[]{:S(2)}, u32[]{:S(2)}) collective-permute-start(bf16[128,4096]{1,0:T(8,128)(2,1)} %collective-permute-done.1.a2), channel_id=1, source_target_pairs={{0,1},{1,0},{2,3},{3,2},{4,5},{5,4},{6,7},{7,6},{8,9},{9,8},{10,11... | collective-permute-start | bytes 3145736 | tf_op jit(solution)/shard_map/ppermute | solution.py:557
  135.7 21.6 %copy-start.9 = (bf16[128,4096]{1,0:T(8,128)(2,1)}, bf16[128,4096]{1,0:T(8,128)(2,1)S(1)}, u32[]{:S(2)}) copy-start(bf16[128,4096]{1,0:T(8,128)(2,1)S(1)} %collective-permute-done.a1) | copy-start | bytes 3145732
  157.3 1.0 copy-start.10
  200.9 13.3 %collective-permute-start.12 = (bf16[512,512]{1,0:T(8,128)(2,1)}, bf16[512,512]{1,0:T(8,128)(2,1)S(1)}, u32[]{:S(2)}, u32[]{:S(2)}) collective-permute-start(bf16[512,512]{1,0:T(8,128)(2,1)} %hidden.2.this), channel_id=1, source_target_pairs={{0,1},{1,0},{2,3},{3,2},{4,5},{5,4},{6,7},{7,6},{8,9},{9,8},{10,11... | collective-permute-start | bytes 1572872 | tf_op jit(solution)/shard_map/ppermute | solution.py:557
  214.2 0.8 copy-start.13
  219.8 10.5 %copy-start.11 = (f32[4,136,128]{2,1,0:T(8,128)S(1)}, f32[4,136,128]{2,1,0:T(8,128)}, u32[]{:S(2)}) copy-start(f32[4,136,128]{2,1,0:T(8,128)} %get-tuple-element.29) | copy-start | bytes 835588
  219.9 10.5 %copy-start.1 = (bf16[32,8,4096]{2,1,0:T(8,128)(2,1)}, bf16[32,8,4096]{2,1,0:T(8,128)(2,1)S(1)}, u32[]{:S(2)}) copy-start(bf16[32,8,4096]{2,1,0:T(8,128)(2,1)S(1)} %all-to-all-done.2) | copy-start | bytes 6291460
  219.9 39.3 %all-to-all-start.3 = ((bf16[32,8,2048]{2,1,0:T(8,128)(2,1)}), bf16[32,8,2048]{2,1,0:T(8,128)(2,1)S(1)}, u32[]{:S(2)}, u32[]{:S(2)}) async-start(bf16[32,8,2048]{2,1,0:T(8,128)(2,1)} %bitcast.49), calls=%async_computation.3 | async-start | bytes 2097152 | tf_op jit(solution)/shard_map/all_to_all | solution.py:573
  227.5 26.8 %collective-permute-start.10 = (bf16[512,512]{1,0:T(8,128)(2,1)}, bf16[512,512]{1,0:T(8,128)(2,1)}, u32[]{:S(2)}, u32[]{:S(2)}) collective-permute-start(bf16[512,512]{1,0:T(8,128)(2,1)} %hidden.2.this), channel_id=1, source_target_pairs={{0,3},{1,2},{2,1},{3,0},{4,7},{5,6},{6,5},{7,4},{8,11},{9,10},{10,... | collective-permute-start | bytes 1572872 | tf_op jit(solution)/shard_map/ppermute | solution.py:561
  230.3 23.9 %collective-permute-start.11 = (bf16[512,512]{1,0:T(8,128)(2,1)}, bf16[512,512]{1,0:T(8,128)(2,1)}, u32[]{:S(2)}, u32[]{:S(2)}) collective-permute-start(bf16[512,512]{1,0:T(8,128)(2,1)} %hidden.2.this), channel_id=1, source_target_pairs={{0,2},{1,3},{2,0},{3,1},{4,6},{5,7},{6,4},{7,5},{8,10},{9,11},{10,... | collective-permute-start | bytes 1572872 | tf_op jit(solution)/shard_map/ppermute | solution.py:567
  230.3 36.4 %collective-permute-start.3 = (f32[4,136,128]{2,1,0:T(8,128)S(1)}, f32[4,136,128]{2,1,0:T(8,128)}, u32[]{:S(2)}, u32[]{:S(2)}) collective-permute-start(f32[4,136,128]{2,1,0:T(8,128)S(1)} %copy-done.11), channel_id=1, source_target_pairs={{0,4},{4,0},{1,5},{5,1},{2,6},{6,2},{3,7},{7,3},{8,12},{12,8},{9,1... | collective-permute-start | bytes 835592 | tf_op jit(solution)/shard_map/ppermute | solution.py:311
  259.2 9.1 %copy-start.6 = (bf16[512,512]{1,0:T(8,128)(2,1)S(1)}, bf16[512,512]{1,0:T(8,128)(2,1)}, u32[]{:S(2)}) copy-start(bf16[512,512]{1,0:T(8,128)(2,1)} %hidden.3.h_own) | copy-start | bytes 1572868
  259.2 44.1 %copy-start.3 = (bf16[32,8,2048]{2,1,0:T(8,128)(2,1)}, bf16[32,8,2048]{2,1,0:T(8,128)(2,1)S(1)}, u32[]{:S(2)}) copy-start(bf16[32,8,2048]{2,1,0:T(8,128)(2,1)S(1)} %all-to-all-done.3) | copy-start | bytes 3145732
  259.2 44.1 %all-to-all-start.4 = ((bf16[32,8,2048]{2,1,0:T(8,128)(2,1)}), bf16[32,8,2048]{2,1,0:T(8,128)(2,1)S(1)}, u32[]{:S(2)}, u32[]{:S(2)}) async-start(bf16[32,8,2048]{2,1,0:T(8,128)(2,1)} %bitcast.48), calls=%async_computation.4 | async-start | bytes 2097152 | tf_op jit(solution)/shard_map/all_to_all | solution.py:573
  268.3 4.9 %copy-start.16 = (f32[2,1,128]{2,1,0:T(1,128)}, f32[2,1,128]{2,1,0:T(1,128)S(1)}, u32[]{:S(2)}) copy-start(f32[2,1,128]{2,1,0:T(1,128)S(1)} %get-tuple-element.57) | copy-start | bytes 3076
  268.3 20.7 %collective-permute-start.16 = (bf16[512,512]{1,0:T(8,128)(2,1)S(1)}, bf16[512,512]{1,0:T(8,128)(2,1)S(1)}, u32[]{:S(2)}, u32[]{:S(2)}) collective-permute-start(bf16[512,512]{1,0:T(8,128)(2,1)S(1)} %copy-done.6), channel_id=1, source_target_pairs={{0,1},{1,0},{2,3},{3,2},{4,5},{5,4},{6,7},{7,6},{8,9},{9,8},{10,11... | collective-permute-start | bytes 1572872 | tf_op jit(solution)/shard_map/ppermute | solution.py:557
  268.3 26.1 %collective-permute-start.17 = (bf16[512,512]{1,0:T(8,128)(2,1)S(1)}, bf16[512,512]{1,0:T(8,128)(2,1)}, u32[]{:S(2)}, u32[]{:S(2)}) collective-permute-start(bf16[512,512]{1,0:T(8,128)(2,1)S(1)} %copy-done.6), channel_id=1, source_target_pairs={{0,3},{1,2},{2,1},{3,0},{4,7},{5,6},{6,5},{7,4},{8,11},{9,10},{10,... | collective-permute-start | bytes 1572872 | tf_op jit(solution)/shard_map/ppermute | solution.py:561
  271.1 25.4 %collective-permute-start.18 = (bf16[512,512]{1,0:T(8,128)(2,1)S(1)}, bf16[512,512]{1,0:T(8,128)(2,1)}, u32[]{:S(2)}, u32[]{:S(2)}) collective-permute-start(bf16[512,512]{1,0:T(8,128)(2,1)S(1)} %copy-done.6), channel_id=1, source_target_pairs={{0,2},{1,3},{2,0},{3,1},{4,6},{5,7},{6,4},{7,5},{8,10},{9,11},{10,... | collective-permute-start | bytes 1572872 | tf_op jit(solution)/shard_map/ppermute | solution.py:567
  273.2 10.3 %collective-permute-start.4 = (f32[2,136,128]{2,1,0:T(8,128)}, f32[2,136,128]{2,1,0:T(8,128)}, u32[]{:S(2)}, u32[]{:S(2)}) collective-permute-start(f32[2,136,128]{2,1,0:T(8,128)} %pad_maximum_fusion.1), channel_id=1, source_target_pairs={{0,24},{8,0},{16,8},{24,16},{1,25},{9,1},{17,9},{25,17},{2,26},{10... | collective-permute-start | bytes 417800 | tf_op jit(solution)/shard_map/ppermute | solution.py:326
  273.5 13.7 %collective-permute-start.5 = (f32[2,136,128]{2,1,0:T(8,128)}, f32[2,136,128]{2,1,0:T(8,128)}, u32[]{:S(2)}, u32[]{:S(2)}) collective-permute-start(f32[2,136,128]{2,1,0:T(8,128)} %pad_maximum_fusion.1), channel_id=1, source_target_pairs={{0,16},{8,24},{16,0},{24,8},{1,17},{9,25},{17,1},{25,9},{2,18},{10... | collective-permute-start | bytes 417800 | tf_op jit(solution)/shard_map/ppermute | solution.py:326
  283.6 5.4 %collective-permute-start.6 = (f32[2,136,128]{2,1,0:T(8,128)}, f32[2,136,128]{2,1,0:T(8,128)}, u32[]{:S(2)}, u32[]{:S(2)}) collective-permute-start(f32[2,136,128]{2,1,0:T(8,128)} %pad_maximum_fusion.1), channel_id=1, source_target_pairs={{0,8},{8,16},{16,24},{24,0},{1,9},{9,17},{17,25},{25,1},{2,10},{10... | collective-permute-start | bytes 417800 | tf_op jit(solution)/shard_map/ppermute | solution.py:326
  289.0 7.5 %copy-start.12 = (bf16[512,512]{1,0:T(8,128)(2,1)}, bf16[512,512]{1,0:T(8,128)(2,1)S(1)}, u32[]{:S(2)}) copy-start(bf16[512,512]{1,0:T(8,128)(2,1)S(1)} %collective-permute-done.16.h_near) | copy-start | bytes 1572868
  303.3 1.0 copy-start.4
  303.3 9.1 %copy-start.17 = (f32[2,1,128]{2,1,0:T(1,128)S(1)}, f32[2,1,128]{2,1,0:T(1,128)}, u32[]{:S(2)}) copy-start(f32[2,1,128]{2,1,0:T(1,128)} %copy-done.16) | copy-start | bytes 3076
  303.3 9.1 %copy-start.18 = (f32[2,1,128]{2,1,0:T(1,128)S(1)}, f32[2,1,128]{2,1,0:T(1,128)}, u32[]{:S(2)}) copy-start(f32[2,1,128]{2,1,0:T(1,128)} %get-tuple-element.56) | copy-start | bytes 3076
  303.4 14.8 %copy-start.15 = (bf16[2,32,128]{2,1,0:T(8,128)(2,1)S(1)}, bf16[2,32,128]{2,1,0:T(8,128)(2,1)}, u32[]{:S(2)}) copy-start(bf16[2,32,128]{2,1,0:T(8,128)(2,1)} %get-tuple-element.51) | copy-start | bytes 49156
  304.3 47.1 %all-to-all-start.5 = ((bf16[32,8,4096]{2,1,0:T(8,128)(2,1)}), bf16[32,8,4096]{2,1,0:T(8,128)(2,1)S(1)}, u32[]{:S(2)}, u32[]{:S(2)}) async-start(bf16[32,8,4096]{2,1,0:T(8,128)(2,1)} %bitcast.42), calls=%async_computation.5 | async-start | bytes 4194304 | tf_op jit(solution)/shard_map/all_to_all | solution.py:573
  313.7 26.7 %collective-permute-start.13 = (f32[2,136,128]{2,1,0:T(8,128)S(1)}, f32[2,136,128]{2,1,0:T(8,128)S(1)}, u32[]{:S(2)}, u32[]{:S(2)}) collective-permute-start(f32[2,136,128]{2,1,0:T(8,128)S(1)} %pad_maximum_fusion.2), channel_id=1, source_target_pairs={{0,96},{32,0},{64,32},{96,64},{1,97},{33,1},{65,33},{97,65},{2,98}... | collective-permute-start | bytes 417800 | tf_op jit(solution)/shard_map/ppermute | solution.py:344
  316.5 25.3 %collective-permute-start.14 = (f32[2,136,128]{2,1,0:T(8,128)S(1)}, f32[2,136,128]{2,1,0:T(8,128)S(1)}, u32[]{:S(2)}, u32[]{:S(2)}) collective-permute-start(f32[2,136,128]{2,1,0:T(8,128)S(1)} %pad_maximum_fusion.2), channel_id=1, source_target_pairs={{0,64},{32,96},{64,0},{96,32},{1,65},{33,97},{65,1},{97,33},{2,66}... | collective-permute-start | bytes 417800 | tf_op jit(solution)/shard_map/ppermute | solution.py:344
  317.3 26.7 %collective-permute-start.15 = (f32[2,136,128]{2,1,0:T(8,128)S(1)}, f32[2,136,128]{2,1,0:T(8,128)S(1)}, u32[]{:S(2)}, u32[]{:S(2)}) collective-permute-start(f32[2,136,128]{2,1,0:T(8,128)S(1)} %pad_maximum_fusion.2), channel_id=1, source_target_pairs={{0,32},{32,64},{64,96},{96,0},{1,33},{33,65},{65,97},{97,1},{2,34}... | collective-permute-start | bytes 417800 | tf_op jit(solution)/shard_map/ppermute | solution.py:344
  318.1 4.9 %collective-permute-start.20 = (bf16[2,32,128]{2,1,0:T(8,128)(2,1)S(1)}, bf16[2,32,128]{2,1,0:T(8,128)(2,1)S(1)}, u32[]{:S(2)}, u32[]{:S(2)}) collective-permute-start(bf16[2,32,128]{2,1,0:T(8,128)(2,1)S(1)} %copy-done.15), channel_id=1, source_target_pairs={{0,3},{1,2},{2,1},{3,0},{4,7},{5,6},{6,5},{7,4},{8,11},{9,10},{10,... | collective-permute-start | bytes 49160 | tf_op jit(solution)/shard_map/ppermute | solution.py:561
  345.1 1.4 collective-permute-start.19
  351.4 1.4 copy-start

commit v3 on v0

--- a/solution.py
+++ b/solution.py
@@ -62,11 +62,11 @@
     return jnp.where(here, weight[:, None, :], 0.0).reshape(experts * HALF, toks)
 
 
-def fill(routes, rows, experts):
+def fill(routes, rows, experts, parts):
     _, _, count, before = chosen(routes, experts)
-    pick = [slot_matrix(count, before, count, half) for half in range(2)]
-    both = mm(jnp.concatenate(pick, axis=0).astype(BF16), rows).astype(BF16)
-    return both[: experts * HALF], both[experts * HALF :]
+    pick = [slot_matrix(count, before, count, half) for half in range(parts)]
+    out = mm(jnp.concatenate(pick, axis=0).astype(BF16), rows).astype(BF16)
+    return [out[k * experts * HALF : (k + 1) * experts * HALF] for k in range(parts)]
 
 
 def front_kernel(src, x_ref, gain_ref, routes_ref, rows_ref, buf_ref, *, group):
@@ -77,12 +77,12 @@
     def _():
         rows_ref[...] = normed(x_ref[...], gain_ref[...]).astype(BF16)
 
-    low, high = fill(routes_ref[0] - step * group, rows_ref[...], group)
+    low, high = fill(routes_ref[0] - step * group, rows_ref[...], group, 2)
     buf_ref[:, :width] = low
     buf_ref[:, width:] = high
 
 
-def refill_kernel(src, own_ref, rows_ref, router_ref, routes_ref, logits_ref, low_ref, high_ref, *, group):
+def refill_kernel(src, own_ref, rows_ref, router_ref, routes_ref, logits_ref, low_ref, *, group):
     step = pl.program_id(0)
 
     @pl.when(step == 0)
@@ -90,7 +90,7 @@
         for k, ref in enumerate((own_ref, rows_ref)):
             logits_ref[k] = mm(router_ref[...], ref[...], ((1,), (1,))).astype(BF16)
 
-    low_ref[...], high_ref[...] = fill(routes_ref[0] - step * group, rows_ref[...], group)
+    (low_ref[...],) = fill(routes_ref[0] - step * group, rows_ref[...], group, 1)
 
 
 def front(src, x, gain, routes, experts):
@@ -140,12 +140,10 @@
             out_specs=[
                 pl.BlockSpec((2, experts, toks), lambda i, s: (0, 0, 0)),
                 pl.BlockSpec((group * HALF, width), lambda i, s: (i, 0)),
-                pl.BlockSpec((group * HALF, width), lambda i, s: (i, 0)),
             ],
         ),
         out_shape=[
             jax.ShapeDtypeStruct((2, experts, toks), BF16),
-            jax.ShapeDtypeStruct((experts * HALF, width), BF16),
             jax.ShapeDtypeStruct((experts * HALF, width), BF16),
         ],
         compiler_params=params(),
@@ -341,7 +339,7 @@
     plane = pack(link(link(before, chip), after))
     count = lax.axis_size("ep_0")
     planes = [
-        lax.ppermute(plane, "ep_0", [(i, i + d) for i in range(count - d)])
+        lax.ppermute(plane, "ep_0", [(i, (i + d) % count) for i in range(count)])
         for d in range(count - 1, 0, -1)
     ]
     return before, planes
@@ -349,9 +347,11 @@
 
 def arriving_state(low, before, planes):
     is_second = lax.axis_index("ep_2") == 1
+    at = lax.axis_index("ep_0")
     total = None
-    for part in planes:
-        total = pieces(part) if total is None else link(total, pieces(part))
+    for k, part in enumerate(planes):
+        part = masked(at >= len(planes) - k, pieces(part))
+        total = part if total is None else link(total, part)
     state = link(total, before)[1]
     swapped = both_cores(state)
     entering = jnp.concatenate(
@@ -436,7 +436,7 @@
             num_scalar_prefetch=1,
             grid=(4,),
             in_specs=[pl.BlockSpec((both, width), whole)] * 4 + [pl.BlockSpec(down.shape, whole)],
-            out_specs=pl.BlockSpec((both // 2, cols), lambda k, s: (0, s[k])),
+            out_specs=pl.BlockSpec((both // 2, cols), lambda k, s: (0, k)),
         ),
         out_shape=jax.ShapeDtypeStruct((both // 2, 4 * cols), BF16),
         compiler_params=params(),
@@ -488,7 +488,7 @@
     slots = low.shape[0]
     cols = low.shape[1] // 4
     toks = place.shape[1] // 2
-    res = pl.BlockSpec((slots, cols), lambda k, s: (0, s[k]))
+    res = pl.BlockSpec((slots, cols), lambda k, s: (0, k))
     return pl.pallas_call(
         combine_kernel,
         grid_spec=pltpu.PrefetchScalarGridSpec(
@@ -509,6 +509,7 @@
 
 NEAR = [(i, i ^ 1) for i in range(4)]
 FAR = [(i, 3 - i) for i in range(4)]
+OPPOSITE = [(i, i ^ 2) for i in range(4)]
 
 
 def to_near(a):
@@ -519,10 +520,10 @@
     return lax.ppermute(a, "tp", FAR)
 
 
-def shared(a):
+def shared(a, direct=True):
     far = to_far(a)
     near = to_near(a)
-    return a, near, far, to_near(far)
+    return a, near, far, (lax.ppermute(a, "tp", OPPOSITE) if direct else to_near(far))
 
 
 def swap(a):
@@ -556,18 +557,19 @@
     by_block = routes.reshape(4, toks, 2).transpose(0, 2, 1)
     router = router_weight.T
 
-    rows_a = normed(mix_input, norm_mix).astype(BF16)
-    group_a = shared(rows_a)
+    width = moe_input.shape[1]
+    gate_far = to_far(expert_gate[0])
     rows_b, own = front(src, moe_input, norm_moe.reshape(1, -1), by_block, router_weight.shape[1])
     own_rows = swap(own)
     rows_near = to_near(rows_b)
-    gate_far = to_far(expert_gate[0])
+    mix_input, _ = lax.optimization_barrier((mix_input, rows_b))
+    rows_a = normed(mix_input, norm_mix).astype(BF16)
+    group_a = shared(rows_a, direct=False)
     up_far = to_far(expert_up[0])
-    logits, low, high = refill(src, rows_b, rows_near, router, by_block)
+    logits, low = refill(src, rows_b, rows_near, router, by_block)
     low, own_rows = lax.optimization_barrier((low, own_rows))
     low_rows = swap(low)
-    high, low_rows = lax.optimization_barrier((high, low_rows))
-    high_rows = swap(high)
+    high_rows = to_near(own_rows[:, width:])
     logits = jnp.concatenate([logits, to_far(logits)])
     place = places(src, by_block, logits)
 
@@ -580,15 +582,16 @@
     weights = (expert_gate[0], expert_up[0], gate_far, up_far)
     h_low = hidden_units(own_rows, low_rows, 0, weights)
     h_low = shared(h_low)
-    high_rows, far = lax.optimization_barrier((high_rows, h_low[2]))
+    high_rows, low_own = lax.optimization_barrier((high_rows, h_low[0]))
     h_high = hidden_units(own_rows, high_rows, 1, weights)
     h_high = shared(h_high)
     opp, high_own = lax.optimization_barrier((h_low[3], h_high[0]))
-    down_low = down_rows(src, h_low[:2] + (far, opp), expert_down[0])
+    down_low = down_rows(src, (low_own,) + h_low[1:3] + (opp,), expert_down[0])
     back_low = swap(down_low)
     came, _ = lax.optimization_barrier((came, down_low))
     before, planes = along_planes(chip, came)
     down_high = down_rows(src, (high_own,) + h_high[1:], expert_down[0])
+    down_high, back_low = lax.optimization_barrier((down_high, back_low))
     back_high = swap(down_high)
     planes, _ = lax.optimization_barrier((planes, down_high))
 

time: 347 us -> 340 us (0.980)
  starting transfers between devices: 69.5 us -> 60.7 us
  local copies, waits for them, and re-layouts: 5.32 us -> 9.55 us
    ppermute x6, waiting for transfers between devices: 94 us -> 2.51 us  [to_far(): return lax.ppermute(a, 'tp', FAR)]
    ppermute x7 -> x6, waiting for transfers between devices: 52.4 us -> 117 us  [to_near(): return lax.ppermute(a, 'tp', NEAR)]
    ppermute x3, waiting for transfers between devices: 10.3 us -> 24.5 us  [along_rows(): lax.ppermute(sent, 'ep_1', [(i, (i + d) % count) for i in range(count)])]
    ppermute x3 -> x5, waiting for transfers between devices: 8.8 us -> 19.7 us  [the longest x3 16.1 us: along_planes(): lax.ppermute(plane, 'ep_0', [(i, (i + d) % count) for i in range(count)])]
    all_to_all x5 -> x4, starting transfers between devices: 37.6 us -> 31.3 us  [swap(): lax.all_to_all(a.reshape(experts, rows // experts, cols), EP, split_axis=...]
    ppermute x6, starting transfers between devices: 14.3 us -> 10.3 us  [to_far(): return lax.ppermute(a, 'tp', FAR)]
    ppermute x7 -> x6, starting transfers between devices: 3.96 us -> 7.11 us  [to_near(): return lax.ppermute(a, 'tp', NEAR)]
    all_to_all x5 -> x4, waiting for transfers between devices: 19.2 us -> 20 us  [swap(): lax.all_to_all(a.reshape(experts, rows // experts, cols), EP, split_axis=...]
  transfers between devices with their start and end apart: 26 -> 26, of which waited for: 16 -> 15; matrix products, arithmetic and copies ran while one was open for 2% -> 3% of each run, Pallas kernels for 16% -> 16%
where the time goes in v3:
time: 340 us; the launch traced here: 338 us
  waiting for transfers between devices  186 us (55%)
  Pallas kernels  73.5 us (22%)
  starting transfers between devices  60.7 us (18%)
  local copies, waits for them, and re-layouts  9.55 us (3%)
  other arithmetic  6.96 us (2%)
    ppermute x6, waiting for transfers between devices, to_near(): return lax.ppermute(a, 'tp', NEAR)  117 us
    all_to_all x4, starting transfers between devices, swap(): lax.all_to_all(a.reshape(experts, rows // experts, cols), EP, split_axis=...  31.3 us
    ppermute x3, waiting for transfers between devices, along_rows(): lax.ppermute(sent, 'ep_1', [(i, (i + d) % count) for i in range(count)])  24.5 us
    all_to_all x4, waiting for transfers between devices, swap(): lax.all_to_all(a.reshape(experts, rows // experts, cols), EP, split_axis=...  20 us
    pallas_call x2, Pallas kernels, hidden_units(): pl.pallas_call(hidden_kernel, grid=(width // kb,), in_specs=[pl.BlockSpec...  17.7 us
    pallas_call x1, Pallas kernels, mixer(): pl.pallas_call(mixer_kernel, grid_spec=pltpu.PrefetchScalarGridSpec(num_s...  17.6 us
    ppermute x3, waiting for transfers between devices, along_planes(): lax.ppermute(plane, 'ep_0', [(i, (i + d) % count) for i in range(count)])  16.1 us
    pallas_call x2, Pallas kernels, down_rows(): pl.pallas_call(down_kernel, grid_spec=pltpu.PrefetchScalarGridSpec(num_sc...  13.6 us
  transfers between devices with their start and end apart: 26, of which 15 were waited for; matrix products, arithmetic and copies ran while one was open for 3% of the time, Pallas kernels for 16%

profile of v3, /device:TPU:8, one launch (start us, length us, event | category | flops | bytes accessed | tf_op | source)
XLA Modules:
  0.0 337.6 jit_solution(15311928961867767741)
XLA Ops:
  1.2 5.7 %front.1 = (bf16[128,4096]{1,0:T(8,128)(2,1)}, bf16[256,8192]{1,0:T(8,128)(2,1)}) custom-call(s32[4]{0:T(128)} %pad_add_fusion.src, bf16[128,4096]{1,0:T(8,128)(2,1)} %x_ref.1, f32[1,4096]{1,0:T(1,128)} %bitcast.47, s32[4,2,128]{2,1,0:T(2,128)} %bitcast.44), custom_call_target="tpu_custom_call" | custom-call | tf_op jit(solution)/shard_map/front/pallas_call | solution.py:100
  6.9 8.8 %all-to-all-start = ((bf16[32,8,8192]{2,1,0:T(8,128)(2,1)}), bf16[32,8,8192]{2,1,0:T(8,128)(2,1)}, u32[]{:S(2)}, u32[]{:S(2)}) async-start(bf16[32,8,8192]{2,1,0:T(8,128)(2,1)} %bitcast.41), calls=%async_computation | async-start | bytes 8388608 | tf_op jit(solution)/shard_map/all_to_all | solution.py:532
  15.7 1.6 collective-permute-start.7
  17.9 2.2 collective-permute-start.1
  20.1 1.1 collective-permute-start.10
  21.2 2.1 collective-permute-start.9
  23.3 17.6 %collective-permute-done.7.rows_ref = bf16[128,4096]{1,0:T(8,128)(2,1)S(1)} collective-permute-done((bf16[128,4096]{1,0:T(8,128)(2,1)S(1)}, bf16[128,4096]{1,0:T(8,128)(2,1)S(1)}, u32[]{:S(2)}, u32[]{:S(2)}) %collective-permute-start.7) | collective-permute-done | bytes 1048608 | tf_op jit(solution)/shard_map/ppermute | solution.py:516
  40.9 1.0 copy-done.6
  41.9 5.2 %refill.1 = (bf16[2,32,128]{2,1,0:T(8,128)(2,1)}, bf16[256,4096]{1,0:T(8,128)(2,1)}) custom-call(s32[4]{0:T(128)} %pad_add_fusion.src, bf16[128,4096]{1,0:T(8,128)(2,1)} %get-tuple-element.25.own_ref, bf16[128,4096]{1,0:T(8,128)(2,1)} %copy-done.6, bf16[32,4096]{1,0:T(8,128)(2,1)} %bitcast.43, s32[4,2,128]{2,1,0:T(2,128)} %bitcast.45), custom_call_target="tpu_custom_call" | custom-call | tf_op jit(solution)/shard_map/refill/pallas_call | solution.py:129
  47.1 20.0 %all-to-all-done = bf16[32,8,8192]{2,1,0:T(8,128)(2,1)} async-done(((bf16[32,8,8192]{2,1,0:T(8,128)(2,1)}), bf16[32,8,8192]{2,1,0:T(8,128)(2,1)}, u32[]{:S(2)}, u32[]{:S(2)}) %all-to-all-start) | async-done | bytes 4194336 | tf_op jit(solution)/shard_map/all_to_all | solution.py:532
  67.1 6.5 %all-to-all-start.1 = ((bf16[32,8,4096]{2,1,0:T(8,128)(2,1)}), bf16[32,8,4096]{2,1,0:T(8,128)(2,1)S(1)}, u32[]{:S(2)}, u32[]{:S(2)}) async-start(bf16[32,8,4096]{2,1,0:T(8,128)(2,1)} %bitcast.42), calls=%async_computation.1 | async-start | bytes 4194304 | tf_op jit(solution)/shard_map/all_to_all | solution.py:532
  73.6 3.2 slice.65
  76.8 1.5 collective-permute-start.8
  78.9 1.5 collective-permute-start.2
  80.4 67.7 %collective-permute-done.a1 = bf16[128,4096]{1,0:T(8,128)(2,1)S(1)} collective-permute-done((bf16[128,4096]{1,0:T(8,128)(2,1)S(1)}, bf16[128,4096]{1,0:T(8,128)(2,1)S(1)}, u32[]{:S(2)}, u32[]{:S(2)}) %collective-permute-start) | collective-permute-done | bytes 1048608 | tf_op jit(solution)/shard_map/ppermute | solution.py:516
  148.0 21.6 %collective-permute-done.2.a3 = bf16[128,4096]{1,0:T(8,128)(2,1)S(1)} collective-permute-done((bf16[128,4096]{1,0:T(8,128)(2,1)}, bf16[128,4096]{1,0:T(8,128)(2,1)S(1)}, u32[]{:S(2)}, u32[]{:S(2)}) %collective-permute-start.2) | collective-permute-done | bytes 1048608 | tf_op jit(solution)/shard_map/ppermute | solution.py:516
  169.6 1.0 copy-done.8
  170.6 17.6 %mixer.1 = (f32[512,512]{1,0:T(8,128)}, f32[512,512]{1,0:T(8,128)}, f32[4,136,128]{2,1,0:T(8,128)}) custom-call(s32[4]{0:T(128)} %pad_add_fusion.src, bf16[128,4096]{1,0:T(8,128)(2,1)} %copy-done.3, bf16[128,4096]{1,0:T(8,128)(2,1)} %copy-done.7, bf16[128,4096]{1,0:T(8,128)(2,1)} %collective-permute-done.1.a2, bf16[128,4096]{1,0:T(8,128)(2,1)} %copy-done.8, ...), custom_call_target="tpu_custom_call" | custom-call | tf_op jit(solution)/shard_map/mixer/pallas_call | solution.py:235
  188.2 1.3 copy-done.1
  189.5 8.8 %hidden.2.h_own = bf16[512,512]{1,0:T(8,128)(2,1)} custom-call(bf16[256,8192]{1,0:T(8,128)(2,1)} %bitcast.14.own_ref, bf16[256,4096]{1,0:T(8,128)(2,1)} %bitcast.40, bf16[4096,256]{1,0:T(8,128)(2,1)} %bitcast.17.go_ref, bf16[4096,256]{1,0:T(8,128)(2,1)} %bitcast.18.uo_ref, bf16[4096,256]{1,0:T(8,128)(2,1)} %collective-permute-done.9.gf_ref, ...), custom_call_target="tpu_custom_call" | custom-call | tf_op jit(solution)/shard_map/hidden/pallas_call | solution.py:393
  198.3 3.0 collective-permute-start.13
  202.5 8.8 %hidden.3.h_own = bf16[512,512]{1,0:T(8,128)(2,1)} custom-call(bf16[256,8192]{1,0:T(8,128)(2,1)} %bitcast.14.own_ref, bf16[256,4096]{1,0:T(8,128)(2,1)} %collective-permute-done.8.near_ref, bf16[4096,256]{1,0:T(8,128)(2,1)} %bitcast.17.go_ref, bf16[4096,256]{1,0:T(8,128)(2,1)} %bitcast.18.uo_ref, bf16[4096,256]{1,0:T(8,128)(2,1)} %collective-permute-done.9.gf_ref, ...), custom_call_target="tpu_custom_call" | custom-call | tf_op jit(solution)/shard_map/hidden/pallas_call | solution.py:393
  211.3 3.5 %collective-permute-done.13.h_opp = bf16[512,512]{1,0:T(8,128)(2,1)S(1)} collective-permute-done((bf16[512,512]{1,0:T(8,128)(2,1)}, bf16[512,512]{1,0:T(8,128)(2,1)S(1)}, u32[]{:S(2)}, u32[]{:S(2)}) %collective-permute-start.13) | collective-permute-done | bytes 524320 | tf_op jit(solution)/shard_map/ppermute | solution.py:526
  214.9 9.6 %collective-permute-done.11.h_near = bf16[512,512]{1,0:T(8,128)(2,1)S(1)} collective-permute-done((bf16[512,512]{1,0:T(8,128)(2,1)}, bf16[512,512]{1,0:T(8,128)(2,1)S(1)}, u32[]{:S(2)}, u32[]{:S(2)}) %collective-permute-start.11) | collective-permute-done | bytes 524320 | tf_op jit(solution)/shard_map/ppermute | solution.py:516
  225.5 6.8 %down.2 = bf16[256,4096]{1,0:T(8,128)(2,1)} custom-call(s32[4]{0:T(128)} %pad_add_fusion.src, bf16[512,512]{1,0:T(8,128)(2,1)} %hidden.2.h_own, bf16[512,512]{1,0:T(8,128)(2,1)} %copy-done.12, bf16[512,512]{1,0:T(8,128)(2,1)} %copy-done.13, bf16[512,512]{1,0:T(8,128)(2,1)} %copy-done.11, bf16[1024,1024]{1,0:T(8,128)(2,1)} %bitcast.35), custom_call_target="tpu_custom_call" | custom-call | tf_op jit(solution)/shard_map/down/pallas_call | solution.py:433
  232.2 7.6 %all-to-all-start.2 = ((bf16[32,8,4096]{2,1,0:T(8,128)(2,1)}), bf16[32,8,4096]{2,1,0:T(8,128)(2,1)S(1)}, u32[]{:S(2)}, u32[]{:S(2)}) async-start(bf16[32,8,4096]{2,1,0:T(8,128)(2,1)} %bitcast.39), calls=%async_computation.2 | async-start | bytes 4194304 | tf_op jit(solution)/shard_map/all_to_all | solution.py:532
  240.1 1.4 collective-permute-done.3
  242.2 1.4 collective-permute-start.17
  243.6 1.9 collective-permute-start.18
  247.2 2.7 collective-permute-start.5
  249.9 19.7 %collective-permute-done.4 = f32[2,136,128]{2,1,0:T(8,128)} collective-permute-done((f32[2,136,128]{2,1,0:T(8,128)}, f32[2,136,128]{2,1,0:T(8,128)}, u32[]{:S(2)}, u32[]{:S(2)}) %collective-permute-start.4) | collective-permute-done | bytes 139296 | tf_op jit(solution)/shard_map/ppermute | solution.py:324
  270.1 1.9 collective-permute-done.5
  271.9 3.0 collective-permute-done.6
  275.7 6.8 %down.3 = bf16[256,4096]{1,0:T(8,128)(2,1)} custom-call(s32[4]{0:T(128)} %pad_add_fusion.src, bf16[512,512]{1,0:T(8,128)(2,1)} %hidden.3.h_own, bf16[512,512]{1,0:T(8,128)(2,1)} %copy-done.10, bf16[512,512]{1,0:T(8,128)(2,1)} %collective-permute-done.18.h_far, bf16[512,512]{1,0:T(8,128)(2,1)} %collective-permute-done.19.h_opp, bf16[1024,1024]{1,0:T(8,128)(2,1)} %bitcast.36), custom_call_target="tpu_custom_call" | custom-call | tf_op jit(solution)/shard_map/down/pallas_call | solution.py:433
  282.5 1.3 copy-done
  283.9 8.5 %all-to-all-start.3 = ((bf16[32,8,4096]{2,1,0:T(8,128)(2,1)}), bf16[32,8,4096]{2,1,0:T(8,128)(2,1)}, u32[]{:S(2)}, u32[]{:S(2)}) async-start(bf16[32,8,4096]{2,1,0:T(8,128)(2,1)} %bitcast.38), calls=%async_computation.3 | async-start | bytes 4194304 | tf_op jit(solution)/shard_map/all_to_all | solution.py:532
  293.1 1.1 add_add_fusion
  294.3 2.8 collective-permute-start.14
  298.8 2.5 collective-permute-start.21
  301.2 2.5 collective-permute-done.21
  304.3 4.1 %places.1.place_ref = bf16[4,256,512]{2,1,0:T(8,128)(2,1)} custom-call(s32[4]{0:T(128)} %pad_add_fusion.src, s32[4,2,128]{2,1,0:T(2,128)} %bitcast.46, bf16[4,32,128]{2,1,0:T(8,128)(2,1)} %pad_maximum_fusion.3.logits_ref), custom_call_target="tpu_custom_call" | custom-call | tf_op jit(solution)/shard_map/places/pallas_call | solution.py:463
  308.4 12.5 %collective-permute-done.14 = f32[2,136,128]{2,1,0:T(8,128)S(1)} collective-permute-done((f32[2,136,128]{2,1,0:T(8,128)S(1)}, f32[2,136,128]{2,1,0:T(8,128)S(1)}, u32[]{:S(2)}, u32[]{:S(2)}) %collective-permute-start.14) | collective-permute-done | bytes 139296 | tf_op jit(solution)/shard_map/ppermute | solution.py:342
  320.9 1.5 collective-permute-done.15
  322.4 2.2 collective-permute-done.16
  324.6 1.1 multiply_add_fusion
  325.8 1.3 collective-permute-done.20
  327.9 4.2 %readout.1 = bf16[512,512]{1,0:T(8,128)(2,1)} custom-call(f32[512,512]{1,0:T(8,128)} %get-tuple-element.27.inside_ref, f32[512,512]{1,0:T(8,128)} %get-tuple-element.28.query_ref, f32[4,128,128]{2,1,0:T(8,128)} %fusion.3.state_ref, f32[1,512]{1,0:T(1,128)} %bitcast.63), custom_call_target="tpu_custom_call" | custom-call | tf_op jit(solution)/shard_map/readout/pallas_call | solution.py:273
  332.0 5.6 %combine.1 = bf16[512,1024]{1,0:T(8,128)(2,1)} custom-call(s32[4]{0:T(128)} %pad_add_fusion.src, bf16[256,4096]{1,0:T(8,128)(2,1)} %bitcast.37, bf16[256,4096]{1,0:T(8,128)(2,1)} %bitcast.34.high_ref, bf16[4,256,512]{2,1,0:T(8,128)(2,1)} %places.1.place_ref), custom_call_target="tpu_custom_call" | custom-call | tf_op jit(solution)/shard_map/combine/pallas_call | solution.py:492
  (74 shorter events, 11.7 us)
Async XLA Ops:
  6.9 8.8 %copy-start.5 = (bf16[128,4096]{1,0:T(8,128)(2,1)S(1)}, bf16[128,4096]{1,0:T(8,128)(2,1)}, u32[]{:S(2)}) copy-start(bf16[128,4096]{1,0:T(8,128)(2,1)} %get-tuple-element.25.own_ref) | copy-start | bytes 3145732
  6.9 10.3 %copy-start.2 = (bf16[128,4096]{1,0:T(8,128)(2,1)S(1)}, bf16[128,4096]{1,0:T(8,128)(2,1)}, u32[]{:S(2)}) copy-start(bf16[128,4096]{1,0:T(8,128)(2,1)} %param.14) | copy-start | bytes 3145732
  6.9 10.6 %copy-start.14 = (f32[4096]{0:T(1024)S(1)}, f32[4096]{0:T(1024)}, u32[]{:S(2)}) copy-start(f32[4096]{0:T(1024)} %param.16) | copy-start | bytes 49156
  6.9 60.2 %all-to-all-start = ((bf16[32,8,8192]{2,1,0:T(8,128)(2,1)}), bf16[32,8,8192]{2,1,0:T(8,128)(2,1)}, u32[]{:S(2)}, u32[]{:S(2)}) async-start(bf16[32,8,8192]{2,1,0:T(8,128)(2,1)} %bitcast.41), calls=%async_computation | async-start | bytes 8388608 | tf_op jit(solution)/shard_map/all_to_all | solution.py:532
  15.7 25.3 %collective-permute-start.7 = (bf16[128,4096]{1,0:T(8,128)(2,1)S(1)}, bf16[128,4096]{1,0:T(8,128)(2,1)S(1)}, u32[]{:S(2)}, u32[]{:S(2)}) collective-permute-start(bf16[128,4096]{1,0:T(8,128)(2,1)S(1)} %copy-done.5), channel_id=1, source_target_pairs={{0,1},{1,0},{2,3},{3,2},{4,5},{5,4},{6,7},{7,6},{8,9},{9,8},{10,11... | collective-permute-start | bytes 3145736 | tf_op jit(solution)/shard_map/ppermute | solution.py:516
  17.9 60.4 %copy-start.3 = (bf16[128,4096]{1,0:T(8,128)(2,1)}, bf16[128,4096]{1,0:T(8,128)(2,1)S(1)}, u32[]{:S(2)}) copy-start(bf16[128,4096]{1,0:T(8,128)(2,1)S(1)} %fusion.2.a0) | copy-start | bytes 3145732
  17.9 61.0 %collective-permute-start.1 = (bf16[128,4096]{1,0:T(8,128)(2,1)S(1)}, bf16[128,4096]{1,0:T(8,128)(2,1)}, u32[]{:S(2)}, u32[]{:S(2)}) collective-permute-start(bf16[128,4096]{1,0:T(8,128)(2,1)S(1)} %fusion.2.a0), channel_id=1, source_target_pairs={{0,3},{1,2},{2,1},{3,0},{4,7},{5,6},{6,5},{7,4},{8,11},{9,10},{10,... | collective-permute-start | bytes 3145736 | tf_op jit(solution)/shard_map/ppermute | solution.py:520
  20.1 168.1 %collective-permute-start.10 = (bf16[4096,256]{1,0:T(8,128)(2,1)}, bf16[4096,256]{1,0:T(8,128)(2,1)}, u32[]{:S(2)}, u32[]{:S(2)}) collective-permute-start(bf16[4096,256]{1,0:T(8,128)(2,1)} %bitcast.18.uo_ref), channel_id=1, source_target_pairs={{0,3},{1,2},{2,1},{3,0},{4,7},{5,6},{6,5},{7,4},{8,11},{9,10},{10,... | collective-permute-start | bytes 6291464 | tf_op jit(solution)/shard_map/ppermute | solution.py:520
  21.2 167.0 %collective-permute-start.9 = (bf16[4096,256]{1,0:T(8,128)(2,1)}, bf16[4096,256]{1,0:T(8,128)(2,1)}, u32[]{:S(2)}, u32[]{:S(2)}) collective-permute-start(bf16[4096,256]{1,0:T(8,128)(2,1)} %bitcast.17.go_ref), channel_id=1, source_target_pairs={{0,3},{1,2},{2,1},{3,0},{4,7},{5,6},{6,5},{7,4},{8,11},{9,10},{10,... | collective-permute-start | bytes 6291464 | tf_op jit(solution)/shard_map/ppermute | solution.py:520
  40.9 1.0 copy-start.6
  67.1 121.1 %all-to-all-start.1 = ((bf16[32,8,4096]{2,1,0:T(8,128)(2,1)}), bf16[32,8,4096]{2,1,0:T(8,128)(2,1)S(1)}, u32[]{:S(2)}, u32[]{:S(2)}) async-start(bf16[32,8,4096]{2,1,0:T(8,128)(2,1)} %bitcast.42), calls=%async_computation.1 | async-start | bytes 4194304 | tf_op jit(solution)/shard_map/all_to_all | solution.py:532
  76.8 125.7 %collective-permute-start.8 = (bf16[256,4096]{1,0:T(8,128)(2,1)}, bf16[256,4096]{1,0:T(8,128)(2,1)}, u32[]{:S(2)}, u32[]{:S(2)}) collective-permute-start(bf16[256,4096]{1,0:T(8,128)(2,1)} %slice.65), channel_id=1, source_target_pairs={{0,1},{1,0},{2,3},{3,2},{4,5},{5,4},{6,7},{7,6},{8,9},{9,8},{10,11... | collective-permute-start | bytes 6291464 | tf_op jit(solution)/shard_map/ppermute | solution.py:516
  78.3 69.7 %collective-permute-start = (bf16[128,4096]{1,0:T(8,128)(2,1)S(1)}, bf16[128,4096]{1,0:T(8,128)(2,1)S(1)}, u32[]{:S(2)}, u32[]{:S(2)}) collective-permute-start(bf16[128,4096]{1,0:T(8,128)(2,1)S(1)} %fusion.2.a0), channel_id=1, source_target_pairs={{0,1},{1,0},{2,3},{3,2},{4,5},{5,4},{6,7},{7,6},{8,9},{9,8},{10,11... | collective-permute-start | bytes 3145736 | tf_op jit(solution)/shard_map/ppermute | solution.py:516
  78.9 90.8 %collective-permute-start.2 = (bf16[128,4096]{1,0:T(8,128)(2,1)}, bf16[128,4096]{1,0:T(8,128)(2,1)S(1)}, u32[]{:S(2)}, u32[]{:S(2)}) collective-permute-start(bf16[128,4096]{1,0:T(8,128)(2,1)} %collective-permute-done.1.a2), channel_id=1, source_target_pairs={{0,1},{1,0},{2,3},{3,2},{4,5},{5,4},{6,7},{7,6},{8,9},{9,8},{10,11... | collective-permute-start | bytes 3145736 | tf_op jit(solution)/shard_map/ppermute | solution.py:516
  148.0 21.6 %copy-start.7 = (bf16[128,4096]{1,0:T(8,128)(2,1)}, bf16[128,4096]{1,0:T(8,128)(2,1)S(1)}, u32[]{:S(2)}) copy-start(bf16[128,4096]{1,0:T(8,128)(2,1)S(1)} %collective-permute-done.a1) | copy-start | bytes 3145732
  169.6 1.0 copy-start.8
  188.2 1.3 copy-start.1
  198.3 16.6 %collective-permute-start.13 = (bf16[512,512]{1,0:T(8,128)(2,1)}, bf16[512,512]{1,0:T(8,128)(2,1)S(1)}, u32[]{:S(2)}, u32[]{:S(2)}) collective-permute-start(bf16[512,512]{1,0:T(8,128)(2,1)} %hidden.2.h_own), channel_id=1, source_target_pairs={{0,2},{1,3},{2,0},{3,1},{4,6},{5,7},{6,4},{7,5},{8,10},{9,11},{10,... | collective-permute-start | bytes 1572872 | tf_op jit(solution)/shard_map/ppermute | solution.py:526
  201.3 23.2 %collective-permute-start.11 = (bf16[512,512]{1,0:T(8,128)(2,1)}, bf16[512,512]{1,0:T(8,128)(2,1)S(1)}, u32[]{:S(2)}, u32[]{:S(2)}) collective-permute-start(bf16[512,512]{1,0:T(8,128)(2,1)} %hidden.2.h_own), channel_id=1, source_target_pairs={{0,1},{1,0},{2,3},{3,2},{4,5},{5,4},{6,7},{7,6},{8,9},{9,8},{10,11... | collective-permute-start | bytes 1572872 | tf_op jit(solution)/shard_map/ppermute | solution.py:516
  201.9 22.6 %collective-permute-start.12 = (bf16[512,512]{1,0:T(8,128)(2,1)}, bf16[512,512]{1,0:T(8,128)(2,1)S(1)}, u32[]{:S(2)}, u32[]{:S(2)}) collective-permute-start(bf16[512,512]{1,0:T(8,128)(2,1)} %hidden.2.h_own), channel_id=1, source_target_pairs={{0,3},{1,2},{2,1},{3,0},{4,7},{5,6},{6,5},{7,4},{8,11},{9,10},{10,... | collective-permute-start | bytes 1572872 | tf_op jit(solution)/shard_map/ppermute | solution.py:520
  214.9 9.6 %copy-start.11 = (bf16[512,512]{1,0:T(8,128)(2,1)}, bf16[512,512]{1,0:T(8,128)(2,1)S(1)}, u32[]{:S(2)}) copy-start(bf16[512,512]{1,0:T(8,128)(2,1)S(1)} %collective-permute-done.13.h_opp) | copy-start | bytes 1572868
  224.5 0.8 copy-start.12
  224.5 1.0 copy-start.13
  232.2 7.6 %copy-start.9 = (f32[4,136,128]{2,1,0:T(8,128)S(1)}, f32[4,136,128]{2,1,0:T(8,128)}, u32[]{:S(2)}) copy-start(f32[4,136,128]{2,1,0:T(8,128)} %get-tuple-element.29) | copy-start | bytes 835588
  232.2 9.9 %copy-start.4 = (bf16[512,512]{1,0:T(8,128)(2,1)S(1)}, bf16[512,512]{1,0:T(8,128)(2,1)}, u32[]{:S(2)}) copy-start(bf16[512,512]{1,0:T(8,128)(2,1)} %hidden.3.h_own) | copy-start | bytes 1572868
  232.2 50.3 %all-to-all-start.2 = ((bf16[32,8,4096]{2,1,0:T(8,128)(2,1)}), bf16[32,8,4096]{2,1,0:T(8,128)(2,1)S(1)}, u32[]{:S(2)}, u32[]{:S(2)}) async-start(bf16[32,8,4096]{2,1,0:T(8,128)(2,1)} %bitcast.39), calls=%async_computation.2 | async-start | bytes 4194304 | tf_op jit(solution)/shard_map/all_to_all | solution.py:532
  239.9 1.6 collective-permute-start.3
  242.2 4.8 %copy-start.16 = (f32[2,1,128]{2,1,0:T(1,128)}, f32[2,1,128]{2,1,0:T(1,128)S(1)}, u32[]{:S(2)}) copy-start(f32[2,1,128]{2,1,0:T(1,128)S(1)} %get-tuple-element.53) | copy-start | bytes 3076
  242.2 32.8 %collective-permute-start.17 = (bf16[512,512]{1,0:T(8,128)(2,1)S(1)}, bf16[512,512]{1,0:T(8,128)(2,1)S(1)}, u32[]{:S(2)}, u32[]{:S(2)}) collective-permute-start(bf16[512,512]{1,0:T(8,128)(2,1)S(1)} %copy-done.4), channel_id=1, source_target_pairs={{0,1},{1,0},{2,3},{3,2},{4,5},{5,4},{6,7},{7,6},{8,9},{9,8},{10,11... | collective-permute-start | bytes 1572872 | tf_op jit(solution)/shard_map/ppermute | solution.py:516
  243.6 31.3 %collective-permute-start.18 = (bf16[512,512]{1,0:T(8,128)(2,1)S(1)}, bf16[512,512]{1,0:T(8,128)(2,1)}, u32[]{:S(2)}, u32[]{:S(2)}) collective-permute-start(bf16[512,512]{1,0:T(8,128)(2,1)S(1)} %copy-done.4), channel_id=1, source_target_pairs={{0,3},{1,2},{2,1},{3,0},{4,7},{5,6},{6,5},{7,4},{8,11},{9,10},{10,... | collective-permute-start | bytes 1572872 | tf_op jit(solution)/shard_map/ppermute | solution.py:520
  245.5 29.5 %collective-permute-start.19 = (bf16[512,512]{1,0:T(8,128)(2,1)S(1)}, bf16[512,512]{1,0:T(8,128)(2,1)}, u32[]{:S(2)}, u32[]{:S(2)}) collective-permute-start(bf16[512,512]{1,0:T(8,128)(2,1)S(1)} %copy-done.4), channel_id=1, source_target_pairs={{0,2},{1,3},{2,0},{3,1},{4,6},{5,7},{6,4},{7,5},{8,10},{9,11},{10,... | collective-permute-start | bytes 1572872 | tf_op jit(solution)/shard_map/ppermute | solution.py:526
  247.0 22.6 %collective-permute-start.4 = (f32[2,136,128]{2,1,0:T(8,128)}, f32[2,136,128]{2,1,0:T(8,128)}, u32[]{:S(2)}, u32[]{:S(2)}) collective-permute-start(f32[2,136,128]{2,1,0:T(8,128)} %pad_maximum_fusion.1), channel_id=1, source_target_pairs={{0,24},{8,0},{16,8},{24,16},{1,25},{9,1},{17,9},{25,17},{2,26},{10... | collective-permute-start | bytes 417800 | tf_op jit(solution)/shard_map/ppermute | solution.py:324
  247.2 24.8 %collective-permute-start.5 = (f32[2,136,128]{2,1,0:T(8,128)}, f32[2,136,128]{2,1,0:T(8,128)}, u32[]{:S(2)}, u32[]{:S(2)}) collective-permute-start(f32[2,136,128]{2,1,0:T(8,128)} %pad_maximum_fusion.1), channel_id=1, source_target_pairs={{0,16},{8,24},{16,0},{24,8},{1,17},{9,25},{17,1},{25,9},{2,18},{10... | collective-permute-start | bytes 417800 | tf_op jit(solution)/shard_map/ppermute | solution.py:324
  269.5 5.4 %collective-permute-start.6 = (f32[2,136,128]{2,1,0:T(8,128)}, f32[2,136,128]{2,1,0:T(8,128)}, u32[]{:S(2)}, u32[]{:S(2)}) collective-permute-start(f32[2,136,128]{2,1,0:T(8,128)} %pad_maximum_fusion.1), channel_id=1, source_target_pairs={{0,8},{8,16},{16,24},{24,0},{1,9},{9,17},{17,25},{25,1},{2,10},{10... | collective-permute-start | bytes 417800 | tf_op jit(solution)/shard_map/ppermute | solution.py:324
  274.9 0.8 copy-start.10
  282.5 1.4 copy-start
  282.5 10.6 %copy-start.17 = (f32[2,1,128]{2,1,0:T(1,128)S(1)}, f32[2,1,128]{2,1,0:T(1,128)}, u32[]{:S(2)}) copy-start(f32[2,1,128]{2,1,0:T(1,128)} %copy-done.16) | copy-start | bytes 3076
  282.5 10.6 %copy-start.18 = (f32[2,1,128]{2,1,0:T(1,128)S(1)}, f32[2,1,128]{2,1,0:T(1,128)}, u32[]{:S(2)}) copy-start(f32[2,1,128]{2,1,0:T(1,128)} %get-tuple-element.52) | copy-start | bytes 3076
  282.5 16.2 %copy-start.15 = (bf16[2,32,128]{2,1,0:T(8,128)(2,1)S(1)}, bf16[2,32,128]{2,1,0:T(8,128)(2,1)}, u32[]{:S(2)}) copy-start(bf16[2,32,128]{2,1,0:T(8,128)(2,1)} %get-tuple-element.47) | copy-start | bytes 49156
  283.9 48.2 %all-to-all-start.3 = ((bf16[32,8,4096]{2,1,0:T(8,128)(2,1)}), bf16[32,8,4096]{2,1,0:T(8,128)(2,1)}, u32[]{:S(2)}, u32[]{:S(2)}) async-start(bf16[32,8,4096]{2,1,0:T(8,128)(2,1)} %bitcast.38), calls=%async_computation.3 | async-start | bytes 4194304 | tf_op jit(solution)/shard_map/all_to_all | solution.py:532
  294.3 26.6 %collective-permute-start.14 = (f32[2,136,128]{2,1,0:T(8,128)S(1)}, f32[2,136,128]{2,1,0:T(8,128)S(1)}, u32[]{:S(2)}, u32[]{:S(2)}) collective-permute-start(f32[2,136,128]{2,1,0:T(8,128)S(1)} %pad_maximum_fusion.2), channel_id=1, source_target_pairs={{0,96},{32,0},{64,32},{96,64},{1,97},{33,1},{65,33},{97,65},{2,98}... | collective-permute-start | bytes 417800 | tf_op jit(solution)/shard_map/ppermute | solution.py:342
  297.1 25.3 %collective-permute-start.15 = (f32[2,136,128]{2,1,0:T(8,128)S(1)}, f32[2,136,128]{2,1,0:T(8,128)S(1)}, u32[]{:S(2)}, u32[]{:S(2)}) collective-permute-start(f32[2,136,128]{2,1,0:T(8,128)S(1)} %pad_maximum_fusion.2), channel_id=1, source_target_pairs={{0,64},{32,96},{64,0},{96,32},{1,65},{33,97},{65,1},{97,33},{2,66}... | collective-permute-start | bytes 417800 | tf_op jit(solution)/shard_map/ppermute | solution.py:342
  297.9 26.6 %collective-permute-start.16 = (f32[2,136,128]{2,1,0:T(8,128)S(1)}, f32[2,136,128]{2,1,0:T(8,128)S(1)}, u32[]{:S(2)}, u32[]{:S(2)}) collective-permute-start(f32[2,136,128]{2,1,0:T(8,128)S(1)} %pad_maximum_fusion.2), channel_id=1, source_target_pairs={{0,32},{32,64},{64,96},{96,0},{1,33},{33,65},{65,97},{97,1},{2,34}... | collective-permute-start | bytes 417800 | tf_op jit(solution)/shard_map/ppermute | solution.py:342
  298.8 4.9 %collective-permute-start.21 = (bf16[2,32,128]{2,1,0:T(8,128)(2,1)S(1)}, bf16[2,32,128]{2,1,0:T(8,128)(2,1)S(1)}, u32[]{:S(2)}, u32[]{:S(2)}) collective-permute-start(bf16[2,32,128]{2,1,0:T(8,128)(2,1)S(1)} %copy-done.15), channel_id=1, source_target_pairs={{0,3},{1,2},{2,1},{3,0},{4,7},{5,6},{6,5},{7,4},{8,11},{9,10},{10,... | collective-permute-start | bytes 49160 | tf_op jit(solution)/shard_map/ppermute | solution.py:520
  325.7 1.4 collective-permute-start.20

commit v4 on v0

--- a/solution.py
+++ b/solution.py
@@ -341,7 +341,7 @@
     plane = pack(link(link(before, chip), after))
     count = lax.axis_size("ep_0")
     planes = [
-        lax.ppermute(plane, "ep_0", [(i, i + d) for i in range(count - d)])
+        lax.ppermute(plane, "ep_0", [(i, (i + d) % count) for i in range(count)])
         for d in range(count - 1, 0, -1)
     ]
     return before, planes
@@ -349,9 +349,11 @@
 
 def arriving_state(low, before, planes):
     is_second = lax.axis_index("ep_2") == 1
+    at = lax.axis_index("ep_0")
     total = None
-    for part in planes:
-        total = pieces(part) if total is None else link(total, pieces(part))
+    for k, part in enumerate(planes):
+        part = masked(at >= len(planes) - k, pieces(part))
+        total = part if total is None else link(total, part)
     state = link(total, before)[1]
     swapped = both_cores(state)
     entering = jnp.concatenate(
@@ -413,17 +415,18 @@
     k = pl.program_id(0)
     n = down_ref.shape[0] // 4
     rows = out_ref.shape[0]
+    cols = down_ref.shape[1]
     unit = lambda s: down_ref[pl.ds(pl.multiple_of(s * n, n), n), :]
-    for this, (mine, other, twin) in enumerate(
-        ((h_own, h_near, 1), (h_near, h_own, 0), (h_far, h_opp, 3), (h_opp, h_far, 2))
-    ):
-
-        @pl.when(k == this)
+    for pair, refs in enumerate(((h_own, h_near), (h_far, h_opp))):
+
+        @pl.when(k == pair)
         def _():
-            s, t = src[this], src[twin]
-            total = mm(mine[:rows, :n], unit(s)) + mm(mine[:rows, n:], unit(3 - s))
-            total += mm(other[rows:, :n], unit(t)) + mm(other[rows:, n:], unit(3 - t))
-            out_ref[...] = total.astype(BF16)
+            both = []
+            for j, ref in enumerate(refs):
+                s = src[2 * pair + j]
+                both.append(mm(ref[:, :n], unit(s)) + mm(ref[:, n:], unit(3 - s)))
+            out_ref[:, :cols] = (both[0][:rows] + both[1][rows:]).astype(BF16)
+            out_ref[:, cols:] = (both[0][rows:] + both[1][:rows]).astype(BF16)
 
 
 def down_rows(src, parts, down):
@@ -434,9 +437,9 @@
         down_kernel,
         grid_spec=pltpu.PrefetchScalarGridSpec(
             num_scalar_prefetch=1,
-            grid=(4,),
+            grid=(2,),
             in_specs=[pl.BlockSpec((both, width), whole)] * 4 + [pl.BlockSpec(down.shape, whole)],
-            out_specs=pl.BlockSpec((both // 2, cols), lambda k, s: (0, s[k])),
+            out_specs=pl.BlockSpec((both // 2, 2 * cols), lambda k, s: (0, k)),
         ),
         out_shape=jax.ShapeDtypeStruct((both // 2, 4 * cols), BF16),
         compiler_params=params(),
@@ -488,7 +491,7 @@
     slots = low.shape[0]
     cols = low.shape[1] // 4
     toks = place.shape[1] // 2
-    res = pl.BlockSpec((slots, cols), lambda k, s: (0, s[k]))
+    res = pl.BlockSpec((slots, cols), lambda k, s: (0, k))
     return pl.pallas_call(
         combine_kernel,
         grid_spec=pltpu.PrefetchScalarGridSpec(
@@ -509,6 +512,7 @@
 
 NEAR = [(i, i ^ 1) for i in range(4)]
 FAR = [(i, 3 - i) for i in range(4)]
+OPPOSITE = [(i, i ^ 2) for i in range(4)]
 
 
 def to_near(a):
@@ -519,10 +523,10 @@
     return lax.ppermute(a, "tp", FAR)
 
 
-def shared(a):
+def shared(a, direct=True):
     far = to_far(a)
     near = to_near(a)
-    return a, near, far, to_near(far)
+    return a, near, far, (lax.ppermute(a, "tp", OPPOSITE) if direct else to_near(far))
 
 
 def swap(a):
@@ -557,16 +561,14 @@
     router = router_weight.T
 
     rows_a = normed(mix_input, norm_mix).astype(BF16)
-    group_a = shared(rows_a)
+    group_a = shared(rows_a, direct=False)
     rows_b, own = front(src, moe_input, norm_moe.reshape(1, -1), by_block, router_weight.shape[1])
     own_rows = swap(own)
     rows_near = to_near(rows_b)
     gate_far = to_far(expert_gate[0])
     up_far = to_far(expert_up[0])
     logits, low, high = refill(src, rows_b, rows_near, router, by_block)
-    low, own_rows = lax.optimization_barrier((low, own_rows))
     low_rows = swap(low)
-    high, low_rows = lax.optimization_barrier((high, low_rows))
     high_rows = swap(high)
     logits = jnp.concatenate([logits, to_far(logits)])
     place = places(src, by_block, logits)
@@ -580,11 +582,11 @@
     weights = (expert_gate[0], expert_up[0], gate_far, up_far)
     h_low = hidden_units(own_rows, low_rows, 0, weights)
     h_low = shared(h_low)
-    high_rows, far = lax.optimization_barrier((high_rows, h_low[2]))
+    high_rows, low_own = lax.optimization_barrier((high_rows, h_low[0]))
     h_high = hidden_units(own_rows, high_rows, 1, weights)
     h_high = shared(h_high)
     opp, high_own = lax.optimization_barrier((h_low[3], h_high[0]))
-    down_low = down_rows(src, h_low[:2] + (far, opp), expert_down[0])
+    down_low = down_rows(src, (low_own,) + h_low[1:3] + (opp,), expert_down[0])
     back_low = swap(down_low)
     came, _ = lax.optimization_barrier((came, down_low))
     before, planes = along_planes(chip, came)

time: 347 us -> 355 us (1.023)
  blocking collectives: 0 us -> 35.9 us
  waiting for transfers between devices: 186 us -> 172 us
  starting transfers between devices: 69.5 us -> 56.7 us
    ppermute x6, waiting for transfers between devices: 94 us -> 3.01 us  [to_far(): return lax.ppermute(a, 'tp', FAR)]
    all_to_all x0 -> x1, blocking collectives: none -> 35.9 us  [swap(): lax.all_to_all(a.reshape(experts, rows // experts, cols), EP, split_axis=...]
    ppermute x7 -> x5, waiting for transfers between devices: 52.4 us -> 79 us  [to_near(): return lax.ppermute(a, 'tp', NEAR)]
    all_to_all x5 -> x4, waiting for transfers between devices: 19.2 us -> 44.8 us  [swap(): lax.all_to_all(a.reshape(experts, rows // experts, cols), EP, split_axis=...]
    ppermute x3, waiting for transfers between devices: 10.3 us -> 24.5 us  [along_rows(): lax.ppermute(sent, 'ep_1', [(i, (i + d) % count) for i in range(count)])]
    ppermute x3 -> x5, waiting for transfers between devices: 8.8 us -> 18.3 us  [the longest x3 16.1 us: along_planes(): lax.ppermute(plane, 'ep_0', [(i, (i + d) % count) for i in range(count)])]
    all_to_all x5 -> x4, starting transfers between devices: 37.6 us -> 28.6 us  [swap(): lax.all_to_all(a.reshape(experts, rows // experts, cols), EP, split_axis=...]
    ppermute x6, starting transfers between devices: 14.3 us -> 9.91 us  [to_far(): return lax.ppermute(a, 'tp', FAR)]
  transfers between devices with their start and end apart: 26 -> 25, of which waited for: 16 -> 15; matrix products, arithmetic and copies ran while one was open for 2% -> 2% of each run, Pallas kernels for 16% -> 14%
where the time goes in v4:
time: 355 us; the launch traced here: 353 us
  waiting for transfers between devices  172 us (48%)
  Pallas kernels  73.9 us (21%)
  starting transfers between devices  56.7 us (16%)
  blocking collectives  35.9 us (10%)
  other arithmetic  6.98 us (2%)
  local copies, waits for them, and re-layouts  6.25 us (2%)
    ppermute x5, waiting for transfers between devices, to_near(): return lax.ppermute(a, 'tp', NEAR)  79 us
    all_to_all x4, waiting for transfers between devices, swap(): lax.all_to_all(a.reshape(experts, rows // experts, cols), EP, split_axis=...  44.8 us
    all_to_all x1, blocking collectives, swap(): lax.all_to_all(a.reshape(experts, rows // experts, cols), EP, split_axis=...  35.9 us
    all_to_all x4, starting transfers between devices, swap(): lax.all_to_all(a.reshape(experts, rows // experts, cols), EP, split_axis=...  28.6 us
    ppermute x3, waiting for transfers between devices, along_rows(): lax.ppermute(sent, 'ep_1', [(i, (i + d) % count) for i in range(count)])  24.5 us
    pallas_call x2, Pallas kernels, hidden_units(): pl.pallas_call(hidden_kernel, grid=(width // kb,), in_specs=[pl.BlockSpec...  17.7 us
    pallas_call x1, Pallas kernels, mixer(): pl.pallas_call(mixer_kernel, grid_spec=pltpu.PrefetchScalarGridSpec(num_s...  17.6 us
    ppermute x3, waiting for transfers between devices, along_planes(): lax.ppermute(plane, 'ep_0', [(i, (i + d) % count) for i in range(count)])  16.1 us
  transfers between devices with their start and end apart: 25, of which 15 were waited for; matrix products, arithmetic and copies ran while one was open for 2% of the time, Pallas kernels for 14%

profile of v4, /device:TPU:8, one launch (start us, length us, event | category | flops | bytes accessed | tf_op | source)
XLA Modules:
  0.0 352.9 jit_solution(4714318378522995800)
XLA Ops:
  1.3 5.8 %front.1 = (bf16[128,4096]{1,0:T(8,128)(2,1)}, bf16[256,8192]{1,0:T(8,128)(2,1)}) custom-call(s32[4]{0:T(128)} %pad_add_fusion.src, bf16[128,4096]{1,0:T(8,128)(2,1)} %x_ref.1, f32[1,4096]{1,0:T(1,128)} %bitcast.51, s32[4,2,128]{2,1,0:T(2,128)} %bitcast.48), custom_call_target="tpu_custom_call" | custom-call | tf_op jit(solution)/shard_map/front/pallas_call | solution.py:100
  7.0 1.5 collective-permute-start.7
  8.5 23.6 %collective-permute-done.7.rows_ref = bf16[128,4096]{1,0:T(8,128)(2,1)S(1)} collective-permute-done((bf16[128,4096]{1,0:T(8,128)(2,1)}, bf16[128,4096]{1,0:T(8,128)(2,1)S(1)}, u32[]{:S(2)}, u32[]{:S(2)}) %collective-permute-start.7) | collective-permute-done | bytes 1048608 | tf_op jit(solution)/shard_map/ppermute | solution.py:519
  32.1 1.0 copy-done.5
  33.1 6.0 %refill.1 = (bf16[2,32,128]{2,1,0:T(8,128)(2,1)}, bf16[256,4096]{1,0:T(8,128)(2,1)}, bf16[256,4096]{1,0:T(8,128)(2,1)}) custom-call(s32[4]{0:T(128)} %pad_add_fusion.src, bf16[128,4096]{1,0:T(8,128)(2,1)} %get-tuple-element.24.own_ref, bf16[128,4096]{1,0:T(8,128)(2,1)} %copy-done.5, bf16[32,4096]{1,0:T(8,128)(2,1)} %bitcast.47, s32[4,2,128]{2,1,0:T(2,128)} %bitcast.49), custom_call_target="tpu_custom_call" | custom-call | tf_op jit(solution)/shard_map/refill/pallas_call | solution.py:129
  39.1 35.9 %all_to_all.25 = bf16[32,8,4096]{2,1,0:T(8,128)(2,1)} all-to-all(bf16[32,8,4096]{2,1,0:T(8,128)(2,1)} %bitcast.46), channel_id=1, replica_groups=mesh['ep_0'=4,'ep_1'=4,'ep_2'=2,'tp'=4] {'ep_0','ep_1','ep_2'}, dimensions={0} | all-to-all | bytes 4194304 | tf_op jit(solution)/shard_map/all_to_all | solution.py:535
  75.0 6.0 %all-to-all-start.1 = ((bf16[32,8,8192]{2,1,0:T(8,128)(2,1)}), bf16[32,8,8192]{2,1,0:T(8,128)(2,1)}, u32[]{:S(2)}, u32[]{:S(2)}) async-start(bf16[32,8,8192]{2,1,0:T(8,128)(2,1)} %bitcast.44), calls=%async_computation.1 | async-start | bytes 8388608 | tf_op jit(solution)/shard_map/all_to_all | solution.py:535
  81.7 2.8 collective-permute-start.1
  85.0 2.8 collective-permute-start.9
  87.8 44.8 %all-to-all-done.1 = bf16[32,8,8192]{2,1,0:T(8,128)(2,1)} async-done(((bf16[32,8,8192]{2,1,0:T(8,128)(2,1)}), bf16[32,8,8192]{2,1,0:T(8,128)(2,1)}, u32[]{:S(2)}, u32[]{:S(2)}) %all-to-all-start.1) | async-done | bytes 4194336 | tf_op jit(solution)/shard_map/all_to_all | solution.py:535
  132.6 6.5 %all-to-all-start = ((bf16[32,8,4096]{2,1,0:T(8,128)(2,1)}), bf16[32,8,4096]{2,1,0:T(8,128)(2,1)S(1)}, u32[]{:S(2)}, u32[]{:S(2)}) async-start(bf16[32,8,4096]{2,1,0:T(8,128)(2,1)} %bitcast.45), calls=%async_computation | async-start | bytes 4194304 | tf_op jit(solution)/shard_map/all_to_all | solution.py:535
  139.1 1.6 collective-permute-start
  141.2 24.0 %collective-permute-done.a1 = bf16[128,4096]{1,0:T(8,128)(2,1)S(1)} collective-permute-done((bf16[128,4096]{1,0:T(8,128)(2,1)S(1)}, bf16[128,4096]{1,0:T(8,128)(2,1)S(1)}, u32[]{:S(2)}, u32[]{:S(2)}) %collective-permute-start) | collective-permute-done | bytes 1048608 | tf_op jit(solution)/shard_map/ppermute | solution.py:519
  165.2 21.6 %collective-permute-done.2.a3 = bf16[128,4096]{1,0:T(8,128)(2,1)S(1)} collective-permute-done((bf16[128,4096]{1,0:T(8,128)(2,1)}, bf16[128,4096]{1,0:T(8,128)(2,1)S(1)}, u32[]{:S(2)}, u32[]{:S(2)}) %collective-permute-start.2) | collective-permute-done | bytes 1048608 | tf_op jit(solution)/shard_map/ppermute | solution.py:519
  186.8 1.0 copy-done.7
  187.8 17.6 %mixer.1 = (f32[512,512]{1,0:T(8,128)}, f32[512,512]{1,0:T(8,128)}, f32[4,136,128]{2,1,0:T(8,128)}) custom-call(s32[4]{0:T(128)} %pad_add_fusion.src, bf16[128,4096]{1,0:T(8,128)(2,1)} %copy-done.3, bf16[128,4096]{1,0:T(8,128)(2,1)} %copy-done.6, bf16[128,4096]{1,0:T(8,128)(2,1)} %collective-permute-done.1.a2, bf16[128,4096]{1,0:T(8,128)(2,1)} %copy-done.7, ...), custom_call_target="tpu_custom_call" | custom-call | tf_op jit(solution)/shard_map/mixer/pallas_call | solution.py:237
  205.4 8.8 %hidden.2.h_own = bf16[512,512]{1,0:T(8,128)(2,1)} custom-call(bf16[256,8192]{1,0:T(8,128)(2,1)} %bitcast.15.own_ref, bf16[256,4096]{1,0:T(8,128)(2,1)} %bitcast.42, bf16[4096,256]{1,0:T(8,128)(2,1)} %bitcast.18.go_ref, bf16[4096,256]{1,0:T(8,128)(2,1)} %bitcast.19.uo_ref, bf16[4096,256]{1,0:T(8,128)(2,1)} %collective-permute-done.8.gf_ref, ...), custom_call_target="tpu_custom_call" | custom-call | tf_op jit(solution)/shard_map/hidden/pallas_call | solution.py:395
  214.3 3.0 collective-permute-start.12
  218.4 1.4 copy-done.1
  219.8 8.8 %hidden.3.h_own = bf16[512,512]{1,0:T(8,128)(2,1)} custom-call(bf16[256,8192]{1,0:T(8,128)(2,1)} %bitcast.15.own_ref, bf16[256,4096]{1,0:T(8,128)(2,1)} %bitcast.43, bf16[4096,256]{1,0:T(8,128)(2,1)} %bitcast.18.go_ref, bf16[4096,256]{1,0:T(8,128)(2,1)} %bitcast.19.uo_ref, bf16[4096,256]{1,0:T(8,128)(2,1)} %collective-permute-done.8.gf_ref, ...), custom_call_target="tpu_custom_call" | custom-call | tf_op jit(solution)/shard_map/hidden/pallas_call | solution.py:395
  228.6 2.2 collective-permute-done.12.h_opp
  230.8 9.7 %collective-permute-done.10.h_near = bf16[512,512]{1,0:T(8,128)(2,1)S(1)} collective-permute-done((bf16[512,512]{1,0:T(8,128)(2,1)}, bf16[512,512]{1,0:T(8,128)(2,1)S(1)}, u32[]{:S(2)}, u32[]{:S(2)}) %collective-permute-start.10) | collective-permute-done | bytes 524320 | tf_op jit(solution)/shard_map/ppermute | solution.py:519
  241.3 6.5 %down.2 = bf16[256,4096]{1,0:T(8,128)(2,1)} custom-call(s32[4]{0:T(128)} %pad_add_fusion.src, bf16[512,512]{1,0:T(8,128)(2,1)} %hidden.2.h_own, bf16[512,512]{1,0:T(8,128)(2,1)} %copy-done.11, bf16[512,512]{1,0:T(8,128)(2,1)} %collective-permute-done.11.h_far, bf16[512,512]{1,0:T(8,128)(2,1)} %copy-done.10, bf16[1024,1024]{1,0:T(8,128)(2,1)} %bitcast.37), custom_call_target="tpu_custom_call" | custom-call | tf_op jit(solution)/shard_map/down/pallas_call | solution.py:436
  247.8 7.6 %all-to-all-start.3 = ((bf16[32,8,4096]{2,1,0:T(8,128)(2,1)}), bf16[32,8,4096]{2,1,0:T(8,128)(2,1)S(1)}, u32[]{:S(2)}, u32[]{:S(2)}) async-start(bf16[32,8,4096]{2,1,0:T(8,128)(2,1)} %bitcast.41), calls=%async_computation.3 | async-start | bytes 4194304 | tf_op jit(solution)/shard_map/all_to_all | solution.py:535
  255.7 1.4 collective-permute-done.3
  257.8 1.4 collective-permute-start.16
  259.2 1.3 collective-permute-start.17
  260.5 1.3 collective-permute-start.18
  262.8 2.7 collective-permute-start.5
  265.5 19.7 %collective-permute-done.4 = f32[2,136,128]{2,1,0:T(8,128)} collective-permute-done((f32[2,136,128]{2,1,0:T(8,128)}, f32[2,136,128]{2,1,0:T(8,128)}, u32[]{:S(2)}, u32[]{:S(2)}) %collective-permute-start.4) | collective-permute-done | bytes 139296 | tf_op jit(solution)/shard_map/ppermute | solution.py:326
  285.7 1.9 collective-permute-done.5
  287.5 3.0 collective-permute-done.6
  291.3 6.5 %down.3 = bf16[256,4096]{1,0:T(8,128)(2,1)} custom-call(s32[4]{0:T(128)} %pad_add_fusion.src, bf16[512,512]{1,0:T(8,128)(2,1)} %hidden.3.h_own, bf16[512,512]{1,0:T(8,128)(2,1)} %copy-done.9, bf16[512,512]{1,0:T(8,128)(2,1)} %collective-permute-done.17.h_far, bf16[512,512]{1,0:T(8,128)(2,1)} %collective-permute-done.18.h_opp, bf16[1024,1024]{1,0:T(8,128)(2,1)} %bitcast.38), custom_call_target="tpu_custom_call" | custom-call | tf_op jit(solution)/shard_map/down/pallas_call | solution.py:436
  297.9 1.3 copy-done
  299.2 8.5 %all-to-all-start.4 = ((bf16[32,8,4096]{2,1,0:T(8,128)(2,1)}), bf16[32,8,4096]{2,1,0:T(8,128)(2,1)}, u32[]{:S(2)}, u32[]{:S(2)}) async-start(bf16[32,8,4096]{2,1,0:T(8,128)(2,1)} %bitcast.40), calls=%async_computation.4 | async-start | bytes 4194304 | tf_op jit(solution)/shard_map/all_to_all | solution.py:535
  308.4 1.1 add_add_fusion
  309.6 2.8 collective-permute-start.13
  313.2 0.9 collective-permute-start.15
  314.1 1.9 collective-permute-start.20
  316.0 3.0 collective-permute-done.20
  319.6 4.1 %places.1.place_ref = bf16[4,256,512]{2,1,0:T(8,128)(2,1)} custom-call(s32[4]{0:T(128)} %pad_add_fusion.src, s32[4,2,128]{2,1,0:T(2,128)} %bitcast.50, bf16[4,32,128]{2,1,0:T(8,128)(2,1)} %pad_maximum_fusion.3.logits_ref), custom_call_target="tpu_custom_call" | custom-call | tf_op jit(solution)/shard_map/places/pallas_call | solution.py:466
  323.7 12.5 %collective-permute-done.13 = f32[2,136,128]{2,1,0:T(8,128)S(1)} collective-permute-done((f32[2,136,128]{2,1,0:T(8,128)S(1)}, f32[2,136,128]{2,1,0:T(8,128)S(1)}, u32[]{:S(2)}, u32[]{:S(2)}) %collective-permute-start.13) | collective-permute-done | bytes 139296 | tf_op jit(solution)/shard_map/ppermute | solution.py:344
  336.2 1.5 collective-permute-done.14
  337.7 2.2 collective-permute-done.15
  339.9 1.1 multiply_add_fusion
  341.1 1.3 collective-permute-done.19
  343.2 4.2 %readout.1 = bf16[512,512]{1,0:T(8,128)(2,1)} custom-call(f32[512,512]{1,0:T(8,128)} %get-tuple-element.21.inside_ref, f32[512,512]{1,0:T(8,128)} %get-tuple-element.22.query_ref, f32[4,128,128]{2,1,0:T(8,128)} %fusion.3.state_ref, f32[1,512]{1,0:T(1,128)} %bitcast.67), custom_call_target="tpu_custom_call" | custom-call | tf_op jit(solution)/shard_map/readout/pallas_call | solution.py:275
  347.3 5.6 %combine.1 = bf16[512,1024]{1,0:T(8,128)(2,1)} custom-call(s32[4]{0:T(128)} %pad_add_fusion.src, bf16[256,4096]{1,0:T(8,128)(2,1)} %bitcast.39, bf16[256,4096]{1,0:T(8,128)(2,1)} %bitcast.35.high_ref, bf16[4,256,512]{2,1,0:T(8,128)(2,1)} %places.1.place_ref), custom_call_target="tpu_custom_call" | custom-call | tf_op jit(solution)/shard_map/combine/pallas_call | solution.py:495
  (68 shorter events, 10.4 us)
Async XLA Ops:
  7.0 25.1 %collective-permute-start.7 = (bf16[128,4096]{1,0:T(8,128)(2,1)}, bf16[128,4096]{1,0:T(8,128)(2,1)S(1)}, u32[]{:S(2)}, u32[]{:S(2)}) collective-permute-start(bf16[128,4096]{1,0:T(8,128)(2,1)} %get-tuple-element.24.own_ref), channel_id=1, source_target_pairs={{0,1},{1,0},{2,3},{3,2},{4,5},{5,4},{6,7},{7,6},{8,9},{9,8},{10,11... | collective-permute-start | bytes 3145736 | tf_op jit(solution)/shard_map/ppermute | solution.py:519
  32.1 1.0 copy-start.5
  75.0 6.0 %copy-start.2 = (bf16[128,4096]{1,0:T(8,128)(2,1)S(1)}, bf16[128,4096]{1,0:T(8,128)(2,1)}, u32[]{:S(2)}) copy-start(bf16[128,4096]{1,0:T(8,128)(2,1)} %param.14) | copy-start | bytes 3145732
  75.0 6.3 %copy-start.12 = (f32[4096]{0:T(1024)S(1)}, f32[4096]{0:T(1024)}, u32[]{:S(2)}) copy-start(f32[4096]{0:T(1024)} %param.16) | copy-start | bytes 49156
  75.0 57.6 %all-to-all-start.1 = ((bf16[32,8,8192]{2,1,0:T(8,128)(2,1)}), bf16[32,8,8192]{2,1,0:T(8,128)(2,1)}, u32[]{:S(2)}, u32[]{:S(2)}) async-start(bf16[32,8,8192]{2,1,0:T(8,128)(2,1)} %bitcast.44), calls=%async_computation.1 | async-start | bytes 8388608 | tf_op jit(solution)/shard_map/all_to_all | solution.py:535
  81.7 57.4 %copy-start.3 = (bf16[128,4096]{1,0:T(8,128)(2,1)}, bf16[128,4096]{1,0:T(8,128)(2,1)S(1)}, u32[]{:S(2)}) copy-start(bf16[128,4096]{1,0:T(8,128)(2,1)S(1)} %fusion.2.a0) | copy-start | bytes 3145732
  81.7 59.0 %collective-permute-start.1 = (bf16[128,4096]{1,0:T(8,128)(2,1)S(1)}, bf16[128,4096]{1,0:T(8,128)(2,1)}, u32[]{:S(2)}, u32[]{:S(2)}) collective-permute-start(bf16[128,4096]{1,0:T(8,128)(2,1)S(1)} %fusion.2.a0), channel_id=1, source_target_pairs={{0,3},{1,2},{2,1},{3,0},{4,7},{5,6},{6,5},{7,4},{8,11},{9,10},{10,... | collective-permute-start | bytes 3145736 | tf_op jit(solution)/shard_map/ppermute | solution.py:523
  84.5 120.9 %collective-permute-start.8 = (bf16[4096,256]{1,0:T(8,128)(2,1)}, bf16[4096,256]{1,0:T(8,128)(2,1)}, u32[]{:S(2)}, u32[]{:S(2)}) collective-permute-start(bf16[4096,256]{1,0:T(8,128)(2,1)} %bitcast.18.go_ref), channel_id=1, source_target_pairs={{0,3},{1,2},{2,1},{3,0},{4,7},{5,6},{6,5},{7,4},{8,11},{9,10},{10,... | collective-permute-start | bytes 6291464 | tf_op jit(solution)/shard_map/ppermute | solution.py:523
  85.0 120.4 %collective-permute-start.9 = (bf16[4096,256]{1,0:T(8,128)(2,1)}, bf16[4096,256]{1,0:T(8,128)(2,1)}, u32[]{:S(2)}, u32[]{:S(2)}) collective-permute-start(bf16[4096,256]{1,0:T(8,128)(2,1)} %bitcast.19.uo_ref), channel_id=1, source_target_pairs={{0,3},{1,2},{2,1},{3,0},{4,7},{5,6},{6,5},{7,4},{8,11},{9,10},{10,... | collective-permute-start | bytes 6291464 | tf_op jit(solution)/shard_map/ppermute | solution.py:523
  132.6 85.9 %all-to-all-start = ((bf16[32,8,4096]{2,1,0:T(8,128)(2,1)}), bf16[32,8,4096]{2,1,0:T(8,128)(2,1)S(1)}, u32[]{:S(2)}, u32[]{:S(2)}) async-start(bf16[32,8,4096]{2,1,0:T(8,128)(2,1)} %bitcast.45), calls=%async_computation | async-start | bytes 4194304 | tf_op jit(solution)/shard_map/all_to_all | solution.py:535
  139.1 26.1 %collective-permute-start = (bf16[128,4096]{1,0:T(8,128)(2,1)S(1)}, bf16[128,4096]{1,0:T(8,128)(2,1)S(1)}, u32[]{:S(2)}, u32[]{:S(2)}) collective-permute-start(bf16[128,4096]{1,0:T(8,128)(2,1)S(1)} %fusion.2.a0), channel_id=1, source_target_pairs={{0,1},{1,0},{2,3},{3,2},{4,5},{5,4},{6,7},{7,6},{8,9},{9,8},{10,11... | collective-permute-start | bytes 3145736 | tf_op jit(solution)/shard_map/ppermute | solution.py:519
  140.7 46.2 %collective-permute-start.2 = (bf16[128,4096]{1,0:T(8,128)(2,1)}, bf16[128,4096]{1,0:T(8,128)(2,1)S(1)}, u32[]{:S(2)}, u32[]{:S(2)}) collective-permute-start(bf16[128,4096]{1,0:T(8,128)(2,1)} %collective-permute-done.1.a2), channel_id=1, source_target_pairs={{0,1},{1,0},{2,3},{3,2},{4,5},{5,4},{6,7},{7,6},{8,9},{9,8},{10,11... | collective-permute-start | bytes 3145736 | tf_op jit(solution)/shard_map/ppermute | solution.py:519
  165.2 21.6 %copy-start.6 = (bf16[128,4096]{1,0:T(8,128)(2,1)}, bf16[128,4096]{1,0:T(8,128)(2,1)S(1)}, u32[]{:S(2)}) copy-start(bf16[128,4096]{1,0:T(8,128)(2,1)S(1)} %collective-permute-done.a1) | copy-start | bytes 3145732
  186.8 1.0 copy-start.7
  214.3 16.6 %collective-permute-start.12 = (bf16[512,512]{1,0:T(8,128)(2,1)}, bf16[512,512]{1,0:T(8,128)(2,1)S(1)}, u32[]{:S(2)}, u32[]{:S(2)}) collective-permute-start(bf16[512,512]{1,0:T(8,128)(2,1)} %hidden.2.h_own), channel_id=1, source_target_pairs={{0,2},{1,3},{2,0},{3,1},{4,6},{5,7},{6,4},{7,5},{8,10},{9,11},{10,... | collective-permute-start | bytes 1572872 | tf_op jit(solution)/shard_map/ppermute | solution.py:529
  217.3 23.3 %collective-permute-start.10 = (bf16[512,512]{1,0:T(8,128)(2,1)}, bf16[512,512]{1,0:T(8,128)(2,1)S(1)}, u32[]{:S(2)}, u32[]{:S(2)}) collective-permute-start(bf16[512,512]{1,0:T(8,128)(2,1)} %hidden.2.h_own), channel_id=1, source_target_pairs={{0,1},{1,0},{2,3},{3,2},{4,5},{5,4},{6,7},{7,6},{8,9},{9,8},{10,11... | collective-permute-start | bytes 1572872 | tf_op jit(solution)/shard_map/ppermute | solution.py:519
  217.9 22.7 %collective-permute-start.11 = (bf16[512,512]{1,0:T(8,128)(2,1)}, bf16[512,512]{1,0:T(8,128)(2,1)}, u32[]{:S(2)}, u32[]{:S(2)}) collective-permute-start(bf16[512,512]{1,0:T(8,128)(2,1)} %hidden.2.h_own), channel_id=1, source_target_pairs={{0,3},{1,2},{2,1},{3,0},{4,7},{5,6},{6,5},{7,4},{8,11},{9,10},{10,... | collective-permute-start | bytes 1572872 | tf_op jit(solution)/shard_map/ppermute | solution.py:523
  218.4 1.4 copy-start.1
  230.8 9.7 %copy-start.10 = (bf16[512,512]{1,0:T(8,128)(2,1)}, bf16[512,512]{1,0:T(8,128)(2,1)S(1)}, u32[]{:S(2)}) copy-start(bf16[512,512]{1,0:T(8,128)(2,1)S(1)} %collective-permute-done.12.h_opp) | copy-start | bytes 1572868
  240.5 0.8 copy-start.11
  247.8 7.6 %copy-start.8 = (f32[4,136,128]{2,1,0:T(8,128)S(1)}, f32[4,136,128]{2,1,0:T(8,128)}, u32[]{:S(2)}) copy-start(f32[4,136,128]{2,1,0:T(8,128)} %get-tuple-element.23) | copy-start | bytes 835588
  247.8 9.9 %copy-start.4 = (bf16[512,512]{1,0:T(8,128)(2,1)S(1)}, bf16[512,512]{1,0:T(8,128)(2,1)}, u32[]{:S(2)}) copy-start(bf16[512,512]{1,0:T(8,128)(2,1)} %hidden.3.h_own) | copy-start | bytes 1572868
  247.8 50.0 %all-to-all-start.3 = ((bf16[32,8,4096]{2,1,0:T(8,128)(2,1)}), bf16[32,8,4096]{2,1,0:T(8,128)(2,1)S(1)}, u32[]{:S(2)}, u32[]{:S(2)}) async-start(bf16[32,8,4096]{2,1,0:T(8,128)(2,1)} %bitcast.41), calls=%async_computation.3 | async-start | bytes 4194304 | tf_op jit(solution)/shard_map/all_to_all | solution.py:535
  255.5 1.6 collective-permute-start.3
  257.8 4.8 %copy-start.14 = (f32[2,1,128]{2,1,0:T(1,128)}, f32[2,1,128]{2,1,0:T(1,128)S(1)}, u32[]{:S(2)}) copy-start(f32[2,1,128]{2,1,0:T(1,128)S(1)} %get-tuple-element.45) | copy-start | bytes 3076
  257.8 32.8 %collective-permute-start.16 = (bf16[512,512]{1,0:T(8,128)(2,1)S(1)}, bf16[512,512]{1,0:T(8,128)(2,1)S(1)}, u32[]{:S(2)}, u32[]{:S(2)}) collective-permute-start(bf16[512,512]{1,0:T(8,128)(2,1)S(1)} %copy-done.4), channel_id=1, source_target_pairs={{0,1},{1,0},{2,3},{3,2},{4,5},{5,4},{6,7},{7,6},{8,9},{9,8},{10,11... | collective-permute-start | bytes 1572872 | tf_op jit(solution)/shard_map/ppermute | solution.py:519
  259.2 31.3 %collective-permute-start.17 = (bf16[512,512]{1,0:T(8,128)(2,1)S(1)}, bf16[512,512]{1,0:T(8,128)(2,1)}, u32[]{:S(2)}, u32[]{:S(2)}) collective-permute-start(bf16[512,512]{1,0:T(8,128)(2,1)S(1)} %copy-done.4), channel_id=1, source_target_pairs={{0,3},{1,2},{2,1},{3,0},{4,7},{5,6},{6,5},{7,4},{8,11},{9,10},{10,... | collective-permute-start | bytes 1572872 | tf_op jit(solution)/shard_map/ppermute | solution.py:523
  260.5 30.0 %collective-permute-start.18 = (bf16[512,512]{1,0:T(8,128)(2,1)S(1)}, bf16[512,512]{1,0:T(8,128)(2,1)}, u32[]{:S(2)}, u32[]{:S(2)}) collective-permute-start(bf16[512,512]{1,0:T(8,128)(2,1)S(1)} %copy-done.4), channel_id=1, source_target_pairs={{0,2},{1,3},{2,0},{3,1},{4,6},{5,7},{6,4},{7,5},{8,10},{9,11},{10,... | collective-permute-start | bytes 1572872 | tf_op jit(solution)/shard_map/ppermute | solution.py:529
  262.6 22.6 %collective-permute-start.4 = (f32[2,136,128]{2,1,0:T(8,128)}, f32[2,136,128]{2,1,0:T(8,128)}, u32[]{:S(2)}, u32[]{:S(2)}) collective-permute-start(f32[2,136,128]{2,1,0:T(8,128)} %pad_maximum_fusion.1), channel_id=1, source_target_pairs={{0,24},{8,0},{16,8},{24,16},{1,25},{9,1},{17,9},{25,17},{2,26},{10... | collective-permute-start | bytes 417800 | tf_op jit(solution)/shard_map/ppermute | solution.py:326
  262.8 24.8 %collective-permute-start.5 = (f32[2,136,128]{2,1,0:T(8,128)}, f32[2,136,128]{2,1,0:T(8,128)}, u32[]{:S(2)}, u32[]{:S(2)}) collective-permute-start(f32[2,136,128]{2,1,0:T(8,128)} %pad_maximum_fusion.1), channel_id=1, source_target_pairs={{0,16},{8,24},{16,0},{24,8},{1,17},{9,25},{17,1},{25,9},{2,18},{10... | collective-permute-start | bytes 417800 | tf_op jit(solution)/shard_map/ppermute | solution.py:326
  285.1 5.4 %collective-permute-start.6 = (f32[2,136,128]{2,1,0:T(8,128)}, f32[2,136,128]{2,1,0:T(8,128)}, u32[]{:S(2)}, u32[]{:S(2)}) collective-permute-start(f32[2,136,128]{2,1,0:T(8,128)} %pad_maximum_fusion.1), channel_id=1, source_target_pairs={{0,8},{8,16},{16,24},{24,0},{1,9},{9,17},{17,25},{25,1},{2,10},{10... | collective-permute-start | bytes 417800 | tf_op jit(solution)/shard_map/ppermute | solution.py:326
  290.5 0.8 copy-start.9
  297.8 1.4 copy-start
  297.8 10.6 %copy-start.15 = (f32[2,1,128]{2,1,0:T(1,128)S(1)}, f32[2,1,128]{2,1,0:T(1,128)}, u32[]{:S(2)}) copy-start(f32[2,1,128]{2,1,0:T(1,128)} %copy-done.14) | copy-start | bytes 3076
  297.8 10.6 %copy-start.16 = (f32[2,1,128]{2,1,0:T(1,128)S(1)}, f32[2,1,128]{2,1,0:T(1,128)}, u32[]{:S(2)}) copy-start(f32[2,1,128]{2,1,0:T(1,128)} %get-tuple-element.44) | copy-start | bytes 3076
  297.8 16.2 %copy-start.13 = (bf16[2,32,128]{2,1,0:T(8,128)(2,1)S(1)}, bf16[2,32,128]{2,1,0:T(8,128)(2,1)}, u32[]{:S(2)}) copy-start(bf16[2,32,128]{2,1,0:T(8,128)(2,1)} %get-tuple-element.39) | copy-start | bytes 49156
  299.2 48.2 %all-to-all-start.4 = ((bf16[32,8,4096]{2,1,0:T(8,128)(2,1)}), bf16[32,8,4096]{2,1,0:T(8,128)(2,1)}, u32[]{:S(2)}, u32[]{:S(2)}) async-start(bf16[32,8,4096]{2,1,0:T(8,128)(2,1)} %bitcast.40), calls=%async_computation.4 | async-start | bytes 4194304 | tf_op jit(solution)/shard_map/all_to_all | solution.py:535
  309.6 26.6 %collective-permute-start.13 = (f32[2,136,128]{2,1,0:T(8,128)S(1)}, f32[2,136,128]{2,1,0:T(8,128)S(1)}, u32[]{:S(2)}, u32[]{:S(2)}) collective-permute-start(f32[2,136,128]{2,1,0:T(8,128)S(1)} %pad_maximum_fusion.2), channel_id=1, source_target_pairs={{0,96},{32,0},{64,32},{96,64},{1,97},{33,1},{65,33},{97,65},{2,98}... | collective-permute-start | bytes 417800 | tf_op jit(solution)/shard_map/ppermute | solution.py:344
  312.4 25.3 %collective-permute-start.14 = (f32[2,136,128]{2,1,0:T(8,128)S(1)}, f32[2,136,128]{2,1,0:T(8,128)S(1)}, u32[]{:S(2)}, u32[]{:S(2)}) collective-permute-start(f32[2,136,128]{2,1,0:T(8,128)S(1)} %pad_maximum_fusion.2), channel_id=1, source_target_pairs={{0,64},{32,96},{64,0},{96,32},{1,65},{33,97},{65,1},{97,33},{2,66}... | collective-permute-start | bytes 417800 | tf_op jit(solution)/shard_map/ppermute | solution.py:344
  313.2 26.6 %collective-permute-start.15 = (f32[2,136,128]{2,1,0:T(8,128)S(1)}, f32[2,136,128]{2,1,0:T(8,128)S(1)}, u32[]{:S(2)}, u32[]{:S(2)}) collective-permute-start(f32[2,136,128]{2,1,0:T(8,128)S(1)} %pad_maximum_fusion.2), channel_id=1, source_target_pairs={{0,32},{32,64},{64,96},{96,0},{1,33},{33,65},{65,97},{97,1},{2,34}... | collective-permute-start | bytes 417800 | tf_op jit(solution)/shard_map/ppermute | solution.py:344
  314.1 4.9 %collective-permute-start.20 = (bf16[2,32,128]{2,1,0:T(8,128)(2,1)S(1)}, bf16[2,32,128]{2,1,0:T(8,128)(2,1)S(1)}, u32[]{:S(2)}, u32[]{:S(2)}) collective-permute-start(bf16[2,32,128]{2,1,0:T(8,128)(2,1)S(1)} %copy-done.13), channel_id=1, source_target_pairs={{0,3},{1,2},{2,1},{3,0},{4,7},{5,6},{6,5},{7,4},{8,11},{9,10},{10,... | collective-permute-start | bytes 49160 | tf_op jit(solution)/shard_map/ppermute | solution.py:523
  341.0 1.4 collective-permute-start.19

commit v5 on v4

--- a/solution.py
+++ b/solution.py
@@ -253,7 +253,7 @@
             jax.ShapeDtypeStruct((rows, cols), F32),
             jax.ShapeDtypeStruct((heads, HEAD_DIM + 8, HEAD_DIM), F32),
         ],
-        compiler_params=params(),
+        compiler_params=params(28),
         name="mixer",
     )(src, *parts, wq, wf, wv, gap)
 
@@ -283,7 +283,7 @@
         ],
         out_specs=block,
         out_shape=jax.ShapeDtypeStruct((rows, cols), BF16),
-        compiler_params=params(),
+        compiler_params=params(8),
         name="readout",
     )(inside, query, state, gain)
 
@@ -406,7 +406,7 @@
         out_specs=pl.BlockSpec((2 * count, 2 * n), lambda i: (0, 0)),
         out_shape=jax.ShapeDtypeStruct((2 * count, 2 * n), BF16),
         scratch_shapes=[pltpu.VMEM((2 * count, 2 * n), F32)] * 2,
-        compiler_params=params(),
+        compiler_params=params(14),
         name="hidden",
     )(own, near, *weights)
 
@@ -442,7 +442,7 @@
             out_specs=pl.BlockSpec((both // 2, 2 * cols), lambda k, s: (0, k)),
         ),
         out_shape=jax.ShapeDtypeStruct((both // 2, 4 * cols), BF16),
-        compiler_params=params(),
+        compiler_params=params(20),
         name="down",
     )(src, *parts, down)
 
@@ -475,7 +475,7 @@
             out_specs=pl.BlockSpec((1, 2 * toks, experts * CAP), lambda k, s: (k, 0, 0)),
         ),
         out_shape=jax.ShapeDtypeStruct((4, 2 * toks, experts * CAP), BF16),
-        compiler_params=params(),
+        compiler_params=params(8),
         name="places",
     )(src, routes, logits)
 
@@ -505,7 +505,7 @@
             out_specs=pl.BlockSpec((toks, cols), lambda k, s: (s[k], 0)),
         ),
         out_shape=jax.ShapeDtypeStruct((4 * toks, cols), BF16),
-        compiler_params=params(),
+        compiler_params=params(10),
         name="combine",
     )(src, low, high, place)
 

time: 355 us -> 355 us (level)
  Pallas kernels: 73.9 us -> 60.5 us
  local copies, waits for them, and re-layouts: 6.25 us -> 13.5 us
    unnamed x34 -> x40, local copies, waits for them, and re-layouts: 6.24 us -> 12.7 us
    pallas_call x2, Pallas kernels: 13 us -> 9.04 us  [down_rows(): pl.pallas_call(down_kernel, grid_spec=pltpu.PrefetchScalarGridSpec(num_sc...]
    pallas_call x1, Pallas kernels: 17.6 us -> 13.7 us  [mixer(): pl.pallas_call(mixer_kernel, grid_spec=pltpu.PrefetchScalarGridSpec(num_s...]
  transfers between devices with their start and end apart: 25 -> 25, of which waited for: 15 -> 15; matrix products, arithmetic and copies ran while one was open for 2% -> 3% of each run, Pallas kernels for 14% -> 11%
where the time goes in v5:
time: 355 us; the launch traced here: 352 us
  waiting for transfers between devices  174 us (49%)
  Pallas kernels  60.5 us (17%)
  starting transfers between devices  58.5 us (16%)
  blocking collectives  35.8 us (10%)
  local copies, waits for them, and re-layouts  13.5 us (4%)
  other arithmetic  8.76 us (2%)
    ppermute x5, waiting for transfers between devices, to_near(): return lax.ppermute(a, 'tp', NEAR)  79 us
    all_to_all x4, waiting for transfers between devices, swap(): lax.all_to_all(a.reshape(experts, rows // experts, cols), EP, split_axis=...  43.6 us
    all_to_all x1, blocking collectives, swap(): lax.all_to_all(a.reshape(experts, rows // experts, cols), EP, split_axis=...  35.8 us
    all_to_all x4, starting transfers between devices, swap(): lax.all_to_all(a.reshape(experts, rows // experts, cols), EP, split_axis=...  29.4 us
    ppermute x3, waiting for transfers between devices, along_rows(): lax.ppermute(sent, 'ep_1', [(i, (i + d) % count) for i in range(count)])  24.8 us
    ppermute x3, waiting for transfers between devices, along_planes(): lax.ppermute(plane, 'ep_0', [(i, (i + d) % count) for i in range(count)])  18.7 us
    pallas_call x2, Pallas kernels, hidden_units(): pl.pallas_call(hidden_kernel, grid=(width // kb,), in_specs=[pl.BlockSpec...  16.7 us
    pallas_call x1, Pallas kernels, mixer(): pl.pallas_call(mixer_kernel, grid_spec=pltpu.PrefetchScalarGridSpec(num_s...  13.7 us
  transfers between devices with their start and end apart: 25, of which 15 were waited for; matrix products, arithmetic and copies ran while one was open for 3% of the time, Pallas kernels for 11%

profile of v5, /device:TPU:8, one launch (start us, length us, event | category | flops | bytes accessed | tf_op | source)
XLA Modules:
  0.0 352.4 jit_solution(11442411758347268175)
XLA Ops:
  1.3 5.8 %front.1 = (bf16[128,4096]{1,0:T(8,128)(2,1)}, bf16[256,8192]{1,0:T(8,128)(2,1)}) custom-call(s32[4]{0:T(128)} %pad_add_fusion.src, bf16[128,4096]{1,0:T(8,128)(2,1)} %x_ref.1, f32[1,4096]{1,0:T(1,128)} %bitcast.52, s32[4,2,128]{2,1,0:T(2,128)} %bitcast.43), custom_call_target="tpu_custom_call" | custom-call | tf_op jit(solution)/shard_map/front/pallas_call | solution.py:100
  7.0 1.5 collective-permute-start.7
  8.5 23.6 %collective-permute-done.7.rows_ref = bf16[128,4096]{1,0:T(8,128)(2,1)S(1)} collective-permute-done((bf16[128,4096]{1,0:T(8,128)(2,1)}, bf16[128,4096]{1,0:T(8,128)(2,1)S(1)}, u32[]{:S(2)}, u32[]{:S(2)}) %collective-permute-start.7) | collective-permute-done | bytes 1048608 | tf_op jit(solution)/shard_map/ppermute | solution.py:519
  33.1 6.0 %refill.1 = (bf16[2,32,128]{2,1,0:T(8,128)(2,1)}, bf16[256,4096]{1,0:T(8,128)(2,1)}, bf16[256,4096]{1,0:T(8,128)(2,1)}) custom-call(s32[4]{0:T(128)} %pad_add_fusion.src, bf16[128,4096]{1,0:T(8,128)(2,1)} %get-tuple-element.24.own_ref, bf16[128,4096]{1,0:T(8,128)(2,1)} %copy-done.16, bf16[32,4096]{1,0:T(8,128)(2,1)} %bitcast.51, s32[4,2,128]{2,1,0:T(2,128)} %bitcast.44), custom_call_target="tpu_custom_call" | custom-call | tf_op jit(solution)/shard_map/refill/pallas_call | solution.py:129
  39.1 35.8 %all_to_all.25 = bf16[32,8,4096]{2,1,0:T(8,128)(2,1)S(1)} all-to-all(bf16[32,8,4096]{2,1,0:T(8,128)(2,1)} %bitcast.50), channel_id=1, replica_groups=mesh['ep_0'=4,'ep_1'=4,'ep_2'=2,'tp'=4] {'ep_0','ep_1','ep_2'}, dimensions={0} | all-to-all | bytes 4194304 | tf_op jit(solution)/shard_map/all_to_all | solution.py:535
  74.9 6.0 %all-to-all-start.1 = ((bf16[32,8,8192]{2,1,0:T(8,128)(2,1)}), bf16[32,8,8192]{2,1,0:T(8,128)(2,1)}, u32[]{:S(2)}, u32[]{:S(2)}) async-start(bf16[32,8,8192]{2,1,0:T(8,128)(2,1)} %bitcast.48), calls=%async_computation.1 | async-start | bytes 8388608 | tf_op jit(solution)/shard_map/all_to_all | solution.py:535
  81.3 1.5 fusion.2.a0
  82.8 2.8 collective-permute-start.1
  86.1 2.8 collective-permute-start.9
  88.9 43.6 %all-to-all-done.1 = bf16[32,8,8192]{2,1,0:T(8,128)(2,1)} async-done(((bf16[32,8,8192]{2,1,0:T(8,128)(2,1)}), bf16[32,8,8192]{2,1,0:T(8,128)(2,1)}, u32[]{:S(2)}, u32[]{:S(2)}) %all-to-all-start.1) | async-done | bytes 4194336 | tf_op jit(solution)/shard_map/all_to_all | solution.py:535
  132.5 7.3 %all-to-all-start = ((bf16[32,8,4096]{2,1,0:T(8,128)(2,1)}), bf16[32,8,4096]{2,1,0:T(8,128)(2,1)}, u32[]{:S(2)}, u32[]{:S(2)}) async-start(bf16[32,8,4096]{2,1,0:T(8,128)(2,1)} %bitcast.49), calls=%async_computation | async-start | bytes 4194304 | tf_op jit(solution)/shard_map/all_to_all | solution.py:535
  139.8 1.6 collective-permute-start
  141.9 24.0 %collective-permute-done.a1 = bf16[128,4096]{1,0:T(8,128)(2,1)S(1)} collective-permute-done((bf16[128,4096]{1,0:T(8,128)(2,1)S(1)}, bf16[128,4096]{1,0:T(8,128)(2,1)S(1)}, u32[]{:S(2)}, u32[]{:S(2)}) %collective-permute-start) | collective-permute-done | bytes 1048608 | tf_op jit(solution)/shard_map/ppermute | solution.py:519
  165.9 21.6 %collective-permute-done.2.a3 = bf16[128,4096]{1,0:T(8,128)(2,1)S(1)} collective-permute-done((bf16[128,4096]{1,0:T(8,128)(2,1)}, bf16[128,4096]{1,0:T(8,128)(2,1)S(1)}, u32[]{:S(2)}, u32[]{:S(2)}) %collective-permute-start.2) | collective-permute-done | bytes 1048608 | tf_op jit(solution)/shard_map/ppermute | solution.py:519
  187.5 2.2 copy-done.3
  189.7 2.2 copy-done.4
  191.9 2.2 copy-done.5
  194.1 13.7 %mixer.1 = (f32[512,512]{1,0:T(8,128)S(1)}, f32[512,512]{1,0:T(8,128)S(1)}, f32[4,136,128]{2,1,0:T(8,128)S(1)}) custom-call(s32[4]{0:T(128)S(1)} %copy-done.11, bf16[128,4096]{1,0:T(8,128)(2,1)S(1)} %fusion.2.a0, bf16[128,4096]{1,0:T(8,128)(2,1)S(1)} %collective-permute-done.a1, bf16[128,4096]{1,0:T(8,128)(2,1)} %collective-permute-done.1.a2, ...), custom_call_target="tpu_custom_call" | custom-call | tf_op jit(solution)/shard_map/mixer/pallas_call | solution.py:237
  207.9 8.4 %hidden.2.h_own = bf16[512,512]{1,0:T(8,128)(2,1)S(1)} custom-call(bf16[256,8192]{1,0:T(8,128)(2,1)} %bitcast.15.own_ref, bf16[256,4096]{1,0:T(8,128)(2,1)S(1)} %bitcast.42, bf16[4096,256]{1,0:T(8,128)(2,1)} %bitcast.18.go_ref, bf16[4096,256]{1,0:T(8,128)(2,1)} %bitcast.19.uo_ref, bf16[4096,256]{1,0:T(8,128)(2,1)} %collective-permute-done.8.gf_ref, ...), custom_call_target="tpu_custom_call" | custom-call | tf_op jit(solution)/shard_map/hidden/pallas_call | solution.py:395
  216.3 3.3 collective-permute-start.12
  220.8 8.2 %hidden.3.h_own = bf16[512,512]{1,0:T(8,128)(2,1)S(1)} custom-call(bf16[256,8192]{1,0:T(8,128)(2,1)} %bitcast.15.own_ref, bf16[256,4096]{1,0:T(8,128)(2,1)} %bitcast.13.near_ref, bf16[4096,256]{1,0:T(8,128)(2,1)} %bitcast.18.go_ref, bf16[4096,256]{1,0:T(8,128)(2,1)} %bitcast.19.uo_ref, bf16[4096,256]{1,0:T(8,128)(2,1)} %collective-permute-done.8.gf_ref, ...), custom_call_target="tpu_custom_call" | custom-call | tf_op jit(solution)/shard_map/hidden/pallas_call | solution.py:395
  229.0 4.0 %collective-permute-done.12.h_opp = bf16[512,512]{1,0:T(8,128)(2,1)} collective-permute-done((bf16[512,512]{1,0:T(8,128)(2,1)S(1)}, bf16[512,512]{1,0:T(8,128)(2,1)}, u32[]{:S(2)}, u32[]{:S(2)}) %collective-permute-start.12) | collective-permute-done | bytes 524320 | tf_op jit(solution)/shard_map/ppermute | solution.py:529
  233.0 9.7 %collective-permute-done.10.h_near = bf16[512,512]{1,0:T(8,128)(2,1)} collective-permute-done((bf16[512,512]{1,0:T(8,128)(2,1)S(1)}, bf16[512,512]{1,0:T(8,128)(2,1)}, u32[]{:S(2)}, u32[]{:S(2)}) %collective-permute-start.10) | collective-permute-done | bytes 524320 | tf_op jit(solution)/shard_map/ppermute | solution.py:519
  242.8 4.6 %down.2 = bf16[256,4096]{1,0:T(8,128)(2,1)S(1)} custom-call(s32[4]{0:T(128)S(1)} %copy-done.11, bf16[512,512]{1,0:T(8,128)(2,1)S(1)} %hidden.2.h_own, bf16[512,512]{1,0:T(8,128)(2,1)} %collective-permute-done.10.h_near, bf16[512,512]{1,0:T(8,128)(2,1)} %collective-permute-done.11.h_far, bf16[512,512]{1,0:T(8,128)(2,1)} %collective-permute-done.12.h_opp, ...), custom_call_target="tpu_custom_call" | custom-call | tf_op jit(solution)/shard_map/down/pallas_call | solution.py:436
  247.4 1.3 copy-done.2
  248.7 7.5 %all-to-all-start.3 = ((bf16[32,8,4096]{2,1,0:T(8,128)(2,1)}), bf16[32,8,4096]{2,1,0:T(8,128)(2,1)}, u32[]{:S(2)}, u32[]{:S(2)}) async-start(bf16[32,8,4096]{2,1,0:T(8,128)(2,1)} %bitcast.41), calls=%async_computation.3 | async-start | bytes 4194304 | tf_op jit(solution)/shard_map/all_to_all | solution.py:535
  256.5 1.4 collective-permute-done.3
  258.0 1.5 collective-permute-start.16
  259.5 2.0 collective-permute-start.17
  263.2 2.6 collective-permute-start.5
  265.8 20.0 %collective-permute-done.4 = f32[2,136,128]{2,1,0:T(8,128)S(1)} collective-permute-done((f32[2,136,128]{2,1,0:T(8,128)}, f32[2,136,128]{2,1,0:T(8,128)S(1)}, u32[]{:S(2)}, u32[]{:S(2)}) %collective-permute-start.4) | collective-permute-done | bytes 139296 | tf_op jit(solution)/shard_map/ppermute | solution.py:326
  286.3 2.0 collective-permute-done.5
  288.3 2.9 collective-permute-done.6
  291.2 4.4 %down.3 = bf16[256,4096]{1,0:T(8,128)(2,1)S(1)} custom-call(s32[4]{0:T(128)S(1)} %copy-done.11, bf16[512,512]{1,0:T(8,128)(2,1)S(1)} %hidden.3.h_own, bf16[512,512]{1,0:T(8,128)(2,1)S(1)} %collective-permute-done.16.h_near, bf16[512,512]{1,0:T(8,128)(2,1)} %collective-permute-done.17.h_far, bf16[512,512]{1,0:T(8,128)(2,1)} %collective-permute-done.18.h_opp, ...), custom_call_target="tpu_custom_call" | custom-call | tf_op jit(solution)/shard_map/down/pallas_call | solution.py:436
  295.6 1.3 copy-done.1
  297.0 8.5 %all-to-all-start.4 = ((bf16[32,8,4096]{2,1,0:T(8,128)(2,1)}), bf16[32,8,4096]{2,1,0:T(8,128)(2,1)S(1)}, u32[]{:S(2)}, u32[]{:S(2)}) async-start(bf16[32,8,4096]{2,1,0:T(8,128)(2,1)} %bitcast.39), calls=%async_computation.4 | async-start | bytes 4194304 | tf_op jit(solution)/shard_map/all_to_all | solution.py:535
  308.1 2.7 collective-permute-start.13
  312.5 2.6 collective-permute-start.20
  315.2 2.3 collective-permute-done.20
  317.5 1.7 places.1.place_ref
  319.2 15.1 %collective-permute-done.13 = f32[2,136,128]{2,1,0:T(8,128)} collective-permute-done((f32[2,136,128]{2,1,0:T(8,128)}, f32[2,136,128]{2,1,0:T(8,128)}, u32[]{:S(2)}, u32[]{:S(2)}) %collective-permute-start.13) | collective-permute-done | bytes 139296 | tf_op jit(solution)/shard_map/ppermute | solution.py:344
  334.3 1.4 collective-permute-done.14
  335.6 2.3 collective-permute-done.15
  338.6 1.3 multiply_add_fusion
  342.3 1.2 copy-done.7
  343.6 1.2 copy-done.9
  344.8 2.7 readout.1
  347.4 5.0 %combine.1 = bf16[512,1024]{1,0:T(8,128)(2,1)} custom-call(s32[4]{0:T(128)S(1)} %copy-done.11, bf16[256,4096]{1,0:T(8,128)(2,1)} %bitcast.33.low_ref, bf16[256,4096]{1,0:T(8,128)(2,1)S(1)} %bitcast.40, bf16[4,256,512]{2,1,0:T(8,128)(2,1)S(1)} %places.1.place_ref), custom_call_target="tpu_custom_call" | custom-call | tf_op jit(solution)/shard_map/combine/pallas_call | solution.py:495
  (74 shorter events, 13.9 us)
Async XLA Ops:
  7.0 25.1 %collective-permute-start.7 = (bf16[128,4096]{1,0:T(8,128)(2,1)}, bf16[128,4096]{1,0:T(8,128)(2,1)S(1)}, u32[]{:S(2)}, u32[]{:S(2)}) collective-permute-start(bf16[128,4096]{1,0:T(8,128)(2,1)} %get-tuple-element.24.own_ref), channel_id=1, source_target_pairs={{0,1},{1,0},{2,3},{3,2},{4,5},{5,4},{6,7},{7,6},{8,9},{9,8},{10,11... | collective-permute-start | bytes 3145736 | tf_op jit(solution)/shard_map/ppermute | solution.py:519
  32.1 1.0 copy-start.16
  74.9 6.0 %copy-start.14 = (bf16[128,4096]{1,0:T(8,128)(2,1)S(1)}, bf16[128,4096]{1,0:T(8,128)(2,1)}, u32[]{:S(2)}) copy-start(bf16[128,4096]{1,0:T(8,128)(2,1)} %param.14) | copy-start | bytes 3145732
  74.9 6.4 %copy-start.18 = (f32[4096]{0:T(1024)S(1)}, f32[4096]{0:T(1024)}, u32[]{:S(2)}) copy-start(f32[4096]{0:T(1024)} %param.16) | copy-start | bytes 49156
  74.9 57.6 %all-to-all-start.1 = ((bf16[32,8,8192]{2,1,0:T(8,128)(2,1)}), bf16[32,8,8192]{2,1,0:T(8,128)(2,1)}, u32[]{:S(2)}, u32[]{:S(2)}) async-start(bf16[32,8,8192]{2,1,0:T(8,128)(2,1)} %bitcast.48), calls=%async_computation.1 | async-start | bytes 8388608 | tf_op jit(solution)/shard_map/all_to_all | solution.py:535
  82.8 58.6 %collective-permute-start.1 = (bf16[128,4096]{1,0:T(8,128)(2,1)S(1)}, bf16[128,4096]{1,0:T(8,128)(2,1)}, u32[]{:S(2)}, u32[]{:S(2)}) collective-permute-start(bf16[128,4096]{1,0:T(8,128)(2,1)S(1)} %fusion.2.a0), channel_id=1, source_target_pairs={{0,3},{1,2},{2,1},{3,0},{4,7},{5,6},{6,5},{7,4},{8,11},{9,10},{10,... | collective-permute-start | bytes 3145736 | tf_op jit(solution)/shard_map/ppermute | solution.py:523
  85.7 122.2 %collective-permute-start.8 = (bf16[4096,256]{1,0:T(8,128)(2,1)}, bf16[4096,256]{1,0:T(8,128)(2,1)}, u32[]{:S(2)}, u32[]{:S(2)}) collective-permute-start(bf16[4096,256]{1,0:T(8,128)(2,1)} %bitcast.18.go_ref), channel_id=1, source_target_pairs={{0,3},{1,2},{2,1},{3,0},{4,7},{5,6},{6,5},{7,4},{8,11},{9,10},{10,... | collective-permute-start | bytes 6291464 | tf_op jit(solution)/shard_map/ppermute | solution.py:523
  86.1 121.7 %collective-permute-start.9 = (bf16[4096,256]{1,0:T(8,128)(2,1)}, bf16[4096,256]{1,0:T(8,128)(2,1)}, u32[]{:S(2)}, u32[]{:S(2)}) collective-permute-start(bf16[4096,256]{1,0:T(8,128)(2,1)} %bitcast.19.uo_ref), channel_id=1, source_target_pairs={{0,3},{1,2},{2,1},{3,0},{4,7},{5,6},{6,5},{7,4},{8,11},{9,10},{10,... | collective-permute-start | bytes 6291464 | tf_op jit(solution)/shard_map/ppermute | solution.py:523
  132.5 55.1 %copy-start.11 = (s32[4]{0:T(128)S(1)}, s32[4]{0:T(128)}, u32[]{:S(2)}) copy-start(s32[4]{0:T(128)} %pad_add_fusion.src) | copy-start | bytes 52
  132.5 55.1 %copy-start.13 = (f32[512]{0:T(512)S(1)}, f32[512]{0:T(512)}, u32[]{:S(2)}) copy-start(f32[512]{0:T(512)} %param.20) | copy-start | bytes 6148
  132.5 88.3 %all-to-all-start = ((bf16[32,8,4096]{2,1,0:T(8,128)(2,1)}), bf16[32,8,4096]{2,1,0:T(8,128)(2,1)}, u32[]{:S(2)}, u32[]{:S(2)}) async-start(bf16[32,8,4096]{2,1,0:T(8,128)(2,1)} %bitcast.49), calls=%async_computation | async-start | bytes 4194304 | tf_op jit(solution)/shard_map/all_to_all | solution.py:535
  139.8 26.1 %collective-permute-start = (bf16[128,4096]{1,0:T(8,128)(2,1)S(1)}, bf16[128,4096]{1,0:T(8,128)(2,1)S(1)}, u32[]{:S(2)}, u32[]{:S(2)}) collective-permute-start(bf16[128,4096]{1,0:T(8,128)(2,1)S(1)} %fusion.2.a0), channel_id=1, source_target_pairs={{0,1},{1,0},{2,3},{3,2},{4,5},{5,4},{6,7},{7,6},{8,9},{9,8},{10,11... | collective-permute-start | bytes 3145736 | tf_op jit(solution)/shard_map/ppermute | solution.py:519
  141.4 46.2 %collective-permute-start.2 = (bf16[128,4096]{1,0:T(8,128)(2,1)}, bf16[128,4096]{1,0:T(8,128)(2,1)S(1)}, u32[]{:S(2)}, u32[]{:S(2)}) collective-permute-start(bf16[128,4096]{1,0:T(8,128)(2,1)} %collective-permute-done.1.a2), channel_id=1, source_target_pairs={{0,1},{1,0},{2,3},{3,2},{4,5},{5,4},{6,7},{7,6},{8,9},{9,8},{10,11... | collective-permute-start | bytes 3145736 | tf_op jit(solution)/shard_map/ppermute | solution.py:519
  187.5 2.2 copy-start.3
  189.7 2.2 copy-start.4
  191.9 2.2 copy-start.5
  207.8 8.5 %copy-start.6 = (f32[512,512]{1,0:T(8,128)}, f32[512,512]{1,0:T(8,128)S(1)}, u32[]{:S(2)}) copy-start(f32[512,512]{1,0:T(8,128)S(1)} %get-tuple-element.21.inside_ref) | copy-start | bytes 3145732
  207.8 8.5 %copy-start.8 = (f32[512,512]{1,0:T(8,128)}, f32[512,512]{1,0:T(8,128)S(1)}, u32[]{:S(2)}) copy-start(f32[512,512]{1,0:T(8,128)S(1)} %get-tuple-element.22.query_ref) | copy-start | bytes 3145732
  216.3 16.7 %collective-permute-start.12 = (bf16[512,512]{1,0:T(8,128)(2,1)S(1)}, bf16[512,512]{1,0:T(8,128)(2,1)}, u32[]{:S(2)}, u32[]{:S(2)}) collective-permute-start(bf16[512,512]{1,0:T(8,128)(2,1)S(1)} %hidden.2.h_own), channel_id=1, source_target_pairs={{0,2},{1,3},{2,0},{3,1},{4,6},{5,7},{6,4},{7,5},{8,10},{9,11},{10,... | collective-permute-start | bytes 1572872 | tf_op jit(solution)/shard_map/ppermute | solution.py:529
  219.6 23.1 %collective-permute-start.10 = (bf16[512,512]{1,0:T(8,128)(2,1)S(1)}, bf16[512,512]{1,0:T(8,128)(2,1)}, u32[]{:S(2)}, u32[]{:S(2)}) collective-permute-start(bf16[512,512]{1,0:T(8,128)(2,1)S(1)} %hidden.2.h_own), channel_id=1, source_target_pairs={{0,1},{1,0},{2,3},{3,2},{4,5},{5,4},{6,7},{7,6},{8,9},{9,8},{10,11... | collective-permute-start | bytes 1572872 | tf_op jit(solution)/shard_map/ppermute | solution.py:519
  220.2 22.6 %collective-permute-start.11 = (bf16[512,512]{1,0:T(8,128)(2,1)S(1)}, bf16[512,512]{1,0:T(8,128)(2,1)}, u32[]{:S(2)}, u32[]{:S(2)}) collective-permute-start(bf16[512,512]{1,0:T(8,128)(2,1)S(1)} %hidden.2.h_own), channel_id=1, source_target_pairs={{0,3},{1,2},{2,1},{3,0},{4,7},{5,6},{6,5},{7,4},{8,11},{9,10},{10,... | collective-permute-start | bytes 1572872 | tf_op jit(solution)/shard_map/ppermute | solution.py:523
  220.8 22.0 %copy-start = (bf16[1,1024,1024]{2,1,0:T(8,128)(2,1)S(1)}, bf16[1,1024,1024]{2,1,0:T(8,128)(2,1)}, u32[]{:S(2)}) copy-start(bf16[1,1024,1024]{2,1,0:T(8,128)(2,1)} %param.26) | copy-start | bytes 6291460
  247.4 1.4 copy-start.2
  248.7 48.3 %all-to-all-start.3 = ((bf16[32,8,4096]{2,1,0:T(8,128)(2,1)}), bf16[32,8,4096]{2,1,0:T(8,128)(2,1)}, u32[]{:S(2)}, u32[]{:S(2)}) async-start(bf16[32,8,4096]{2,1,0:T(8,128)(2,1)} %bitcast.41), calls=%async_computation.3 | async-start | bytes 4194304 | tf_op jit(solution)/shard_map/all_to_all | solution.py:535
  256.3 1.6 collective-permute-start.3
  258.0 4.2 %copy-start.15 = (f32[4,136,128]{2,1,0:T(8,128)}, f32[4,136,128]{2,1,0:T(8,128)S(1)}, u32[]{:S(2)}) copy-start(f32[4,136,128]{2,1,0:T(8,128)S(1)} %broadcast_select_fusion) | copy-start | bytes 835588
  258.0 33.2 %collective-permute-start.16 = (bf16[512,512]{1,0:T(8,128)(2,1)S(1)}, bf16[512,512]{1,0:T(8,128)(2,1)S(1)}, u32[]{:S(2)}, u32[]{:S(2)}) collective-permute-start(bf16[512,512]{1,0:T(8,128)(2,1)S(1)} %hidden.3.h_own), channel_id=1, source_target_pairs={{0,1},{1,0},{2,3},{3,2},{4,5},{5,4},{6,7},{7,6},{8,9},{9,8},{10,11... | collective-permute-start | bytes 1572872 | tf_op jit(solution)/shard_map/ppermute | solution.py:519
  259.5 31.6 %collective-permute-start.17 = (bf16[512,512]{1,0:T(8,128)(2,1)S(1)}, bf16[512,512]{1,0:T(8,128)(2,1)}, u32[]{:S(2)}, u32[]{:S(2)}) collective-permute-start(bf16[512,512]{1,0:T(8,128)(2,1)S(1)} %hidden.3.h_own), channel_id=1, source_target_pairs={{0,3},{1,2},{2,1},{3,0},{4,7},{5,6},{6,5},{7,4},{8,11},{9,10},{10,... | collective-permute-start | bytes 1572872 | tf_op jit(solution)/shard_map/ppermute | solution.py:523
  261.5 29.6 %collective-permute-start.18 = (bf16[512,512]{1,0:T(8,128)(2,1)S(1)}, bf16[512,512]{1,0:T(8,128)(2,1)}, u32[]{:S(2)}, u32[]{:S(2)}) collective-permute-start(bf16[512,512]{1,0:T(8,128)(2,1)S(1)} %hidden.3.h_own), channel_id=1, source_target_pairs={{0,2},{1,3},{2,0},{3,1},{4,6},{5,7},{6,4},{7,5},{8,10},{9,11},{10,... | collective-permute-start | bytes 1572872 | tf_op jit(solution)/shard_map/ppermute | solution.py:529
  262.9 22.9 %collective-permute-start.4 = (f32[2,136,128]{2,1,0:T(8,128)}, f32[2,136,128]{2,1,0:T(8,128)S(1)}, u32[]{:S(2)}, u32[]{:S(2)}) collective-permute-start(f32[2,136,128]{2,1,0:T(8,128)} %pad_maximum_fusion.1), channel_id=1, source_target_pairs={{0,24},{8,0},{16,8},{24,16},{1,25},{9,1},{17,9},{25,17},{2,26},{10... | collective-permute-start | bytes 417800 | tf_op jit(solution)/shard_map/ppermute | solution.py:326
  263.2 25.1 %collective-permute-start.5 = (f32[2,136,128]{2,1,0:T(8,128)}, f32[2,136,128]{2,1,0:T(8,128)}, u32[]{:S(2)}, u32[]{:S(2)}) collective-permute-start(f32[2,136,128]{2,1,0:T(8,128)} %pad_maximum_fusion.1), channel_id=1, source_target_pairs={{0,16},{8,24},{16,0},{24,8},{1,17},{9,25},{17,1},{25,9},{2,18},{10... | collective-permute-start | bytes 417800 | tf_op jit(solution)/shard_map/ppermute | solution.py:326
  285.8 19.7 %copy-start.17 = (f32[2,136,128]{2,1,0:T(8,128)}, f32[2,136,128]{2,1,0:T(8,128)S(1)}, u32[]{:S(2)}) copy-start(f32[2,136,128]{2,1,0:T(8,128)S(1)} %collective-permute-done.4) | copy-start | bytes 417796
  285.8 5.4 %collective-permute-start.6 = (f32[2,136,128]{2,1,0:T(8,128)}, f32[2,136,128]{2,1,0:T(8,128)}, u32[]{:S(2)}, u32[]{:S(2)}) collective-permute-start(f32[2,136,128]{2,1,0:T(8,128)} %pad_maximum_fusion.1), channel_id=1, source_target_pairs={{0,8},{8,16},{16,24},{24,0},{1,9},{9,17},{17,25},{25,1},{2,10},{10... | collective-permute-start | bytes 417800 | tf_op jit(solution)/shard_map/ppermute | solution.py:326
  295.6 1.4 copy-start.1
  297.0 15.6 %copy-start.19 = (bf16[2,32,128]{2,1,0:T(8,128)(2,1)S(1)}, bf16[2,32,128]{2,1,0:T(8,128)(2,1)}, u32[]{:S(2)}) copy-start(bf16[2,32,128]{2,1,0:T(8,128)(2,1)} %get-tuple-element.39) | copy-start | bytes 49156
  297.0 20.5 %copy-start.10 = (s32[512,2]{0,1:T(2,128)S(1)}, s32[512,2]{0,1:T(2,128)}, u32[]{:S(2)}) copy-start(s32[512,2]{0,1:T(2,128)} %param.27) | copy-start | bytes 12292
  297.0 50.5 %all-to-all-start.4 = ((bf16[32,8,4096]{2,1,0:T(8,128)(2,1)}), bf16[32,8,4096]{2,1,0:T(8,128)(2,1)S(1)}, u32[]{:S(2)}, u32[]{:S(2)}) async-start(bf16[32,8,4096]{2,1,0:T(8,128)(2,1)} %bitcast.39), calls=%async_computation.4 | async-start | bytes 4194304 | tf_op jit(solution)/shard_map/all_to_all | solution.py:535
  306.3 36.0 %copy-start.12 = (f32[512]{0:T(512)S(1)}, f32[512]{0:T(512)}, u32[]{:S(2)}) copy-start(f32[512]{0:T(512)} %param.21) | copy-start | bytes 6148
  308.1 26.1 %collective-permute-start.13 = (f32[2,136,128]{2,1,0:T(8,128)}, f32[2,136,128]{2,1,0:T(8,128)}, u32[]{:S(2)}, u32[]{:S(2)}) collective-permute-start(f32[2,136,128]{2,1,0:T(8,128)} %pad_maximum_fusion.2), channel_id=1, source_target_pairs={{0,96},{32,0},{64,32},{96,64},{1,97},{33,1},{65,33},{97,65},{2,98}... | collective-permute-start | bytes 417800 | tf_op jit(solution)/shard_map/ppermute | solution.py:344
  310.9 24.8 %collective-permute-start.14 = (f32[2,136,128]{2,1,0:T(8,128)}, f32[2,136,128]{2,1,0:T(8,128)S(1)}, u32[]{:S(2)}, u32[]{:S(2)}) collective-permute-start(f32[2,136,128]{2,1,0:T(8,128)} %pad_maximum_fusion.2), channel_id=1, source_target_pairs={{0,64},{32,96},{64,0},{96,32},{1,65},{33,97},{65,1},{97,33},{2,66}... | collective-permute-start | bytes 417800 | tf_op jit(solution)/shard_map/ppermute | solution.py:344
  311.7 26.2 %collective-permute-start.15 = (f32[2,136,128]{2,1,0:T(8,128)}, f32[2,136,128]{2,1,0:T(8,128)}, u32[]{:S(2)}, u32[]{:S(2)}) collective-permute-start(f32[2,136,128]{2,1,0:T(8,128)} %pad_maximum_fusion.2), channel_id=1, source_target_pairs={{0,32},{32,64},{64,96},{96,0},{1,33},{33,65},{65,97},{97,1},{2,34}... | collective-permute-start | bytes 417800 | tf_op jit(solution)/shard_map/ppermute | solution.py:344
  312.5 4.9 %collective-permute-start.20 = (bf16[2,32,128]{2,1,0:T(8,128)(2,1)S(1)}, bf16[2,32,128]{2,1,0:T(8,128)(2,1)S(1)}, u32[]{:S(2)}, u32[]{:S(2)}) collective-permute-start(bf16[2,32,128]{2,1,0:T(8,128)(2,1)S(1)} %copy-done.19), channel_id=1, source_target_pairs={{0,3},{1,2},{2,1},{3,0},{4,7},{5,6},{6,5},{7,4},{8,11},{9,10},{10,... | collective-permute-start | bytes 49160 | tf_op jit(solution)/shard_map/ppermute | solution.py:523
  339.8 1.4 collective-permute-start.19
  342.3 1.2 copy-start.7
  343.5 1.2 copy-start.9

commit v6 on v5

--- a/solution.py
+++ b/solution.py
@@ -67,6 +67,24 @@
     pick = [slot_matrix(count, before, count, half) for half in range(2)]
     both = mm(jnp.concatenate(pick, axis=0).astype(BF16), rows).astype(BF16)
     return both[: experts * HALF], both[experts * HALF :]
+
+
+def norm_kernel(x_ref, gain_ref, out_ref):
+    out_ref[...] = normed(x_ref[...], gain_ref[...]).astype(BF16)
+
+
+def norm_rows(x, gain):
+    toks, width = x.shape
+    block = pl.BlockSpec((toks // 4, width), lambda i: (i, 0))
+    return pl.pallas_call(
+        norm_kernel,
+        grid=(4,),
+        in_specs=[block, pl.BlockSpec((1, width), lambda i: (0, 0))],
+        out_specs=block,
+        out_shape=jax.ShapeDtypeStruct((toks, width), BF16),
+        compiler_params=params(),
+        name="norm",
+    )(x, gain)
 
 
 def front_kernel(src, x_ref, gain_ref, routes_ref, rows_ref, buf_ref, *, group):
@@ -253,7 +271,7 @@
             jax.ShapeDtypeStruct((rows, cols), F32),
             jax.ShapeDtypeStruct((heads, HEAD_DIM + 8, HEAD_DIM), F32),
         ],
-        compiler_params=params(28),
+        compiler_params=params(),
         name="mixer",
     )(src, *parts, wq, wf, wv, gap)
 
@@ -406,7 +424,7 @@
         out_specs=pl.BlockSpec((2 * count, 2 * n), lambda i: (0, 0)),
         out_shape=jax.ShapeDtypeStruct((2 * count, 2 * n), BF16),
         scratch_shapes=[pltpu.VMEM((2 * count, 2 * n), F32)] * 2,
-        compiler_params=params(14),
+        compiler_params=params(),
         name="hidden",
     )(own, near, *weights)
 
@@ -560,7 +578,7 @@
     by_block = routes.reshape(4, toks, 2).transpose(0, 2, 1)
     router = router_weight.T
 
-    rows_a = normed(mix_input, norm_mix).astype(BF16)
+    rows_a = norm_rows(mix_input, norm_mix.reshape(1, -1))
     group_a = shared(rows_a, direct=False)
     rows_b, own = front(src, moe_input, norm_moe.reshape(1, -1), by_block, router_weight.shape[1])
     own_rows = swap(own)

time: 355 us -> 352 us (level)
  Pallas kernels: 60.5 us -> 68.9 us
  waiting for transfers between devices: 174 us -> 170 us
  local copies, waits for them, and re-layouts: 13.5 us -> 9.87 us
    pallas_call x1, Pallas kernels: 13.7 us -> 17.6 us  [mixer(): pl.pallas_call(mixer_kernel, grid_spec=pltpu.PrefetchScalarGridSpec(num_s...]
    pallas_call x0 -> x1, Pallas kernels: none -> 3.68 us  [norm_rows(): pl.pallas_call(norm_kernel, grid=(4,), in_specs=[block, pl.BlockSpec((1,...]
  transfers between devices with their start and end apart: 25 -> 25, of which waited for: 15 -> 15; matrix products, arithmetic and copies ran while one was open for 3% -> 2% of each run, Pallas kernels for 11% -> 14%
where the time goes in v6:
time: 352 us; the launch traced here: 349 us
  waiting for transfers between devices  170 us (48%)
  Pallas kernels  68.9 us (20%)
  starting transfers between devices  57.6 us (16%)
  blocking collectives  35.9 us (10%)
  local copies, waits for them, and re-layouts  9.87 us (3%)
  other arithmetic  6.08 us (2%)
    ppermute x5, waiting for transfers between devices, to_near(): return lax.ppermute(a, 'tp', NEAR)  79 us
    all_to_all x4, waiting for transfers between devices, swap(): lax.all_to_all(a.reshape(experts, rows // experts, cols), EP, split_axis=...  41.9 us
    all_to_all x1, blocking collectives, swap(): lax.all_to_all(a.reshape(experts, rows // experts, cols), EP, split_axis=...  35.9 us
    all_to_all x4, starting transfers between devices, swap(): lax.all_to_all(a.reshape(experts, rows // experts, cols), EP, split_axis=...  28.8 us
    ppermute x3, waiting for transfers between devices, along_rows(): lax.ppermute(sent, 'ep_1', [(i, (i + d) % count) for i in range(count)])  23.5 us
    ppermute x3, waiting for transfers between devices, along_planes(): lax.ppermute(plane, 'ep_0', [(i, (i + d) % count) for i in range(count)])  18.7 us
    pallas_call x2, Pallas kernels, hidden_units(): pl.pallas_call(hidden_kernel, grid=(width // kb,), in_specs=[pl.BlockSpec...  17.8 us
    pallas_call x1, Pallas kernels, mixer(): pl.pallas_call(mixer_kernel, grid_spec=pltpu.PrefetchScalarGridSpec(num_s...  17.6 us
  transfers between devices with their start and end apart: 25, of which 15 were waited for; matrix products, arithmetic and copies ran while one was open for 2% of the time, Pallas kernels for 14%

profile of v6, /device:TPU:8, one launch (start us, length us, event | category | flops | bytes accessed | tf_op | source)
XLA Modules:
  0.0 349.3 jit_solution(3564088421542351965)
XLA Ops:
  1.3 5.8 %front.1 = (bf16[128,4096]{1,0:T(8,128)(2,1)}, bf16[256,8192]{1,0:T(8,128)(2,1)}) custom-call(s32[4]{0:T(128)} %pad_add_fusion.src, bf16[128,4096]{1,0:T(8,128)(2,1)} %x_ref.3, f32[1,4096]{1,0:T(1,128)} %bitcast.53, s32[4,2,128]{2,1,0:T(2,128)} %bitcast.43), custom_call_target="tpu_custom_call" | custom-call | tf_op jit(solution)/shard_map/front/pallas_call | solution.py:118
  7.1 1.5 collective-permute-start.7
  8.5 23.6 %collective-permute-done.7.rows_ref = bf16[128,4096]{1,0:T(8,128)(2,1)S(1)} collective-permute-done((bf16[128,4096]{1,0:T(8,128)(2,1)}, bf16[128,4096]{1,0:T(8,128)(2,1)S(1)}, u32[]{:S(2)}, u32[]{:S(2)}) %collective-permute-start.7) | collective-permute-done | bytes 1048608 | tf_op jit(solution)/shard_map/ppermute | solution.py:537
  33.1 6.0 %refill.1 = (bf16[2,32,128]{2,1,0:T(8,128)(2,1)}, bf16[256,4096]{1,0:T(8,128)(2,1)}, bf16[256,4096]{1,0:T(8,128)(2,1)}) custom-call(s32[4]{0:T(128)} %pad_add_fusion.src, bf16[128,4096]{1,0:T(8,128)(2,1)} %get-tuple-element.24.own_ref, bf16[128,4096]{1,0:T(8,128)(2,1)} %copy-done.14, bf16[32,4096]{1,0:T(8,128)(2,1)} %bitcast.52, s32[4,2,128]{2,1,0:T(2,128)} %bitcast.44), custom_call_target="tpu_custom_call" | custom-call | tf_op jit(solution)/shard_map/refill/pallas_call | solution.py:147
  39.2 35.9 %all_to_all.25 = bf16[32,8,4096]{2,1,0:T(8,128)(2,1)} all-to-all(bf16[32,8,4096]{2,1,0:T(8,128)(2,1)} %bitcast.51), channel_id=1, replica_groups=mesh['ep_0'=4,'ep_1'=4,'ep_2'=2,'tp'=4] {'ep_0','ep_1','ep_2'}, dimensions={0} | all-to-all | bytes 4194304 | tf_op jit(solution)/shard_map/all_to_all | solution.py:553
  75.1 5.9 %all-to-all-start.1 = ((bf16[32,8,8192]{2,1,0:T(8,128)(2,1)}), bf16[32,8,8192]{2,1,0:T(8,128)(2,1)}, u32[]{:S(2)}, u32[]{:S(2)}) async-start(bf16[32,8,8192]{2,1,0:T(8,128)(2,1)} %bitcast.49), calls=%async_computation.1 | async-start | bytes 8388608 | tf_op jit(solution)/shard_map/all_to_all | solution.py:553
  81.0 3.7 %norm.1.a0 = bf16[128,4096]{1,0:T(8,128)(2,1)} custom-call(bf16[128,4096]{1,0:T(8,128)(2,1)} %x_ref.2, f32[1,4096]{1,0:T(1,128)} %bitcast.54), custom_call_target="tpu_custom_call" | custom-call | tf_op jit(solution)/shard_map/norm/pallas_call | solution.py:79
  84.7 2.8 collective-permute-start.1
  87.9 2.8 collective-permute-start.9
  90.6 41.9 %all-to-all-done.1 = bf16[32,8,8192]{2,1,0:T(8,128)(2,1)} async-done(((bf16[32,8,8192]{2,1,0:T(8,128)(2,1)}), bf16[32,8,8192]{2,1,0:T(8,128)(2,1)}, u32[]{:S(2)}, u32[]{:S(2)}) %all-to-all-start.1) | async-done | bytes 4194336 | tf_op jit(solution)/shard_map/all_to_all | solution.py:553
  132.5 6.6 %all-to-all-start = ((bf16[32,8,4096]{2,1,0:T(8,128)(2,1)}), bf16[32,8,4096]{2,1,0:T(8,128)(2,1)S(1)}, u32[]{:S(2)}, u32[]{:S(2)}) async-start(bf16[32,8,4096]{2,1,0:T(8,128)(2,1)} %bitcast.50), calls=%async_computation | async-start | bytes 4194304 | tf_op jit(solution)/shard_map/all_to_all | solution.py:553
  139.2 1.6 collective-permute-start
  141.3 24.0 %collective-permute-done.a1 = bf16[128,4096]{1,0:T(8,128)(2,1)S(1)} collective-permute-done((bf16[128,4096]{1,0:T(8,128)(2,1)S(1)}, bf16[128,4096]{1,0:T(8,128)(2,1)S(1)}, u32[]{:S(2)}, u32[]{:S(2)}) %collective-permute-start) | collective-permute-done | bytes 1048608 | tf_op jit(solution)/shard_map/ppermute | solution.py:537
  165.3 21.6 %collective-permute-done.2.a3 = bf16[128,4096]{1,0:T(8,128)(2,1)S(1)} collective-permute-done((bf16[128,4096]{1,0:T(8,128)(2,1)}, bf16[128,4096]{1,0:T(8,128)(2,1)S(1)}, u32[]{:S(2)}, u32[]{:S(2)}) %collective-permute-start.2) | collective-permute-done | bytes 1048608 | tf_op jit(solution)/shard_map/ppermute | solution.py:537
  187.9 17.6 %mixer.1 = (f32[512,512]{1,0:T(8,128)}, f32[512,512]{1,0:T(8,128)}, f32[4,136,128]{2,1,0:T(8,128)}) custom-call(s32[4]{0:T(128)} %pad_add_fusion.src, bf16[128,4096]{1,0:T(8,128)(2,1)} %norm.1.a0, bf16[128,4096]{1,0:T(8,128)(2,1)} %copy-done.15, bf16[128,4096]{1,0:T(8,128)(2,1)} %collective-permute-done.1.a2, bf16[128,4096]{1,0:T(8,128)(2,1)} %copy-done.16, ...), custom_call_target="tpu_custom_call" | custom-call | tf_op jit(solution)/shard_map/mixer/pallas_call | solution.py:255
  205.5 8.8 %hidden.2.h_own = bf16[512,512]{1,0:T(8,128)(2,1)} custom-call(bf16[256,8192]{1,0:T(8,128)(2,1)} %bitcast.16.own_ref, bf16[256,4096]{1,0:T(8,128)(2,1)} %bitcast.47, bf16[4096,256]{1,0:T(8,128)(2,1)} %bitcast.19.go_ref, bf16[4096,256]{1,0:T(8,128)(2,1)} %bitcast.20.uo_ref, bf16[4096,256]{1,0:T(8,128)(2,1)} %collective-permute-done.8.gf_ref, ...), custom_call_target="tpu_custom_call" | custom-call | tf_op jit(solution)/shard_map/hidden/pallas_call | solution.py:413
  214.3 3.0 collective-permute-start.12
  218.5 1.4 copy-done.10
  219.9 9.0 %hidden.3.h_own = bf16[512,512]{1,0:T(8,128)(2,1)} custom-call(bf16[256,8192]{1,0:T(8,128)(2,1)} %bitcast.16.own_ref, bf16[256,4096]{1,0:T(8,128)(2,1)} %bitcast.48, bf16[4096,256]{1,0:T(8,128)(2,1)} %bitcast.19.go_ref, bf16[4096,256]{1,0:T(8,128)(2,1)} %bitcast.20.uo_ref, bf16[4096,256]{1,0:T(8,128)(2,1)} %collective-permute-done.8.gf_ref, ...), custom_call_target="tpu_custom_call" | custom-call | tf_op jit(solution)/shard_map/hidden/pallas_call | solution.py:413
  228.8 2.0 collective-permute-done.12.h_opp
  230.9 9.7 %collective-permute-done.10.h_near = bf16[512,512]{1,0:T(8,128)(2,1)S(1)} collective-permute-done((bf16[512,512]{1,0:T(8,128)(2,1)}, bf16[512,512]{1,0:T(8,128)(2,1)S(1)}, u32[]{:S(2)}, u32[]{:S(2)}) %collective-permute-start.10) | collective-permute-done | bytes 524320 | tf_op jit(solution)/shard_map/ppermute | solution.py:537
  240.6 4.3 %down.2 = bf16[256,4096]{1,0:T(8,128)(2,1)S(1)} custom-call(s32[4]{0:T(128)S(1)} %copy-done.8, bf16[512,512]{1,0:T(8,128)(2,1)S(1)} %copy-done.4, bf16[512,512]{1,0:T(8,128)(2,1)S(1)} %collective-permute-done.10.h_near, bf16[512,512]{1,0:T(8,128)(2,1)} %collective-permute-done.11.h_far, bf16[512,512]{1,0:T(8,128)(2,1)S(1)} %collective-permute-done.12.h_opp, ...), custom_call_target="tpu_custom_call" | custom-call | tf_op jit(solution)/shard_map/down/pallas_call | solution.py:454
  244.9 1.4 copy-done.2
  246.3 7.7 %all-to-all-start.3 = ((bf16[32,8,4096]{2,1,0:T(8,128)(2,1)}), bf16[32,8,4096]{2,1,0:T(8,128)(2,1)}, u32[]{:S(2)}, u32[]{:S(2)}) async-start(bf16[32,8,4096]{2,1,0:T(8,128)(2,1)} %bitcast.42), calls=%async_computation.3 | async-start | bytes 4194304 | tf_op jit(solution)/shard_map/all_to_all | solution.py:553
  254.2 1.4 collective-permute-done.3
  256.4 1.5 collective-permute-start.16
  258.0 2.1 collective-permute-start.17
  262.4 2.6 collective-permute-start.5
  265.0 18.6 %collective-permute-done.4 = f32[2,136,128]{2,1,0:T(8,128)} collective-permute-done((f32[2,136,128]{2,1,0:T(8,128)}, f32[2,136,128]{2,1,0:T(8,128)}, u32[]{:S(2)}, u32[]{:S(2)}) %collective-permute-start.4) | collective-permute-done | bytes 139296 | tf_op jit(solution)/shard_map/ppermute | solution.py:344
  284.1 1.9 collective-permute-done.5
  286.0 3.0 collective-permute-done.6
  289.0 4.4 %down.3 = bf16[256,4096]{1,0:T(8,128)(2,1)S(1)} custom-call(s32[4]{0:T(128)S(1)} %copy-done.8, bf16[512,512]{1,0:T(8,128)(2,1)S(1)} %copy-done.3, bf16[512,512]{1,0:T(8,128)(2,1)S(1)} %collective-permute-done.16.h_near, bf16[512,512]{1,0:T(8,128)(2,1)} %collective-permute-done.17.h_far, bf16[512,512]{1,0:T(8,128)(2,1)} %collective-permute-done.18.h_opp, ...), custom_call_target="tpu_custom_call" | custom-call | tf_op jit(solution)/shard_map/down/pallas_call | solution.py:454
  293.4 1.3 copy-done.1
  294.8 8.6 %all-to-all-start.4 = ((bf16[32,8,4096]{2,1,0:T(8,128)(2,1)}), bf16[32,8,4096]{2,1,0:T(8,128)(2,1)S(1)}, u32[]{:S(2)}, u32[]{:S(2)}) async-start(bf16[32,8,4096]{2,1,0:T(8,128)(2,1)} %bitcast.40), calls=%async_computation.4 | async-start | bytes 4194304 | tf_op jit(solution)/shard_map/all_to_all | solution.py:553
  304.1 1.1 add_add_fusion
  306.0 2.7 collective-permute-start.13
  310.4 2.7 collective-permute-start.20
  313.1 2.2 collective-permute-done.20
  315.3 1.7 places.1.place_ref
  317.0 15.1 %collective-permute-done.13 = f32[2,136,128]{2,1,0:T(8,128)} collective-permute-done((f32[2,136,128]{2,1,0:T(8,128)}, f32[2,136,128]{2,1,0:T(8,128)}, u32[]{:S(2)}, u32[]{:S(2)}) %collective-permute-start.13) | collective-permute-done | bytes 139296 | tf_op jit(solution)/shard_map/ppermute | solution.py:362
  332.1 1.5 collective-permute-done.14
  333.6 2.2 collective-permute-done.15
  336.4 1.3 multiply_add_fusion
  337.8 1.3 collective-permute-done.19
  339.2 1.2 copy-done.5
  340.5 1.2 copy-done.6
  341.7 2.7 readout.1
  344.4 5.0 %combine.1 = bf16[512,1024]{1,0:T(8,128)(2,1)} custom-call(s32[4]{0:T(128)S(1)} %copy-done.8, bf16[256,4096]{1,0:T(8,128)(2,1)} %bitcast.34.low_ref, bf16[256,4096]{1,0:T(8,128)(2,1)S(1)} %bitcast.41, bf16[4,256,512]{2,1,0:T(8,128)(2,1)S(1)} %places.1.place_ref), custom_call_target="tpu_custom_call" | custom-call | tf_op jit(solution)/shard_map/combine/pallas_call | solution.py:513
  (72 shorter events, 12.6 us)
Async XLA Ops:
  7.1 25.1 %collective-permute-start.7 = (bf16[128,4096]{1,0:T(8,128)(2,1)}, bf16[128,4096]{1,0:T(8,128)(2,1)S(1)}, u32[]{:S(2)}, u32[]{:S(2)}) collective-permute-start(bf16[128,4096]{1,0:T(8,128)(2,1)} %get-tuple-element.24.own_ref), channel_id=1, source_target_pairs={{0,1},{1,0},{2,3},{3,2},{4,5},{5,4},{6,7},{7,6},{8,9},{9,8},{10,11... | collective-permute-start | bytes 3145736 | tf_op jit(solution)/shard_map/ppermute | solution.py:537
  32.2 1.0 copy-start.14
  75.1 57.4 %all-to-all-start.1 = ((bf16[32,8,8192]{2,1,0:T(8,128)(2,1)}), bf16[32,8,8192]{2,1,0:T(8,128)(2,1)}, u32[]{:S(2)}, u32[]{:S(2)}) async-start(bf16[32,8,8192]{2,1,0:T(8,128)(2,1)} %bitcast.49), calls=%async_computation.1 | async-start | bytes 8388608 | tf_op jit(solution)/shard_map/all_to_all | solution.py:553
  84.7 56.1 %collective-permute-start.1 = (bf16[128,4096]{1,0:T(8,128)(2,1)}, bf16[128,4096]{1,0:T(8,128)(2,1)}, u32[]{:S(2)}, u32[]{:S(2)}) collective-permute-start(bf16[128,4096]{1,0:T(8,128)(2,1)} %norm.1.a0), channel_id=1, source_target_pairs={{0,3},{1,2},{2,1},{3,0},{4,7},{5,6},{6,5},{7,4},{8,11},{9,10},{10,... | collective-permute-start | bytes 3145736 | tf_op jit(solution)/shard_map/ppermute | solution.py:541
  87.4 118.1 %collective-permute-start.8 = (bf16[4096,256]{1,0:T(8,128)(2,1)}, bf16[4096,256]{1,0:T(8,128)(2,1)}, u32[]{:S(2)}, u32[]{:S(2)}) collective-permute-start(bf16[4096,256]{1,0:T(8,128)(2,1)} %bitcast.19.go_ref), channel_id=1, source_target_pairs={{0,3},{1,2},{2,1},{3,0},{4,7},{5,6},{6,5},{7,4},{8,11},{9,10},{10,... | collective-permute-start | bytes 6291464 | tf_op jit(solution)/shard_map/ppermute | solution.py:541
  87.9 117.6 %collective-permute-start.9 = (bf16[4096,256]{1,0:T(8,128)(2,1)}, bf16[4096,256]{1,0:T(8,128)(2,1)}, u32[]{:S(2)}, u32[]{:S(2)}) collective-permute-start(bf16[4096,256]{1,0:T(8,128)(2,1)} %bitcast.20.uo_ref), channel_id=1, source_target_pairs={{0,3},{1,2},{2,1},{3,0},{4,7},{5,6},{6,5},{7,4},{8,11},{9,10},{10,... | collective-permute-start | bytes 6291464 | tf_op jit(solution)/shard_map/ppermute | solution.py:541
  132.5 6.7 %copy-start.11 = (bf16[128,4096]{1,0:T(8,128)(2,1)S(1)}, bf16[128,4096]{1,0:T(8,128)(2,1)}, u32[]{:S(2)}) copy-start(bf16[128,4096]{1,0:T(8,128)(2,1)} %norm.1.a0) | copy-start | bytes 3145732
  132.5 86.0 %all-to-all-start = ((bf16[32,8,4096]{2,1,0:T(8,128)(2,1)}), bf16[32,8,4096]{2,1,0:T(8,128)(2,1)S(1)}, u32[]{:S(2)}, u32[]{:S(2)}) async-start(bf16[32,8,4096]{2,1,0:T(8,128)(2,1)} %bitcast.50), calls=%async_computation | async-start | bytes 4194304 | tf_op jit(solution)/shard_map/all_to_all | solution.py:553
  139.2 26.1 %collective-permute-start = (bf16[128,4096]{1,0:T(8,128)(2,1)S(1)}, bf16[128,4096]{1,0:T(8,128)(2,1)S(1)}, u32[]{:S(2)}, u32[]{:S(2)}) collective-permute-start(bf16[128,4096]{1,0:T(8,128)(2,1)S(1)} %copy-done.11), channel_id=1, source_target_pairs={{0,1},{1,0},{2,3},{3,2},{4,5},{5,4},{6,7},{7,6},{8,9},{9,8},{10,11... | collective-permute-start | bytes 3145736 | tf_op jit(solution)/shard_map/ppermute | solution.py:537
  140.7 46.2 %collective-permute-start.2 = (bf16[128,4096]{1,0:T(8,128)(2,1)}, bf16[128,4096]{1,0:T(8,128)(2,1)S(1)}, u32[]{:S(2)}, u32[]{:S(2)}) collective-permute-start(bf16[128,4096]{1,0:T(8,128)(2,1)} %collective-permute-done.1.a2), channel_id=1, source_target_pairs={{0,1},{1,0},{2,3},{3,2},{4,5},{5,4},{6,7},{7,6},{8,9},{9,8},{10,11... | collective-permute-start | bytes 3145736 | tf_op jit(solution)/shard_map/ppermute | solution.py:537
  165.3 21.6 %copy-start.15 = (bf16[128,4096]{1,0:T(8,128)(2,1)}, bf16[128,4096]{1,0:T(8,128)(2,1)S(1)}, u32[]{:S(2)}) copy-start(bf16[128,4096]{1,0:T(8,128)(2,1)S(1)} %collective-permute-done.a1) | copy-start | bytes 3145732
  186.9 1.0 copy-start.16
  214.3 16.6 %collective-permute-start.12 = (bf16[512,512]{1,0:T(8,128)(2,1)}, bf16[512,512]{1,0:T(8,128)(2,1)S(1)}, u32[]{:S(2)}, u32[]{:S(2)}) collective-permute-start(bf16[512,512]{1,0:T(8,128)(2,1)} %hidden.2.h_own), channel_id=1, source_target_pairs={{0,2},{1,3},{2,0},{3,1},{4,6},{5,7},{6,4},{7,5},{8,10},{9,11},{10,... | collective-permute-start | bytes 1572872 | tf_op jit(solution)/shard_map/ppermute | solution.py:547
  217.3 23.3 %collective-permute-start.10 = (bf16[512,512]{1,0:T(8,128)(2,1)}, bf16[512,512]{1,0:T(8,128)(2,1)S(1)}, u32[]{:S(2)}, u32[]{:S(2)}) collective-permute-start(bf16[512,512]{1,0:T(8,128)(2,1)} %hidden.2.h_own), channel_id=1, source_target_pairs={{0,1},{1,0},{2,3},{3,2},{4,5},{5,4},{6,7},{7,6},{8,9},{9,8},{10,11... | collective-permute-start | bytes 1572872 | tf_op jit(solution)/shard_map/ppermute | solution.py:537
  217.9 22.7 %collective-permute-start.11 = (bf16[512,512]{1,0:T(8,128)(2,1)}, bf16[512,512]{1,0:T(8,128)(2,1)}, u32[]{:S(2)}, u32[]{:S(2)}) collective-permute-start(bf16[512,512]{1,0:T(8,128)(2,1)} %hidden.2.h_own), channel_id=1, source_target_pairs={{0,3},{1,2},{2,1},{3,0},{4,7},{5,6},{6,5},{7,4},{8,11},{9,10},{10,... | collective-permute-start | bytes 1572872 | tf_op jit(solution)/shard_map/ppermute | solution.py:541
  218.5 1.4 copy-start.10
  219.9 20.7 %copy-start = (bf16[1,1024,1024]{2,1,0:T(8,128)(2,1)S(1)}, bf16[1,1024,1024]{2,1,0:T(8,128)(2,1)}, u32[]{:S(2)}) copy-start(bf16[1,1024,1024]{2,1,0:T(8,128)(2,1)} %param.26) | copy-start | bytes 6291460
  219.9 20.7 %copy-start.4 = (bf16[512,512]{1,0:T(8,128)(2,1)S(1)}, bf16[512,512]{1,0:T(8,128)(2,1)}, u32[]{:S(2)}) copy-start(bf16[512,512]{1,0:T(8,128)(2,1)} %hidden.2.h_own) | copy-start | bytes 1572868
  219.9 20.7 %copy-start.8 = (s32[4]{0:T(128)S(1)}, s32[4]{0:T(128)}, u32[]{:S(2)}) copy-start(s32[4]{0:T(128)} %pad_add_fusion.src) | copy-start | bytes 52
  244.9 1.4 copy-start.2
  246.3 7.7 %copy-start.17 = (f32[4,136,128]{2,1,0:T(8,128)S(1)}, f32[4,136,128]{2,1,0:T(8,128)}, u32[]{:S(2)}) copy-start(f32[4,136,128]{2,1,0:T(8,128)} %get-tuple-element.23) | copy-start | bytes 835588
  246.3 10.2 %copy-start.3 = (bf16[512,512]{1,0:T(8,128)(2,1)S(1)}, bf16[512,512]{1,0:T(8,128)(2,1)}, u32[]{:S(2)}) copy-start(bf16[512,512]{1,0:T(8,128)(2,1)} %hidden.3.h_own) | copy-start | bytes 1572868
  246.3 48.5 %all-to-all-start.3 = ((bf16[32,8,4096]{2,1,0:T(8,128)(2,1)}), bf16[32,8,4096]{2,1,0:T(8,128)(2,1)}, u32[]{:S(2)}, u32[]{:S(2)}) async-start(bf16[32,8,4096]{2,1,0:T(8,128)(2,1)} %bitcast.42), calls=%async_computation.3 | async-start | bytes 4194304 | tf_op jit(solution)/shard_map/all_to_all | solution.py:553
  254.0 1.6 collective-permute-start.3
  255.6 0.7 copy-start.18
  256.4 32.5 %collective-permute-start.16 = (bf16[512,512]{1,0:T(8,128)(2,1)S(1)}, bf16[512,512]{1,0:T(8,128)(2,1)S(1)}, u32[]{:S(2)}, u32[]{:S(2)}) collective-permute-start(bf16[512,512]{1,0:T(8,128)(2,1)S(1)} %copy-done.3), channel_id=1, source_target_pairs={{0,1},{1,0},{2,3},{3,2},{4,5},{5,4},{6,7},{7,6},{8,9},{9,8},{10,11... | collective-permute-start | bytes 1572872 | tf_op jit(solution)/shard_map/ppermute | solution.py:537
  258.0 31.0 %collective-permute-start.17 = (bf16[512,512]{1,0:T(8,128)(2,1)S(1)}, bf16[512,512]{1,0:T(8,128)(2,1)}, u32[]{:S(2)}, u32[]{:S(2)}) collective-permute-start(bf16[512,512]{1,0:T(8,128)(2,1)S(1)} %copy-done.3), channel_id=1, source_target_pairs={{0,3},{1,2},{2,1},{3,0},{4,7},{5,6},{6,5},{7,4},{8,11},{9,10},{10,... | collective-permute-start | bytes 1572872 | tf_op jit(solution)/shard_map/ppermute | solution.py:541
  260.1 28.9 %collective-permute-start.18 = (bf16[512,512]{1,0:T(8,128)(2,1)S(1)}, bf16[512,512]{1,0:T(8,128)(2,1)}, u32[]{:S(2)}, u32[]{:S(2)}) collective-permute-start(bf16[512,512]{1,0:T(8,128)(2,1)S(1)} %copy-done.3), channel_id=1, source_target_pairs={{0,2},{1,3},{2,0},{3,1},{4,6},{5,7},{6,4},{7,5},{8,10},{9,11},{10,... | collective-permute-start | bytes 1572872 | tf_op jit(solution)/shard_map/ppermute | solution.py:547
  260.7 0.7 copy-start.12
  262.0 21.5 %collective-permute-start.4 = (f32[2,136,128]{2,1,0:T(8,128)}, f32[2,136,128]{2,1,0:T(8,128)}, u32[]{:S(2)}, u32[]{:S(2)}) collective-permute-start(f32[2,136,128]{2,1,0:T(8,128)} %pad_maximum_fusion.1), channel_id=1, source_target_pairs={{0,24},{8,0},{16,8},{24,16},{1,25},{9,1},{17,9},{25,17},{2,26},{10... | collective-permute-start | bytes 417800 | tf_op jit(solution)/shard_map/ppermute | solution.py:344
  262.4 23.6 %collective-permute-start.5 = (f32[2,136,128]{2,1,0:T(8,128)}, f32[2,136,128]{2,1,0:T(8,128)}, u32[]{:S(2)}, u32[]{:S(2)}) collective-permute-start(f32[2,136,128]{2,1,0:T(8,128)} %pad_maximum_fusion.1), channel_id=1, source_target_pairs={{0,16},{8,24},{16,0},{24,8},{1,17},{9,25},{17,1},{25,9},{2,18},{10... | collective-permute-start | bytes 417800 | tf_op jit(solution)/shard_map/ppermute | solution.py:344
  283.6 5.4 %collective-permute-start.6 = (f32[2,136,128]{2,1,0:T(8,128)}, f32[2,136,128]{2,1,0:T(8,128)}, u32[]{:S(2)}, u32[]{:S(2)}) collective-permute-start(f32[2,136,128]{2,1,0:T(8,128)} %pad_maximum_fusion.1), channel_id=1, source_target_pairs={{0,8},{8,16},{16,24},{24,0},{1,9},{9,17},{17,25},{25,1},{2,10},{10... | collective-permute-start | bytes 417800 | tf_op jit(solution)/shard_map/ppermute | solution.py:344
  293.4 1.4 copy-start.1
  294.8 9.3 %copy-start.13 = (f32[2,128,128]{2,1,0:T(8,128)S(1)}, f32[2,128,128]{2,1,0:T(8,128)}, u32[]{:S(2)}) copy-start(f32[2,128,128]{2,1,0:T(8,128)} %copy-done.12) | copy-start | bytes 393220
  294.8 15.6 %copy-start.19 = (bf16[2,32,128]{2,1,0:T(8,128)(2,1)S(1)}, bf16[2,32,128]{2,1,0:T(8,128)(2,1)}, u32[]{:S(2)}) copy-start(bf16[2,32,128]{2,1,0:T(8,128)(2,1)} %get-tuple-element.39) | copy-start | bytes 49156
  294.8 20.5 %copy-start.7 = (s32[512,2]{0,1:T(2,128)S(1)}, s32[512,2]{0,1:T(2,128)}, u32[]{:S(2)}) copy-start(s32[512,2]{0,1:T(2,128)} %param.27) | copy-start | bytes 12292
  294.8 49.6 %all-to-all-start.4 = ((bf16[32,8,4096]{2,1,0:T(8,128)(2,1)}), bf16[32,8,4096]{2,1,0:T(8,128)(2,1)S(1)}, u32[]{:S(2)}, u32[]{:S(2)}) async-start(bf16[32,8,4096]{2,1,0:T(8,128)(2,1)} %bitcast.40), calls=%async_computation.4 | async-start | bytes 4194304 | tf_op jit(solution)/shard_map/all_to_all | solution.py:553
  304.1 35.1 %copy-start.9 = (f32[512]{0:T(512)S(1)}, f32[512]{0:T(512)}, u32[]{:S(2)}) copy-start(f32[512]{0:T(512)} %param.21) | copy-start | bytes 6148
  306.0 26.1 %collective-permute-start.13 = (f32[2,136,128]{2,1,0:T(8,128)}, f32[2,136,128]{2,1,0:T(8,128)}, u32[]{:S(2)}, u32[]{:S(2)}) collective-permute-start(f32[2,136,128]{2,1,0:T(8,128)} %pad_maximum_fusion.2), channel_id=1, source_target_pairs={{0,96},{32,0},{64,32},{96,64},{1,97},{33,1},{65,33},{97,65},{2,98}... | collective-permute-start | bytes 417800 | tf_op jit(solution)/shard_map/ppermute | solution.py:362
  308.7 24.9 %collective-permute-start.14 = (f32[2,136,128]{2,1,0:T(8,128)}, f32[2,136,128]{2,1,0:T(8,128)}, u32[]{:S(2)}, u32[]{:S(2)}) collective-permute-start(f32[2,136,128]{2,1,0:T(8,128)} %pad_maximum_fusion.2), channel_id=1, source_target_pairs={{0,64},{32,96},{64,0},{96,32},{1,65},{33,97},{65,1},{97,33},{2,66}... | collective-permute-start | bytes 417800 | tf_op jit(solution)/shard_map/ppermute | solution.py:362
  309.5 26.2 %collective-permute-start.15 = (f32[2,136,128]{2,1,0:T(8,128)}, f32[2,136,128]{2,1,0:T(8,128)}, u32[]{:S(2)}, u32[]{:S(2)}) collective-permute-start(f32[2,136,128]{2,1,0:T(8,128)} %pad_maximum_fusion.2), channel_id=1, source_target_pairs={{0,32},{32,64},{64,96},{96,0},{1,33},{33,65},{65,97},{97,1},{2,34}... | collective-permute-start | bytes 417800 | tf_op jit(solution)/shard_map/ppermute | solution.py:362
  310.4 4.9 %collective-permute-start.20 = (bf16[2,32,128]{2,1,0:T(8,128)(2,1)S(1)}, bf16[2,32,128]{2,1,0:T(8,128)(2,1)S(1)}, u32[]{:S(2)}, u32[]{:S(2)}) collective-permute-start(bf16[2,32,128]{2,1,0:T(8,128)(2,1)S(1)} %copy-done.19), channel_id=1, source_target_pairs={{0,3},{1,2},{2,1},{3,0},{4,7},{5,6},{6,5},{7,4},{8,11},{9,10},{10,... | collective-permute-start | bytes 49160 | tf_op jit(solution)/shard_map/ppermute | solution.py:541
  337.7 1.4 collective-permute-start.19
  339.2 1.2 copy-start.5
  340.5 1.2 copy-start.6

commit v7 on v5

--- a/solution.py
+++ b/solution.py
@@ -231,7 +231,7 @@
     rows = 4 * toks
     cols = wq.shape[1]
     heads = cols // HEAD_DIM
-    kb = 512
+    kb = 1024
     fixed = lambda i, s: (0, 0)
     weight = pl.BlockSpec((kb, cols), lambda i, s: (i, 0))
     return pl.pallas_call(
@@ -253,7 +253,7 @@
             jax.ShapeDtypeStruct((rows, cols), F32),
             jax.ShapeDtypeStruct((heads, HEAD_DIM + 8, HEAD_DIM), F32),
         ],
-        compiler_params=params(28),
+        compiler_params=params(),
         name="mixer",
     )(src, *parts, wq, wf, wv, gap)
 
@@ -406,7 +406,7 @@
         out_specs=pl.BlockSpec((2 * count, 2 * n), lambda i: (0, 0)),
         out_shape=jax.ShapeDtypeStruct((2 * count, 2 * n), BF16),
         scratch_shapes=[pltpu.VMEM((2 * count, 2 * n), F32)] * 2,
-        compiler_params=params(14),
+        compiler_params=params(),
         name="hidden",
     )(own, near, *weights)
 

time: 355 us -> 350 us (0.986)
  local copies, waits for them, and re-layouts: 13.5 us -> 9.88 us
    unnamed x40 -> x44, local copies, waits for them, and re-layouts: 12.7 us -> 9.87 us
  transfers between devices with their start and end apart: 25 -> 25, of which waited for: 15 -> 15; matrix products, arithmetic and copies ran while one was open for 3% -> 2% of each run, Pallas kernels for 11% -> 12%
where the time goes in v7:
time: 350 us; the launch traced here: 348 us
  waiting for transfers between devices  173 us (49%)
  Pallas kernels  63.9 us (18%)
  starting transfers between devices  57.7 us (16%)
  blocking collectives  35.9 us (10%)
  local copies, waits for them, and re-layouts  9.88 us (3%)
  other arithmetic  6.69 us (2%)
    ppermute x5, waiting for transfers between devices, to_near(): return lax.ppermute(a, 'tp', NEAR)  79 us
    all_to_all x4, waiting for transfers between devices, swap(): lax.all_to_all(a.reshape(experts, rows // experts, cols), EP, split_axis=...  44.8 us
    all_to_all x1, blocking collectives, swap(): lax.all_to_all(a.reshape(experts, rows // experts, cols), EP, split_axis=...  35.9 us
    all_to_all x4, starting transfers between devices, swap(): lax.all_to_all(a.reshape(experts, rows // experts, cols), EP, split_axis=...  28.8 us
    ppermute x3, waiting for transfers between devices, along_rows(): lax.ppermute(sent, 'ep_1', [(i, (i + d) % count) for i in range(count)])  23.5 us
    ppermute x3, waiting for transfers between devices, along_planes(): lax.ppermute(plane, 'ep_0', [(i, (i + d) % count) for i in range(count)])  18.7 us
    pallas_call x2, Pallas kernels, hidden_units(): pl.pallas_call(hidden_kernel, grid=(width // kb,), in_specs=[pl.BlockSpec...  17.8 us
    pallas_call x1, Pallas kernels, mixer(): pl.pallas_call(mixer_kernel, grid_spec=pltpu.PrefetchScalarGridSpec(num_s...  16.2 us
  transfers between devices with their start and end apart: 25, of which 15 were waited for; matrix products, arithmetic and copies ran while one was open for 2% of the time, Pallas kernels for 12%

profile of v7, /device:TPU:8, one launch (start us, length us, event | category | flops | bytes accessed | tf_op | source)
XLA Modules:
  0.0 348.0 jit_solution(15686996632693638620)
XLA Ops:
  1.3 5.8 %front.1 = (bf16[128,4096]{1,0:T(8,128)(2,1)}, bf16[256,8192]{1,0:T(8,128)(2,1)}) custom-call(s32[4]{0:T(128)} %pad_add_fusion.src, bf16[128,4096]{1,0:T(8,128)(2,1)} %x_ref.1, f32[1,4096]{1,0:T(1,128)} %bitcast.52, s32[4,2,128]{2,1,0:T(2,128)} %bitcast.42), custom_call_target="tpu_custom_call" | custom-call | tf_op jit(solution)/shard_map/front/pallas_call | solution.py:100
  7.1 1.5 collective-permute-start.7
  8.5 23.6 %collective-permute-done.7.rows_ref = bf16[128,4096]{1,0:T(8,128)(2,1)S(1)} collective-permute-done((bf16[128,4096]{1,0:T(8,128)(2,1)}, bf16[128,4096]{1,0:T(8,128)(2,1)S(1)}, u32[]{:S(2)}, u32[]{:S(2)}) %collective-permute-start.7) | collective-permute-done | bytes 1048608 | tf_op jit(solution)/shard_map/ppermute | solution.py:519
  33.1 6.0 %refill.1 = (bf16[2,32,128]{2,1,0:T(8,128)(2,1)}, bf16[256,4096]{1,0:T(8,128)(2,1)}, bf16[256,4096]{1,0:T(8,128)(2,1)}) custom-call(s32[4]{0:T(128)} %pad_add_fusion.src, bf16[128,4096]{1,0:T(8,128)(2,1)} %get-tuple-element.24.own_ref, bf16[128,4096]{1,0:T(8,128)(2,1)} %copy-done.15, bf16[32,4096]{1,0:T(8,128)(2,1)} %bitcast.51, s32[4,2,128]{2,1,0:T(2,128)} %bitcast.43), custom_call_target="tpu_custom_call" | custom-call | tf_op jit(solution)/shard_map/refill/pallas_call | solution.py:129
  39.2 35.9 %all_to_all.25 = bf16[32,8,4096]{2,1,0:T(8,128)(2,1)} all-to-all(bf16[32,8,4096]{2,1,0:T(8,128)(2,1)} %bitcast.50), channel_id=1, replica_groups=mesh['ep_0'=4,'ep_1'=4,'ep_2'=2,'tp'=4] {'ep_0','ep_1','ep_2'}, dimensions={0} | all-to-all | bytes 4194304 | tf_op jit(solution)/shard_map/all_to_all | solution.py:535
  75.1 6.0 %all-to-all-start.1 = ((bf16[32,8,8192]{2,1,0:T(8,128)(2,1)}), bf16[32,8,8192]{2,1,0:T(8,128)(2,1)}, u32[]{:S(2)}, u32[]{:S(2)}) async-start(bf16[32,8,8192]{2,1,0:T(8,128)(2,1)} %bitcast.48), calls=%async_computation.1 | async-start | bytes 8388608 | tf_op jit(solution)/shard_map/all_to_all | solution.py:535
  81.8 2.8 collective-permute-start.1
  85.1 2.8 collective-permute-start.9
  87.8 44.8 %all-to-all-done.1 = bf16[32,8,8192]{2,1,0:T(8,128)(2,1)} async-done(((bf16[32,8,8192]{2,1,0:T(8,128)(2,1)}), bf16[32,8,8192]{2,1,0:T(8,128)(2,1)}, u32[]{:S(2)}, u32[]{:S(2)}) %all-to-all-start.1) | async-done | bytes 4194336 | tf_op jit(solution)/shard_map/all_to_all | solution.py:535
  132.6 6.5 %all-to-all-start = ((bf16[32,8,4096]{2,1,0:T(8,128)(2,1)}), bf16[32,8,4096]{2,1,0:T(8,128)(2,1)S(1)}, u32[]{:S(2)}, u32[]{:S(2)}) async-start(bf16[32,8,4096]{2,1,0:T(8,128)(2,1)} %bitcast.49), calls=%async_computation | async-start | bytes 4194304 | tf_op jit(solution)/shard_map/all_to_all | solution.py:535
  139.2 1.6 collective-permute-start
  141.3 24.0 %collective-permute-done.a1 = bf16[128,4096]{1,0:T(8,128)(2,1)S(1)} collective-permute-done((bf16[128,4096]{1,0:T(8,128)(2,1)S(1)}, bf16[128,4096]{1,0:T(8,128)(2,1)S(1)}, u32[]{:S(2)}, u32[]{:S(2)}) %collective-permute-start) | collective-permute-done | bytes 1048608 | tf_op jit(solution)/shard_map/ppermute | solution.py:519
  165.3 21.6 %collective-permute-done.2.a3 = bf16[128,4096]{1,0:T(8,128)(2,1)S(1)} collective-permute-done((bf16[128,4096]{1,0:T(8,128)(2,1)}, bf16[128,4096]{1,0:T(8,128)(2,1)S(1)}, u32[]{:S(2)}, u32[]{:S(2)}) %collective-permute-start.2) | collective-permute-done | bytes 1048608 | tf_op jit(solution)/shard_map/ppermute | solution.py:519
  186.9 1.0 copy-done.17
  187.9 16.2 %mixer.1 = (f32[512,512]{1,0:T(8,128)}, f32[512,512]{1,0:T(8,128)}, f32[4,136,128]{2,1,0:T(8,128)}) custom-call(s32[4]{0:T(128)} %pad_add_fusion.src, bf16[128,4096]{1,0:T(8,128)(2,1)} %copy-done.12, bf16[128,4096]{1,0:T(8,128)(2,1)} %copy-done.16, bf16[128,4096]{1,0:T(8,128)(2,1)} %collective-permute-done.1.a2, bf16[128,4096]{1,0:T(8,128)(2,1)} %copy-done.17, ...), custom_call_target="tpu_custom_call" | custom-call | tf_op jit(solution)/shard_map/mixer/pallas_call | solution.py:237
  204.1 8.8 %hidden.2.h_own = bf16[512,512]{1,0:T(8,128)(2,1)} custom-call(bf16[256,8192]{1,0:T(8,128)(2,1)} %bitcast.15.own_ref, bf16[256,4096]{1,0:T(8,128)(2,1)} %bitcast.46, bf16[4096,256]{1,0:T(8,128)(2,1)} %bitcast.18.go_ref, bf16[4096,256]{1,0:T(8,128)(2,1)} %bitcast.19.uo_ref, bf16[4096,256]{1,0:T(8,128)(2,1)} %collective-permute-done.8.gf_ref, ...), custom_call_target="tpu_custom_call" | custom-call | tf_op jit(solution)/shard_map/hidden/pallas_call | solution.py:395
  213.0 3.0 collective-permute-start.12
  217.2 1.4 copy-done.10
  218.5 9.0 %hidden.3.h_own = bf16[512,512]{1,0:T(8,128)(2,1)} custom-call(bf16[256,8192]{1,0:T(8,128)(2,1)} %bitcast.15.own_ref, bf16[256,4096]{1,0:T(8,128)(2,1)} %bitcast.47, bf16[4096,256]{1,0:T(8,128)(2,1)} %bitcast.18.go_ref, bf16[4096,256]{1,0:T(8,128)(2,1)} %bitcast.19.uo_ref, bf16[4096,256]{1,0:T(8,128)(2,1)} %collective-permute-done.8.gf_ref, ...), custom_call_target="tpu_custom_call" | custom-call | tf_op jit(solution)/shard_map/hidden/pallas_call | solution.py:395
  227.5 2.0 collective-permute-done.12.h_opp
  229.5 9.7 %collective-permute-done.10.h_near = bf16[512,512]{1,0:T(8,128)(2,1)S(1)} collective-permute-done((bf16[512,512]{1,0:T(8,128)(2,1)}, bf16[512,512]{1,0:T(8,128)(2,1)S(1)}, u32[]{:S(2)}, u32[]{:S(2)}) %collective-permute-start.10) | collective-permute-done | bytes 524320 | tf_op jit(solution)/shard_map/ppermute | solution.py:519
  239.3 4.3 %down.2 = bf16[256,4096]{1,0:T(8,128)(2,1)S(1)} custom-call(s32[4]{0:T(128)S(1)} %copy-done.8, bf16[512,512]{1,0:T(8,128)(2,1)S(1)} %copy-done.4, bf16[512,512]{1,0:T(8,128)(2,1)S(1)} %collective-permute-done.10.h_near, bf16[512,512]{1,0:T(8,128)(2,1)} %collective-permute-done.11.h_far, bf16[512,512]{1,0:T(8,128)(2,1)S(1)} %collective-permute-done.12.h_opp, ...), custom_call_target="tpu_custom_call" | custom-call | tf_op jit(solution)/shard_map/down/pallas_call | solution.py:436
  243.6 1.4 copy-done.2
  244.9 7.7 %all-to-all-start.3 = ((bf16[32,8,4096]{2,1,0:T(8,128)(2,1)}), bf16[32,8,4096]{2,1,0:T(8,128)(2,1)}, u32[]{:S(2)}, u32[]{:S(2)}) async-start(bf16[32,8,4096]{2,1,0:T(8,128)(2,1)} %bitcast.41), calls=%async_computation.3 | async-start | bytes 4194304 | tf_op jit(solution)/shard_map/all_to_all | solution.py:535
  252.8 1.4 collective-permute-done.3
  255.1 1.5 collective-permute-start.16
  256.6 2.1 collective-permute-start.17
  261.0 2.6 collective-permute-start.5
  263.6 18.6 %collective-permute-done.4 = f32[2,136,128]{2,1,0:T(8,128)} collective-permute-done((f32[2,136,128]{2,1,0:T(8,128)}, f32[2,136,128]{2,1,0:T(8,128)}, u32[]{:S(2)}, u32[]{:S(2)}) %collective-permute-start.4) | collective-permute-done | bytes 139296 | tf_op jit(solution)/shard_map/ppermute | solution.py:326
  282.8 1.9 collective-permute-done.5
  284.6 3.0 collective-permute-done.6
  287.6 4.4 %down.3 = bf16[256,4096]{1,0:T(8,128)(2,1)S(1)} custom-call(s32[4]{0:T(128)S(1)} %copy-done.8, bf16[512,512]{1,0:T(8,128)(2,1)S(1)} %copy-done.3, bf16[512,512]{1,0:T(8,128)(2,1)S(1)} %collective-permute-done.16.h_near, bf16[512,512]{1,0:T(8,128)(2,1)} %collective-permute-done.17.h_far, bf16[512,512]{1,0:T(8,128)(2,1)} %collective-permute-done.18.h_opp, ...), custom_call_target="tpu_custom_call" | custom-call | tf_op jit(solution)/shard_map/down/pallas_call | solution.py:436
  292.1 1.3 copy-done.1
  293.5 8.6 %all-to-all-start.4 = ((bf16[32,8,4096]{2,1,0:T(8,128)(2,1)}), bf16[32,8,4096]{2,1,0:T(8,128)(2,1)S(1)}, u32[]{:S(2)}, u32[]{:S(2)}) async-start(bf16[32,8,4096]{2,1,0:T(8,128)(2,1)} %bitcast.39), calls=%async_computation.4 | async-start | bytes 4194304 | tf_op jit(solution)/shard_map/all_to_all | solution.py:535
  302.8 1.1 add_add_fusion
  304.6 2.7 collective-permute-start.13
  309.0 2.7 collective-permute-start.20
  311.7 2.2 collective-permute-done.20
  314.0 1.7 places.1.place_ref
  315.7 15.1 %collective-permute-done.13 = f32[2,136,128]{2,1,0:T(8,128)} collective-permute-done((f32[2,136,128]{2,1,0:T(8,128)}, f32[2,136,128]{2,1,0:T(8,128)}, u32[]{:S(2)}, u32[]{:S(2)}) %collective-permute-start.13) | collective-permute-done | bytes 139296 | tf_op jit(solution)/shard_map/ppermute | solution.py:344
  330.7 1.5 collective-permute-done.14
  332.2 2.2 collective-permute-done.15
  335.1 1.3 multiply_add_fusion
  336.5 1.3 collective-permute-done.19
  337.9 1.2 copy-done.5
  339.1 1.2 copy-done.6
  340.3 2.7 readout.1
  343.0 5.0 %combine.1 = bf16[512,1024]{1,0:T(8,128)(2,1)} custom-call(s32[4]{0:T(128)S(1)} %copy-done.8, bf16[256,4096]{1,0:T(8,128)(2,1)} %bitcast.33.low_ref, bf16[256,4096]{1,0:T(8,128)(2,1)S(1)} %bitcast.40, bf16[4,256,512]{2,1,0:T(8,128)(2,1)S(1)} %places.1.place_ref), custom_call_target="tpu_custom_call" | custom-call | tf_op jit(solution)/shard_map/combine/pallas_call | solution.py:495
  (78 shorter events, 12.3 us)
Async XLA Ops:
  7.1 25.1 %collective-permute-start.7 = (bf16[128,4096]{1,0:T(8,128)(2,1)}, bf16[128,4096]{1,0:T(8,128)(2,1)S(1)}, u32[]{:S(2)}, u32[]{:S(2)}) collective-permute-start(bf16[128,4096]{1,0:T(8,128)(2,1)} %get-tuple-element.24.own_ref), channel_id=1, source_target_pairs={{0,1},{1,0},{2,3},{3,2},{4,5},{5,4},{6,7},{7,6},{8,9},{9,8},{10,11... | collective-permute-start | bytes 3145736 | tf_op jit(solution)/shard_map/ppermute | solution.py:519
  32.2 1.0 copy-start.15
  75.1 6.1 %copy-start.11 = (bf16[128,4096]{1,0:T(8,128)(2,1)S(1)}, bf16[128,4096]{1,0:T(8,128)(2,1)}, u32[]{:S(2)}) copy-start(bf16[128,4096]{1,0:T(8,128)(2,1)} %param.14) | copy-start | bytes 3145732
  75.1 6.4 %copy-start.20 = (f32[4096]{0:T(1024)S(1)}, f32[4096]{0:T(1024)}, u32[]{:S(2)}) copy-start(f32[4096]{0:T(1024)} %param.16) | copy-start | bytes 49156
  75.1 57.6 %all-to-all-start.1 = ((bf16[32,8,8192]{2,1,0:T(8,128)(2,1)}), bf16[32,8,8192]{2,1,0:T(8,128)(2,1)}, u32[]{:S(2)}, u32[]{:S(2)}) async-start(bf16[32,8,8192]{2,1,0:T(8,128)(2,1)} %bitcast.48), calls=%async_computation.1 | async-start | bytes 8388608 | tf_op jit(solution)/shard_map/all_to_all | solution.py:535
  81.8 57.4 %copy-start.12 = (bf16[128,4096]{1,0:T(8,128)(2,1)}, bf16[128,4096]{1,0:T(8,128)(2,1)S(1)}, u32[]{:S(2)}) copy-start(bf16[128,4096]{1,0:T(8,128)(2,1)S(1)} %fusion.2.a0) | copy-start | bytes 3145732
  81.8 59.0 %collective-permute-start.1 = (bf16[128,4096]{1,0:T(8,128)(2,1)S(1)}, bf16[128,4096]{1,0:T(8,128)(2,1)}, u32[]{:S(2)}, u32[]{:S(2)}) collective-permute-start(bf16[128,4096]{1,0:T(8,128)(2,1)S(1)} %fusion.2.a0), channel_id=1, source_target_pairs={{0,3},{1,2},{2,1},{3,0},{4,7},{5,6},{6,5},{7,4},{8,11},{9,10},{10,... | collective-permute-start | bytes 3145736 | tf_op jit(solution)/shard_map/ppermute | solution.py:523
  84.6 119.5 %collective-permute-start.8 = (bf16[4096,256]{1,0:T(8,128)(2,1)}, bf16[4096,256]{1,0:T(8,128)(2,1)}, u32[]{:S(2)}, u32[]{:S(2)}) collective-permute-start(bf16[4096,256]{1,0:T(8,128)(2,1)} %bitcast.18.go_ref), channel_id=1, source_target_pairs={{0,3},{1,2},{2,1},{3,0},{4,7},{5,6},{6,5},{7,4},{8,11},{9,10},{10,... | collective-permute-start | bytes 6291464 | tf_op jit(solution)/shard_map/ppermute | solution.py:523
  85.1 119.0 %collective-permute-start.9 = (bf16[4096,256]{1,0:T(8,128)(2,1)}, bf16[4096,256]{1,0:T(8,128)(2,1)}, u32[]{:S(2)}, u32[]{:S(2)}) collective-permute-start(bf16[4096,256]{1,0:T(8,128)(2,1)} %bitcast.19.uo_ref), channel_id=1, source_target_pairs={{0,3},{1,2},{2,1},{3,0},{4,7},{5,6},{6,5},{7,4},{8,11},{9,10},{10,... | collective-permute-start | bytes 6291464 | tf_op jit(solution)/shard_map/ppermute | solution.py:523
  132.6 84.5 %all-to-all-start = ((bf16[32,8,4096]{2,1,0:T(8,128)(2,1)}), bf16[32,8,4096]{2,1,0:T(8,128)(2,1)S(1)}, u32[]{:S(2)}, u32[]{:S(2)}) async-start(bf16[32,8,4096]{2,1,0:T(8,128)(2,1)} %bitcast.49), calls=%async_computation | async-start | bytes 4194304 | tf_op jit(solution)/shard_map/all_to_all | solution.py:535
  139.2 26.1 %collective-permute-start = (bf16[128,4096]{1,0:T(8,128)(2,1)S(1)}, bf16[128,4096]{1,0:T(8,128)(2,1)S(1)}, u32[]{:S(2)}, u32[]{:S(2)}) collective-permute-start(bf16[128,4096]{1,0:T(8,128)(2,1)S(1)} %fusion.2.a0), channel_id=1, source_target_pairs={{0,1},{1,0},{2,3},{3,2},{4,5},{5,4},{6,7},{7,6},{8,9},{9,8},{10,11... | collective-permute-start | bytes 3145736 | tf_op jit(solution)/shard_map/ppermute | solution.py:519
  140.7 46.2 %collective-permute-start.2 = (bf16[128,4096]{1,0:T(8,128)(2,1)}, bf16[128,4096]{1,0:T(8,128)(2,1)S(1)}, u32[]{:S(2)}, u32[]{:S(2)}) collective-permute-start(bf16[128,4096]{1,0:T(8,128)(2,1)} %collective-permute-done.1.a2), channel_id=1, source_target_pairs={{0,1},{1,0},{2,3},{3,2},{4,5},{5,4},{6,7},{7,6},{8,9},{9,8},{10,11... | collective-permute-start | bytes 3145736 | tf_op jit(solution)/shard_map/ppermute | solution.py:519
  165.3 21.6 %copy-start.16 = (bf16[128,4096]{1,0:T(8,128)(2,1)}, bf16[128,4096]{1,0:T(8,128)(2,1)S(1)}, u32[]{:S(2)}) copy-start(bf16[128,4096]{1,0:T(8,128)(2,1)S(1)} %collective-permute-done.a1) | copy-start | bytes 3145732
  186.9 1.0 copy-start.17
  213.0 16.6 %collective-permute-start.12 = (bf16[512,512]{1,0:T(8,128)(2,1)}, bf16[512,512]{1,0:T(8,128)(2,1)S(1)}, u32[]{:S(2)}, u32[]{:S(2)}) collective-permute-start(bf16[512,512]{1,0:T(8,128)(2,1)} %hidden.2.h_own), channel_id=1, source_target_pairs={{0,2},{1,3},{2,0},{3,1},{4,6},{5,7},{6,4},{7,5},{8,10},{9,11},{10,... | collective-permute-start | bytes 1572872 | tf_op jit(solution)/shard_map/ppermute | solution.py:529
  216.0 23.2 %collective-permute-start.10 = (bf16[512,512]{1,0:T(8,128)(2,1)}, bf16[512,512]{1,0:T(8,128)(2,1)S(1)}, u32[]{:S(2)}, u32[]{:S(2)}) collective-permute-start(bf16[512,512]{1,0:T(8,128)(2,1)} %hidden.2.h_own), channel_id=1, source_target_pairs={{0,1},{1,0},{2,3},{3,2},{4,5},{5,4},{6,7},{7,6},{8,9},{9,8},{10,11... | collective-permute-start | bytes 1572872 | tf_op jit(solution)/shard_map/ppermute | solution.py:519
  216.6 22.7 %collective-permute-start.11 = (bf16[512,512]{1,0:T(8,128)(2,1)}, bf16[512,512]{1,0:T(8,128)(2,1)}, u32[]{:S(2)}, u32[]{:S(2)}) collective-permute-start(bf16[512,512]{1,0:T(8,128)(2,1)} %hidden.2.h_own), channel_id=1, source_target_pairs={{0,3},{1,2},{2,1},{3,0},{4,7},{5,6},{6,5},{7,4},{8,11},{9,10},{10,... | collective-permute-start | bytes 1572872 | tf_op jit(solution)/shard_map/ppermute | solution.py:523
  217.2 1.4 copy-start.10
  218.5 20.7 %copy-start = (bf16[1,1024,1024]{2,1,0:T(8,128)(2,1)S(1)}, bf16[1,1024,1024]{2,1,0:T(8,128)(2,1)}, u32[]{:S(2)}) copy-start(bf16[1,1024,1024]{2,1,0:T(8,128)(2,1)} %param.26) | copy-start | bytes 6291460
  218.5 20.7 %copy-start.4 = (bf16[512,512]{1,0:T(8,128)(2,1)S(1)}, bf16[512,512]{1,0:T(8,128)(2,1)}, u32[]{:S(2)}) copy-start(bf16[512,512]{1,0:T(8,128)(2,1)} %hidden.2.h_own) | copy-start | bytes 1572868
  218.5 20.7 %copy-start.8 = (s32[4]{0:T(128)S(1)}, s32[4]{0:T(128)}, u32[]{:S(2)}) copy-start(s32[4]{0:T(128)} %pad_add_fusion.src) | copy-start | bytes 52
  243.6 1.4 copy-start.2
  244.9 7.7 %copy-start.18 = (f32[4,136,128]{2,1,0:T(8,128)S(1)}, f32[4,136,128]{2,1,0:T(8,128)}, u32[]{:S(2)}) copy-start(f32[4,136,128]{2,1,0:T(8,128)} %get-tuple-element.23) | copy-start | bytes 835588
  244.9 10.2 %copy-start.3 = (bf16[512,512]{1,0:T(8,128)(2,1)S(1)}, bf16[512,512]{1,0:T(8,128)(2,1)}, u32[]{:S(2)}) copy-start(bf16[512,512]{1,0:T(8,128)(2,1)} %hidden.3.h_own) | copy-start | bytes 1572868
  244.9 48.5 %all-to-all-start.3 = ((bf16[32,8,4096]{2,1,0:T(8,128)(2,1)}), bf16[32,8,4096]{2,1,0:T(8,128)(2,1)}, u32[]{:S(2)}, u32[]{:S(2)}) async-start(bf16[32,8,4096]{2,1,0:T(8,128)(2,1)} %bitcast.41), calls=%async_computation.3 | async-start | bytes 4194304 | tf_op jit(solution)/shard_map/all_to_all | solution.py:535
  252.6 1.6 collective-permute-start.3
  254.3 0.7 copy-start.19
  255.1 32.5 %collective-permute-start.16 = (bf16[512,512]{1,0:T(8,128)(2,1)S(1)}, bf16[512,512]{1,0:T(8,128)(2,1)S(1)}, u32[]{:S(2)}, u32[]{:S(2)}) collective-permute-start(bf16[512,512]{1,0:T(8,128)(2,1)S(1)} %copy-done.3), channel_id=1, source_target_pairs={{0,1},{1,0},{2,3},{3,2},{4,5},{5,4},{6,7},{7,6},{8,9},{9,8},{10,11... | collective-permute-start | bytes 1572872 | tf_op jit(solution)/shard_map/ppermute | solution.py:519
  256.6 31.0 %collective-permute-start.17 = (bf16[512,512]{1,0:T(8,128)(2,1)S(1)}, bf16[512,512]{1,0:T(8,128)(2,1)}, u32[]{:S(2)}, u32[]{:S(2)}) collective-permute-start(bf16[512,512]{1,0:T(8,128)(2,1)S(1)} %copy-done.3), channel_id=1, source_target_pairs={{0,3},{1,2},{2,1},{3,0},{4,7},{5,6},{6,5},{7,4},{8,11},{9,10},{10,... | collective-permute-start | bytes 1572872 | tf_op jit(solution)/shard_map/ppermute | solution.py:523
  258.7 28.9 %collective-permute-start.18 = (bf16[512,512]{1,0:T(8,128)(2,1)S(1)}, bf16[512,512]{1,0:T(8,128)(2,1)}, u32[]{:S(2)}, u32[]{:S(2)}) collective-permute-start(bf16[512,512]{1,0:T(8,128)(2,1)S(1)} %copy-done.3), channel_id=1, source_target_pairs={{0,2},{1,3},{2,0},{3,1},{4,6},{5,7},{6,4},{7,5},{8,10},{9,11},{10,... | collective-permute-start | bytes 1572872 | tf_op jit(solution)/shard_map/ppermute | solution.py:529
  259.4 0.7 copy-start.13
  260.7 21.5 %collective-permute-start.4 = (f32[2,136,128]{2,1,0:T(8,128)}, f32[2,136,128]{2,1,0:T(8,128)}, u32[]{:S(2)}, u32[]{:S(2)}) collective-permute-start(f32[2,136,128]{2,1,0:T(8,128)} %pad_maximum_fusion.1), channel_id=1, source_target_pairs={{0,24},{8,0},{16,8},{24,16},{1,25},{9,1},{17,9},{25,17},{2,26},{10... | collective-permute-start | bytes 417800 | tf_op jit(solution)/shard_map/ppermute | solution.py:326
  261.0 23.6 %collective-permute-start.5 = (f32[2,136,128]{2,1,0:T(8,128)}, f32[2,136,128]{2,1,0:T(8,128)}, u32[]{:S(2)}, u32[]{:S(2)}) collective-permute-start(f32[2,136,128]{2,1,0:T(8,128)} %pad_maximum_fusion.1), channel_id=1, source_target_pairs={{0,16},{8,24},{16,0},{24,8},{1,17},{9,25},{17,1},{25,9},{2,18},{10... | collective-permute-start | bytes 417800 | tf_op jit(solution)/shard_map/ppermute | solution.py:326
  282.2 5.4 %collective-permute-start.6 = (f32[2,136,128]{2,1,0:T(8,128)}, f32[2,136,128]{2,1,0:T(8,128)}, u32[]{:S(2)}, u32[]{:S(2)}) collective-permute-start(f32[2,136,128]{2,1,0:T(8,128)} %pad_maximum_fusion.1), channel_id=1, source_target_pairs={{0,8},{8,16},{16,24},{24,0},{1,9},{9,17},{17,25},{25,1},{2,10},{10... | collective-permute-start | bytes 417800 | tf_op jit(solution)/shard_map/ppermute | solution.py:326
  292.1 1.4 copy-start.1
  293.4 9.3 %copy-start.14 = (f32[2,128,128]{2,1,0:T(8,128)S(1)}, f32[2,128,128]{2,1,0:T(8,128)}, u32[]{:S(2)}) copy-start(f32[2,128,128]{2,1,0:T(8,128)} %copy-done.13) | copy-start | bytes 393220
  293.4 15.6 %copy-start.21 = (bf16[2,32,128]{2,1,0:T(8,128)(2,1)S(1)}, bf16[2,32,128]{2,1,0:T(8,128)(2,1)}, u32[]{:S(2)}) copy-start(bf16[2,32,128]{2,1,0:T(8,128)(2,1)} %get-tuple-element.39) | copy-start | bytes 49156
  293.4 20.5 %copy-start.7 = (s32[512,2]{0,1:T(2,128)S(1)}, s32[512,2]{0,1:T(2,128)}, u32[]{:S(2)}) copy-start(s32[512,2]{0,1:T(2,128)} %param.27) | copy-start | bytes 12292
  293.5 49.6 %all-to-all-start.4 = ((bf16[32,8,4096]{2,1,0:T(8,128)(2,1)}), bf16[32,8,4096]{2,1,0:T(8,128)(2,1)S(1)}, u32[]{:S(2)}, u32[]{:S(2)}) async-start(bf16[32,8,4096]{2,1,0:T(8,128)(2,1)} %bitcast.39), calls=%async_computation.4 | async-start | bytes 4194304 | tf_op jit(solution)/shard_map/all_to_all | solution.py:535
  302.8 35.1 %copy-start.9 = (f32[512]{0:T(512)S(1)}, f32[512]{0:T(512)}, u32[]{:S(2)}) copy-start(f32[512]{0:T(512)} %param.21) | copy-start | bytes 6148
  304.6 26.1 %collective-permute-start.13 = (f32[2,136,128]{2,1,0:T(8,128)}, f32[2,136,128]{2,1,0:T(8,128)}, u32[]{:S(2)}, u32[]{:S(2)}) collective-permute-start(f32[2,136,128]{2,1,0:T(8,128)} %pad_maximum_fusion.2), channel_id=1, source_target_pairs={{0,96},{32,0},{64,32},{96,64},{1,97},{33,1},{65,33},{97,65},{2,98}... | collective-permute-start | bytes 417800 | tf_op jit(solution)/shard_map/ppermute | solution.py:344
  307.4 24.9 %collective-permute-start.14 = (f32[2,136,128]{2,1,0:T(8,128)}, f32[2,136,128]{2,1,0:T(8,128)}, u32[]{:S(2)}, u32[]{:S(2)}) collective-permute-start(f32[2,136,128]{2,1,0:T(8,128)} %pad_maximum_fusion.2), channel_id=1, source_target_pairs={{0,64},{32,96},{64,0},{96,32},{1,65},{33,97},{65,1},{97,33},{2,66}... | collective-permute-start | bytes 417800 | tf_op jit(solution)/shard_map/ppermute | solution.py:344
  308.2 26.2 %collective-permute-start.15 = (f32[2,136,128]{2,1,0:T(8,128)}, f32[2,136,128]{2,1,0:T(8,128)}, u32[]{:S(2)}, u32[]{:S(2)}) collective-permute-start(f32[2,136,128]{2,1,0:T(8,128)} %pad_maximum_fusion.2), channel_id=1, source_target_pairs={{0,32},{32,64},{64,96},{96,0},{1,33},{33,65},{65,97},{97,1},{2,34}... | collective-permute-start | bytes 417800 | tf_op jit(solution)/shard_map/ppermute | solution.py:344
  309.0 4.9 %collective-permute-start.20 = (bf16[2,32,128]{2,1,0:T(8,128)(2,1)S(1)}, bf16[2,32,128]{2,1,0:T(8,128)(2,1)S(1)}, u32[]{:S(2)}, u32[]{:S(2)}) collective-permute-start(bf16[2,32,128]{2,1,0:T(8,128)(2,1)S(1)} %copy-done.21), channel_id=1, source_target_pairs={{0,3},{1,2},{2,1},{3,0},{4,7},{5,6},{6,5},{7,4},{8,11},{9,10},{10,... | collective-permute-start | bytes 49160 | tf_op jit(solution)/shard_map/ppermute | solution.py:523
  336.4 1.4 collective-permute-start.19
  337.9 1.2 copy-start.5
  339.1 1.2 copy-start.6
